TPU v7x, 32 devices: a whole 2x2x4 slice. The times are simulated.
32 devices in a mesh: row: 8 (over z, core), col: 4 (over y, x).
Axes of the slice: x: 2, y: 2, z: 4, core: 2. Of those that a mesh axis runs over, the one named last changes fastest.
Arguments:
- mix_input: bfloat16 [4, 2048, 1024], P('col', 'row'), may hold values from -6 to 6
- gate_logits: bfloat16 [4, 2048, 2048], P('col', 'row'), may hold values from -8 to 8
- w_proj: bfloat16 [1024, 2048], P('col'), may hold values from -0.1875 to 0.1875
Outputs:
- mixed: bfloat16 [4, 2048, 2048], P('col', 'row')
All inputs are finite; a program needn't handle non-finite values.
Results may differ from a plain program's by a relative error of at most 0.0049.
Values may be sent and summed in bfloat16 or wider, within the bound.
No kernel may reach another device: no remote copies, remote signals or barrier semaphores. Data moves between devices by JAX's collectives and lax.ppermute only.
A program may use at most 64 MiB of HBM per device.

v0:
```python
import functools
import math

import jax
import jax.numpy as jnp
import numpy as np
from jax import lax
from jax.experimental import pallas as pl
from jax.experimental.pallas import tpu as pltpu
from jax.sharding import PartitionSpec as P


GROUP = 256
CHUNKS = 2
MIB = 1 << 20


def split_halves(table):
    head = table.astype(jnp.bfloat16)
    return head, (table - head.astype(np.float64)).astype(jnp.bfloat16)


def feature_table(pairs):
    chunks = GROUP // (2 * pairs)
    out = np.zeros((chunks, 2 * pairs, GROUP))
    m = np.arange(GROUP)
    for t in range(chunks):
        for j in range(pairs):
            c = pairs * t + j
            out[t, j] = np.cos(2 * math.pi * (m * c % GROUP) / GROUP)
            out[t, pairs + j] = -np.sin(2 * math.pi * (m * c % GROUP) / GROUP)
        if t == 0:
            out[0, pairs] = np.where(m % 2 == 0, 1.0, -1.0)
    return out


def position_table(inner, scale):
    angle = 2 * math.pi * (np.outer(np.arange(inner), np.arange(inner)) % inner) / inner
    return np.concatenate([np.cos(angle), np.sin(angle)], axis=1) * scale


def twist_table(rows, inner):
    length = rows * inner
    n2 = np.arange(inner)[:, None]
    res = []
    for core in range(2):
        k1 = 2 * np.arange(rows // 2)[None, :] + core
        angle = 2 * math.pi * (n2 * k1 % length) / length
        res.append(np.concatenate([np.cos(angle), np.sin(angle)], axis=1))
    return np.stack(res).astype(np.float32)


def vmem_call(body, outs, scratch, flops, moved, limit=24):
    return pl.pallas_call(
        body,
        out_shape=outs,
        scratch_shapes=scratch,
        compiler_params=pltpu.CompilerParams(vmem_limit_bytes=limit * MIB),
        cost_estimate=pl.CostEstimate(flops=flops, bytes_accessed=moved, transcendentals=0),
    )


def pick_kernel(chips, q, x_ref, *outs):
    chip = lax.axis_index("row") // 2
    lanes = outs[0].shape[1]
    pairs = lanes // 2
    chips_per_group = GROUP // (CHUNKS * lanes)
    src = lax.broadcasted_iota(jnp.int32, (GROUP, lanes), 0)
    lane = lax.broadcasted_iota(jnp.int32, (GROUP, lanes), 1)
    for zs in range(chips):
        dest = chip ^ zs
        group = dest // chips_per_group
        part = (dest % chips_per_group) * CHUNKS + q
        j = lane - pairs
        mirrored = jnp.where((j == 0) & (part == 0), GROUP // 2, GROUP - pairs * part - j)
        wanted = jnp.where(lane < pairs, pairs * part + lane, mirrored)
        choose = (src == wanted).astype(jnp.bfloat16)
        block = x_ref[:, pl.ds(pl.multiple_of(group * GROUP, GROUP), GROUP)]
        outs[zs][...] = jnp.dot(block, choose, preferred_element_type=jnp.float32).astype(
            jnp.bfloat16
        )


def complex_dft(values):
    n = len(values)
    if n == 1:
        return values
    even, odd = complex_dft(values[0::2]), complex_dft(values[1::2])
    low, high = [], []
    for k in range(n // 2):
        c, s = math.cos(2 * math.pi * k / n), math.sin(2 * math.pi * k / n)
        re, im = odd[k]
        if k == 0:
            tr, ti = re, im
        elif 4 * k == n:
            tr, ti = im, -re
        else:
            tr, ti = re * c + im * s, im * c - re * s
        er, ei = even[k]
        low.append((er + tr, ei + ti))
        high.append((er - tr, ei - ti))
    return low + high


def position_kernel(rows, q, *refs):
    chips = rows // 2
    mine, theirs = refs[:chips], refs[chips]
    table_hi, table_lo, twist = refs[chips + 1 : chips + 4]
    outs = refs[chips + 4 : 2 * chips + 4]
    folded, z_hi, z_lo, spect = refs[2 * chips + 4 :]
    inner, lanes = mine[0].shape
    pairs = lanes // 2
    row = lax.axis_index("row")
    core, chip = row % 2, row // 2
    half = rows // 2

    lane = lax.broadcasted_iota(jnp.int32, (1, lanes), 1)
    chips_per_group = GROUP // (CHUNKS * lanes)
    first = (chip % chips_per_group == 0) if q == 0 else False
    lone_low = (lane == 0) & first
    lone_high = (lane == pairs) & first
    own = jnp.where((lane < pairs) | lone_high, 1.0, -1.0).astype(jnp.float32)
    other = jnp.where(lone_low | lone_high, 0.0, 1.0).astype(jnp.float32)
    cosine = (lane < pairs) | lone_high

    def fold(block):
        value = block.astype(jnp.float32)
        if lanes % 128 == 0:
            turned = pltpu.roll(value, pairs, 1)
        else:
            turned = jnp.concatenate([value[:, pairs:], value[:, :pairs]], axis=1)
        return value * own + turned * other

    for zs in range(chips):
        folded[row ^ (2 * zs)] = fold(mine[zs][...])
        folded[row ^ (2 * zs + 1)] = fold(theirs[zs])

    odd_core = core == 1
    sign = jnp.where(odd_core, -1.0, 1.0).astype(jnp.float32)
    turns = []
    for n in range(half):
        angle = 2 * math.pi * n / rows
        turns.append(
            (
                jnp.where(odd_core, math.cos(angle), 1.0).astype(jnp.float32),
                jnp.where(odd_core, -math.sin(angle), 0.0).astype(jnp.float32),
            )
        )
    tile = min(inner, 32)

    def step(i, carry):
        at = pl.ds(pl.multiple_of(i * tile, tile), tile)
        low_at = pl.ds(pl.multiple_of(inner + i * tile, tile), tile)
        values = []
        for n in range(half):
            v = folded[n, at, :] + sign * folded[n + half, at, :]
            values.append((v * turns[n][0], v * turns[n][1]))
        tw = twist[core, at, :]
        for j, (re, im) in enumerate(complex_dft(values)):
            a = jnp.where(cosine, re, -im)
            b = jnp.where(cosine, im, re)
            c, s = tw[:, j : j + 1], tw[:, half + j : half + j + 1]
            for where, z in ((at, a * c + b * s), (low_at, b * c - a * s)):
                head = z.astype(jnp.bfloat16)
                cols = slice(j * lanes, (j + 1) * lanes)
                z_hi[where, cols] = head
                z_lo[where, cols] = (z - head.astype(jnp.float32)).astype(jnp.bfloat16)
        return carry

    lax.fori_loop(0, inner // tile, step, 0)
    dot = functools.partial(jnp.dot, preferred_element_type=jnp.float32)
    width = min(half * lanes, 256)
    for start in range(0, half * lanes, width):
        cols = slice(start, start + width)
        value = dot(table_hi[...], z_hi[:, cols])
        value += dot(table_hi[...], z_lo[:, cols])
        value += dot(table_lo[...], z_hi[:, cols])
        for j in range(start // lanes, (start + width) // lanes):
            piece = value[:, j * lanes - start : (j + 1) * lanes - start]
            spect[j] = piece
    per = inner // rows
    for zs in range(chips):
        for rel in range(2):
            dest = row ^ (2 * zs + rel)
            for j in range(half):
                outs[zs][rel, j * per : (j + 1) * per, :] = spect[
                    j, pl.ds(pl.multiple_of(dest * per, per), per), :
                ].astype(jnp.bfloat16)


def order_rows(rows, count):
    core = lax.axis_index("row") % 2
    half, per = rows // 2, count // rows
    natural = lax.broadcasted_iota(jnp.int32, (count, count), 0)
    received = lax.broadcasted_iota(jnp.int32, (count, count), 1)
    rel, j, k2 = received // (half * per), received // per % half, received % per
    return (natural == rows * k2 + 2 * j + (core ^ rel)).astype(jnp.bfloat16)


def give_kernel(*refs):
    out = refs[-1]
    for zs, ref in enumerate(refs[:-1]):
        out[zs] = ref[1]


def channel_part(order, mine, theirs, feat_hi, feat_lo):
    lanes = feat_hi.shape[0]
    got = jnp.concatenate(
        [jnp.concatenate([m[0], theirs[zs]], axis=0) for zs, m in enumerate(mine)], axis=1
    )
    got = jnp.dot(order, got, preferred_element_type=jnp.float32).astype(jnp.bfloat16)
    parts = []
    for zs in range(len(mine)):
        piece = got[:, zs * lanes : (zs + 1) * lanes]
        part = jnp.dot(piece, feat_hi, preferred_element_type=jnp.float32)
        parts.append(part + jnp.dot(piece, feat_lo, preferred_element_type=jnp.float32))
    return parts


def prepare_kernel(rows, *refs):
    chips = rows // 2
    mine, theirs, feat_hi, feat_lo, gate_ref = refs[:chips], *refs[chips : chips + 4]
    spect, opened = refs[chips + 4 :]
    order = order_rows(rows, gate_ref.shape[0])
    for zs, part in enumerate(channel_part(order, mine, theirs, feat_hi[...], feat_lo[...])):
        spect[zs] = part
    for start in range(0, gate_ref.shape[1], GROUP):
        cols = slice(start, start + GROUP)
        opened[:, cols] = jax.nn.sigmoid(gate_ref[:, cols].astype(jnp.float32))


def final_kernel(rows, n_col, *refs):
    chips = rows // 2
    mine, theirs, feat_hi, feat_lo, spect, opened = refs[:chips], *refs[chips : chips + 5]
    at = chips + 5
    w_here = refs[at]
    w_own = refs[at + 1 : at + n_col]
    w_other = refs[at + n_col : at + 2 * n_col - 1]
    out_ref, lhs, result, sems = refs[at + 2 * n_col - 1 :]
    count, width = opened.shape
    half = GROUP // 2
    row, col = lax.axis_index("row"), lax.axis_index("col")
    core, chip = row % 2, row // 2
    order = order_rows(rows, count)
    for zs, part in enumerate(channel_part(order, mine, theirs, feat_hi[...], feat_lo[...])):
        whole = (part + spect[zs]).astype(jnp.bfloat16)
        for h in range(2):
            spot = pl.ds(pl.multiple_of((core ^ h) * half, half), half)
            lhs[zs, :, spot] = whole[:, h * half : (h + 1) * half]
    copies = []
    for t in range(width // GROUP):
        cols = slice(t * GROUP, (t + 1) * GROUP)
        total = jnp.zeros((count, GROUP), jnp.float32)
        for s in range(n_col):
            if s == 0:
                own = w_here[pl.ds(pl.multiple_of(core * half, half), half), cols]
                other = w_here[pl.ds(pl.multiple_of((1 - core) * half, half), half), cols]
            else:
                own, other = w_own[s - 1][:, cols], w_other[s - 1][:, cols]
            rhs = jnp.concatenate([own, other], axis=0)
            total += jnp.dot(lhs[chip ^ col ^ s], rhs, preferred_element_type=jnp.float32)
        result[:, cols] = (opened[:, cols] * total).astype(jnp.bfloat16)
        copies.append(pltpu.make_async_copy(result.at[:, cols], out_ref.at[:, cols], sems.at[t]))
        copies[-1].start()
    for copy in copies:
        copy.wait()


def swap(value, axis, size, bit):
    return lax.ppermute(value, axis, [(i, i ^ bit) for i in range(size)])


def send_order(chips):
    return sorted(range(1, chips), key=lambda zs: (zs < 2, zs))


def across_chips(pieces, rows):
    chips = rows // 2
    got = [pieces[0]] + [None] * (chips - 1)
    for zs in send_order(chips):
        got[zs] = swap(pieces[zs], "row", rows, 2 * zs)
    return got


def on_device(mix_input, gate_logits, w_proj):
    return program(mix_input[0], gate_logits[0], w_proj)[None]


def program(tokens, gate, w_proj):
    count, features = tokens.shape
    rows, n_col = lax.axis_size("row"), lax.axis_size("col")
    chips = rows // 2
    lanes = features // (chips * CHUNKS)
    half = rows // 2
    width = w_proj.shape[1]
    scale = 1.0 / math.sqrt(count * rows * GROUP)
    table_hi, table_lo = split_halves(position_table(count, scale))
    twist = twist_table(rows, count)
    features_of = feature_table(lanes // 2)
    feat_hi, feat_lo = split_halves(features_of)
    bf = jnp.bfloat16
    fast = w_proj.shape[0] == GROUP and CHUNKS * lanes == GROUP and n_col == chips

    if fast:
        core = lax.axis_index("row") % 2
        mine = lax.dynamic_slice_in_dim(w_proj, core * (GROUP // 2), GROUP // 2, 0)
        w_own = []
        for s in range(1, n_col):
            w_own.append(swap(mine, "col", n_col, s))

    arrived = []
    for q in range(CHUNKS):
        picked = vmem_call(
            functools.partial(pick_kernel, chips, q),
            [jax.ShapeDtypeStruct((count, lanes), bf)] * chips,
            [],
            2 * count * GROUP * lanes * chips,
            3 * count * lanes * chips * 2,
        )(tokens)
        arrived.append(across_chips(picked, rows))

    spectra = []
    for q in range(CHUNKS):
        theirs = swap(jnp.stack(arrived[q]), "row", rows, 1)
        sent = vmem_call(
            functools.partial(position_kernel, rows, q),
            [jax.ShapeDtypeStruct((2, half * (count // rows), lanes), bf)] * chips,
            [
                pltpu.VMEM((rows, count, lanes), jnp.float32),
                pltpu.VMEM((2 * count, half * lanes), bf),
                pltpu.VMEM((2 * count, half * lanes), bf),
                pltpu.VMEM((half, count, lanes), jnp.float32),
            ],
            12 * count * count * half * lanes,
            rows * count * lanes * 4,
        )(*arrived[q], theirs, table_hi, table_lo, twist)
        spectra.append(across_chips(sent, rows))

    if fast:
        w_other = []
        for s in range(1, n_col):
            w_other.append(swap(w_own[s - 1], "row", rows, 1))
    operands = []
    for q in range(CHUNKS):
        give = vmem_call(
            give_kernel,
            jax.ShapeDtypeStruct((chips, half * (count // rows), lanes), bf),
            [],
            count * lanes * chips,
            2 * count * lanes * chips,
        )(*spectra[q])
        theirs = swap(give, "row", rows, 1)
        operands.append([*spectra[q], theirs])
    if fast:
        spect, opened = vmem_call(
            functools.partial(prepare_kernel, rows),
            [
                jax.ShapeDtypeStruct((chips, count, GROUP), jnp.float32),
                jax.ShapeDtypeStruct((count, width), jnp.float32),
            ],
            [],
            2 * count * features * GROUP,
            6 * count * width,
        )(*operands[0], feat_hi[0], feat_lo[0], gate)
        return pl.pallas_call(
            functools.partial(final_kernel, rows, n_col),
            out_shape=jax.ShapeDtypeStruct((count, width), bf),
            in_specs=[pl.BlockSpec(memory_space=pltpu.VMEM)] * (chips + 5 + 2 * n_col - 1),
            out_specs=pl.BlockSpec(memory_space=pl.ANY),
            scratch_shapes=[
                pltpu.VMEM((chips, count, GROUP), bf),
                pltpu.VMEM((count, width), bf),
                pltpu.SemaphoreType.DMA((width // GROUP,)),
            ],
            compiler_params=pltpu.CompilerParams(vmem_limit_bytes=32 * MIB),
            cost_estimate=pl.CostEstimate(
                flops=2 * count * features * width,
                bytes_accessed=2 * features * width,
                transcendentals=0,
            ),
        )(*operands[1], feat_hi[1], feat_lo[1], spect, opened, w_proj, *w_own, *w_other)

    weights = lax.all_gather(w_proj, "col", axis=0, tiled=True).reshape(-1, GROUP, width)
    order = order_rows(rows, count)
    chip = lax.axis_index("row") // 2
    table = jnp.asarray(features_of, jnp.float32).reshape(-1, CHUNKS, lanes, GROUP)
    per_group = table.shape[0]
    spectrum = jnp.zeros((count, weights.shape[0], GROUP), jnp.float32)
    here = chip ^ jnp.arange(chips)
    for q in range(CHUNKS):
        got = jnp.stack(
            [
                jnp.concatenate([operands[q][zs][0], operands[q][chips][zs]], axis=0)
                for zs in range(chips)
            ]
        )[here]
        got = jnp.einsum("kr,zrl->kzl", order, got, preferred_element_type=jnp.float32)
        spectrum += jnp.einsum(
            "kgtl,tlm->kgm",
            got.reshape(count, -1, per_group, lanes),
            table[:, q],
            precision=lax.Precision.HIGHEST,
        )
    total = jnp.einsum(
        "kgm,gmd->kd", spectrum.astype(bf), weights, preferred_element_type=jnp.float32
    )
    return (jax.nn.sigmoid(gate.astype(jnp.float32)) * total).astype(bf)


def solution(mesh):
    spec = P("col", "row", None)
    return jax.shard_map(
        on_device, mesh=mesh, in_specs=(spec, spec, P("col", None)), out_specs=spec, check_vma=False
    )
```

profile of v0, /device:TPU:0, one launch (start us, length us, event | category | flops | bytes accessed | tf_op | source)
XLA Modules:
  0.0 55.6 jit_solution(353914767492213948)
XLA Ops:
  0.0 1.2 %constant_dynamic-slice_fusion = bf16[128,2048]{1,0:T(8,128)(2,1)S(1)} fusion(bf16[256,2048]{1,0:T(8,128)(2,1)} %refs_9_.1, s32[]{:T(128)S(6)} %select_n.11), kind=kLoop, calls=%fused_computation.2 | loop fusion | bytes 1048580 | tf_op jit(solution)/shard_map/dynamic_slice | solution.py:306
  1.2 4.0 %collective-permute-start.18 = (bf16[128,2048]{1,0:T(8,128)(2,1)S(1)}, bf16[128,2048]{1,0:T(8,128)(2,1)S(1)}, u32[]{:S(2)}, u32[]{:S(2)}) collective-permute-start(bf16[128,2048]{1,0:T(8,128)(2,1)S(1)} %constant_dynamic-slice_fusion), channel_id=1, source_target_pairs={{0,3},{1,2},{2,1},{3,0},{4,7},{5,6},{6,5},{7,4},{8,11},{9,10},{10,... | collective-permute-start | bytes 1572872 | tf_op jit(solution)/shard_map/ppermute | solution.py:270
  5.2 0.5 collective-permute-start.17
  5.8 1.0 %copy-done.1 = bf16[1,256,1024]{2,1,0:T(8,128)(2,1)S(1)} copy-done((bf16[1,256,1024]{2,1,0:T(8,128)(2,1)S(1)}, bf16[1,256,1024]{2,1,0:T(8,128)(2,1)}, u32[]{:S(2)}) %copy-start.1) | copy-done | bytes 524312
  7.2 2.0 %collective-permute-start.8 = (bf16[256,128]{1,0:T(8,128)(2,1)S(1)}, bf16[256,128]{1,0:T(8,128)(2,1)S(1)}, u32[]{:S(2)}, u32[]{:S(2)}) collective-permute-start(bf16[256,128]{1,0:T(8,128)(2,1)S(1)} %get-tuple-element.32), channel_id=1, source_target_pairs={{0,8},{4,12},{8,0},{12,4},{16,24},{20,28},{24,16},{28,20},{1,9},{5... | collective-permute-start | bytes 196616 | tf_op jit(solution)/shard_map/ppermute | solution.py:270
  9.6 2.5 %collective-permute-done.8.refs_1_ = bf16[256,128]{1,0:T(8,128)(2,1)S(1)} collective-permute-done((bf16[256,128]{1,0:T(8,128)(2,1)S(1)}, bf16[256,128]{1,0:T(8,128)(2,1)S(1)}, u32[]{:S(2)}, u32[]{:S(2)}) %collective-permute-start.8) | collective-permute-done | bytes 65568 | tf_op jit(solution)/shard_map/ppermute | solution.py:270
  12.1 2.8 %collective-permute-start.1 = (bf16[256,128]{1,0:T(8,128)(2,1)S(1)}, bf16[256,128]{1,0:T(8,128)(2,1)S(1)}, u32[]{:S(2)}, u32[]{:S(2)}) collective-permute-start(bf16[256,128]{1,0:T(8,128)(2,1)S(1)} %get-tuple-element.25), channel_id=1, source_target_pairs={{0,16},{4,20},{8,24},{12,28},{16,0},{20,4},{24,8},{28,12},{1,17},{... | collective-permute-start | bytes 196616 | tf_op jit(solution)/shard_map/ppermute | solution.py:270
  14.9 1.4 %collective-permute-start.2 = (bf16[256,128]{1,0:T(8,128)(2,1)S(1)}, bf16[256,128]{1,0:T(8,128)(2,1)S(1)}, u32[]{:S(2)}, u32[]{:S(2)}) collective-permute-start(bf16[256,128]{1,0:T(8,128)(2,1)S(1)} %get-tuple-element.26), channel_id=1, source_target_pairs={{0,24},{4,28},{8,16},{12,20},{16,8},{20,12},{24,0},{28,4},{1,25},{... | collective-permute-start | bytes 196616 | tf_op jit(solution)/shard_map/ppermute | solution.py:270
  16.3 3.0 %collective-permute-done.1.refs_2_ = bf16[256,128]{1,0:T(8,128)(2,1)S(1)} collective-permute-done((bf16[256,128]{1,0:T(8,128)(2,1)S(1)}, bf16[256,128]{1,0:T(8,128)(2,1)S(1)}, u32[]{:S(2)}, u32[]{:S(2)}) %collective-permute-start.1) | collective-permute-done | bytes 65568 | tf_op jit(solution)/shard_map/ppermute | solution.py:270
  19.3 0.9 %collective-permute-start.9 = (bf16[256,128]{1,0:T(8,128)(2,1)S(1)}, bf16[256,128]{1,0:T(8,128)(2,1)S(1)}, u32[]{:S(2)}, u32[]{:S(2)}) collective-permute-start(bf16[256,128]{1,0:T(8,128)(2,1)S(1)} %get-tuple-element.33), channel_id=1, source_target_pairs={{0,16},{4,20},{8,24},{12,28},{16,0},{20,4},{24,8},{28,12},{1,17},{... | collective-permute-start | bytes 196616 | tf_op jit(solution)/shard_map/ppermute | solution.py:270
  20.1 0.8 %collective-permute-done.2.refs_3_ = bf16[256,128]{1,0:T(8,128)(2,1)S(1)} collective-permute-done((bf16[256,128]{1,0:T(8,128)(2,1)S(1)}, bf16[256,128]{1,0:T(8,128)(2,1)S(1)}, u32[]{:S(2)}, u32[]{:S(2)}) %collective-permute-start.2) | collective-permute-done | bytes 65568 | tf_op jit(solution)/shard_map/ppermute | solution.py:270
  20.9 1.9 %collective-permute-start.10 = (bf16[256,128]{1,0:T(8,128)(2,1)S(1)}, bf16[256,128]{1,0:T(8,128)(2,1)S(1)}, u32[]{:S(2)}, u32[]{:S(2)}) collective-permute-start(bf16[256,128]{1,0:T(8,128)(2,1)S(1)} %get-tuple-element.34), channel_id=1, source_target_pairs={{0,24},{4,28},{8,16},{12,20},{16,8},{20,12},{24,0},{28,4},{1,25},{... | collective-permute-start | bytes 196616 | tf_op jit(solution)/shard_map/ppermute | solution.py:270
  22.8 1.6 %collective-permute-done.9.refs_2_ = bf16[256,128]{1,0:T(8,128)(2,1)S(1)} collective-permute-done((bf16[256,128]{1,0:T(8,128)(2,1)S(1)}, bf16[256,128]{1,0:T(8,128)(2,1)S(1)}, u32[]{:S(2)}, u32[]{:S(2)}) %collective-permute-start.9) | collective-permute-done | bytes 65568 | tf_op jit(solution)/shard_map/ppermute | solution.py:270
  24.5 2.6 %collective-permute-done.10.refs_3_ = bf16[256,128]{1,0:T(8,128)(2,1)S(1)} collective-permute-done((bf16[256,128]{1,0:T(8,128)(2,1)S(1)}, bf16[256,128]{1,0:T(8,128)(2,1)S(1)}, u32[]{:S(2)}, u32[]{:S(2)}) %collective-permute-start.10) | collective-permute-done | bytes 65568 | tf_op jit(solution)/shard_map/ppermute | solution.py:270
  27.2 0.5 collective-permute-start.21
  27.7 0.6 %collective-permute-done.17.refs_11_ = bf16[128,2048]{1,0:T(8,128)(2,1)S(1)} collective-permute-done((bf16[128,2048]{1,0:T(8,128)(2,1)S(1)}, bf16[128,2048]{1,0:T(8,128)(2,1)S(1)}, u32[]{:S(2)}, u32[]{:S(2)}) %collective-permute-start.17) | collective-permute-done | bytes 524320 | tf_op jit(solution)/shard_map/ppermute | solution.py:270
  28.9 1.8 %shard_map.101 = (bf16[2,128,128]{2,1,0:T(8,128)(2,1)S(1)}, bf16[2,128,128]{2,1,0:T(8,128)(2,1)S(1)}, bf16[2,128,128]{2,1,0:T(8,128)(2,1)S(1)}, bf16[2,128,128]{2,1,0:T(8,128)(2,1)S(1)}) custom-call(bf16[256,128]{1,0:T(8,128)(2,1)S(1)} %get-tuple-element.23.refs_0_, bf16[256,128]{1,0:T(8,128)(2,1)S(1)} %collective-permute-done.refs_1_, ...), custom_call_target="tpu_custom_call" | custom-call | flops 402653184 | bytes 1048576 | tf_op jit(solution)/shard_map/pallas_call | solution.py:325
  30.7 1.8 %collective-permute-start.4 = (bf16[2,128,128]{2,1,0:T(8,128)(2,1)S(1)}, bf16[2,128,128]{2,1,0:T(8,128)(2,1)S(1)}, u32[]{:S(2)}, u32[]{:S(2)}) collective-permute-start(bf16[2,128,128]{2,1,0:T(8,128)(2,1)S(1)} %get-tuple-element.28), channel_id=1, source_target_pairs={{0,8},{4,12},{8,0},{12,4},{16,24},{20,28},{24,16},{28,20},{1,9},{5... | collective-permute-start | bytes 196616 | tf_op jit(solution)/shard_map/ppermute | solution.py:270
  32.5 1.8 %shard_map.104 = (bf16[2,128,128]{2,1,0:T(8,128)(2,1)S(1)}, bf16[2,128,128]{2,1,0:T(8,128)(2,1)S(1)}, bf16[2,128,128]{2,1,0:T(8,128)(2,1)S(1)}, bf16[2,128,128]{2,1,0:T(8,128)(2,1)S(1)}) custom-call(bf16[256,128]{1,0:T(8,128)(2,1)S(1)} %get-tuple-element.31.refs_0_, bf16[256,128]{1,0:T(8,128)(2,1)S(1)} %collective-permute-done.8.refs_1_, ...), custom_call_target="tpu_custom_call" | custom-call | flops 402653184 | bytes 1048576 | tf_op jit(solution)/shard_map/pallas_call | solution.py:325
  34.6 0.4 collective-permute-done.4.refs_1_
  35.0 2.8 %collective-permute-start.13 = (bf16[2,128,128]{2,1,0:T(8,128)(2,1)S(1)}, bf16[2,128,128]{2,1,0:T(8,128)(2,1)S(1)}, u32[]{:S(2)}, u32[]{:S(2)}) collective-permute-start(bf16[2,128,128]{2,1,0:T(8,128)(2,1)S(1)} %get-tuple-element.37), channel_id=1, source_target_pairs={{0,16},{4,20},{8,24},{12,28},{16,0},{20,4},{24,8},{28,12},{1,17},{... | collective-permute-start | bytes 196616 | tf_op jit(solution)/shard_map/ppermute | solution.py:270
  37.8 1.6 %collective-permute-done.12.refs_1_ = bf16[2,128,128]{2,1,0:T(8,128)(2,1)S(1)} collective-permute-done((bf16[2,128,128]{2,1,0:T(8,128)(2,1)S(1)}, bf16[2,128,128]{2,1,0:T(8,128)(2,1)S(1)}, u32[]{:S(2)}, u32[]{:S(2)}) %collective-permute-start.12) | collective-permute-done | bytes 65568 | tf_op jit(solution)/shard_map/ppermute | solution.py:270
  39.3 1.8 %collective-permute-start.14 = (bf16[2,128,128]{2,1,0:T(8,128)(2,1)S(1)}, bf16[2,128,128]{2,1,0:T(8,128)(2,1)S(1)}, u32[]{:S(2)}, u32[]{:S(2)}) collective-permute-start(bf16[2,128,128]{2,1,0:T(8,128)(2,1)S(1)} %get-tuple-element.38), channel_id=1, source_target_pairs={{0,24},{4,28},{8,16},{12,20},{16,8},{20,12},{24,0},{28,4},{1,25},{... | collective-permute-start | bytes 196616 | tf_op jit(solution)/shard_map/ppermute | solution.py:270
  41.1 1.3 %collective-permute-done.13.refs_2_ = bf16[2,128,128]{2,1,0:T(8,128)(2,1)S(1)} collective-permute-done((bf16[2,128,128]{2,1,0:T(8,128)(2,1)S(1)}, bf16[2,128,128]{2,1,0:T(8,128)(2,1)S(1)}, u32[]{:S(2)}, u32[]{:S(2)}) %collective-permute-start.13) | collective-permute-done | bytes 65568 | tf_op jit(solution)/shard_map/ppermute | solution.py:270
  42.4 0.6 %collective-permute-start.5 = (bf16[2,128,128]{2,1,0:T(8,128)(2,1)S(1)}, bf16[2,128,128]{2,1,0:T(8,128)(2,1)S(1)}, u32[]{:S(2)}, u32[]{:S(2)}) collective-permute-start(bf16[2,128,128]{2,1,0:T(8,128)(2,1)S(1)} %get-tuple-element.29), channel_id=1, source_target_pairs={{0,16},{4,20},{8,24},{12,28},{16,0},{20,4},{24,8},{28,12},{1,17},{... | collective-permute-start | bytes 196616 | tf_op jit(solution)/shard_map/ppermute | solution.py:270
  43.0 2.4 %collective-permute-done.14.refs_3_ = bf16[2,128,128]{2,1,0:T(8,128)(2,1)S(1)} collective-permute-done((bf16[2,128,128]{2,1,0:T(8,128)(2,1)S(1)}, bf16[2,128,128]{2,1,0:T(8,128)(2,1)S(1)}, u32[]{:S(2)}, u32[]{:S(2)}) %collective-permute-start.14) | collective-permute-done | bytes 65568 | tf_op jit(solution)/shard_map/ppermute | solution.py:270
  45.4 2.0 %collective-permute-start.6 = (bf16[2,128,128]{2,1,0:T(8,128)(2,1)S(1)}, bf16[2,128,128]{2,1,0:T(8,128)(2,1)S(1)}, u32[]{:S(2)}, u32[]{:S(2)}) collective-permute-start(bf16[2,128,128]{2,1,0:T(8,128)(2,1)S(1)} %get-tuple-element.30), channel_id=1, source_target_pairs={{0,24},{4,28},{8,16},{12,20},{16,8},{20,12},{24,0},{28,4},{1,25},{... | collective-permute-start | bytes 196616 | tf_op jit(solution)/shard_map/ppermute | solution.py:270
  47.4 1.3 %collective-permute-done.5.refs_2_ = bf16[2,128,128]{2,1,0:T(8,128)(2,1)S(1)} collective-permute-done((bf16[2,128,128]{2,1,0:T(8,128)(2,1)S(1)}, bf16[2,128,128]{2,1,0:T(8,128)(2,1)S(1)}, u32[]{:S(2)}, u32[]{:S(2)}) %collective-permute-start.5) | collective-permute-done | bytes 65568 | tf_op jit(solution)/shard_map/ppermute | solution.py:270
  48.6 2.9 %collective-permute-done.6.refs_3_ = bf16[2,128,128]{2,1,0:T(8,128)(2,1)S(1)} collective-permute-done((bf16[2,128,128]{2,1,0:T(8,128)(2,1)S(1)}, bf16[2,128,128]{2,1,0:T(8,128)(2,1)S(1)}, u32[]{:S(2)}, u32[]{:S(2)}) %collective-permute-start.6) | collective-permute-done | bytes 65568 | tf_op jit(solution)/shard_map/ppermute | solution.py:270
  51.7 0.8 %shard_map.106 = (f32[4,256,256]{2,1,0:T(8,128)S(1)}, f32[256,2048]{1,0:T(8,128)S(1)}) custom-call(bf16[2,128,128]{2,1,0:T(8,128)(2,1)S(1)} %get-tuple-element.35.refs_0_, bf16[2,128,128]{2,1,0:T(8,128)(2,1)S(1)} %collective-permute-done.12.refs_1_, bf16[2,128,128]{2,1,0:T(8,128)(2,1)S(1)} %collective-permute-done.13.refs_2_, ...), custom_call_target="tpu_custom_call" | custom-call | flops 134217728 | bytes 3145728 | tf_op jit(solution)/shard_map/pallas_call | solution.py:355
  52.4 0.5 collective-permute-done.7.refs_4_
  53.0 2.7 %shard_map.107 = bf16[256,2048]{1,0:T(8,128)(2,1)} custom-call(bf16[2,128,128]{2,1,0:T(8,128)(2,1)S(1)} %get-tuple-element.27.refs_0_, bf16[2,128,128]{2,1,0:T(8,128)(2,1)S(1)} %collective-permute-done.4.refs_1_, bf16[2,128,128]{2,1,0:T(8,128)(2,1)S(1)} %collective-permute-done.5.refs_2_, bf16[2,128,128]{2,1,0:T(8,128)(2,1)S(1)} %collective-permute-done.6.refs_3_, ...), custom_call_target="tpu_custom_call" | custom-call | flops 1073741824 | bytes 4194304 | tf_op jit(solution)/shard_map/pallas_call | solution.py:365
  (43 shorter events, 2.0 us)
Async XLA Ops:
  0.0 28.9 %copy-start.7 = (f32[2,256,8]{2,1,0:T(8,128)S(1)}, f32[2,256,8]{2,1,0:T(8,128)}, u32[]{:S(2)}) copy-start(f32[2,256,8]{2,1,0:T(8,128)} %constant.40.clone.refs_7_) | copy-start | bytes 49156
  0.0 28.9 %copy-start.8 = (bf16[256,512]{1,0:T(8,128)(2,1)S(1)}, bf16[256,512]{1,0:T(8,128)(2,1)}, u32[]{:S(2)}) copy-start(bf16[256,512]{1,0:T(8,128)(2,1)} %constant.39.clone.refs_6_) | copy-start | bytes 786436
  0.0 28.9 %copy-start.9 = (bf16[256,512]{1,0:T(8,128)(2,1)S(1)}, bf16[256,512]{1,0:T(8,128)(2,1)}, u32[]{:S(2)}) copy-start(bf16[256,512]{1,0:T(8,128)(2,1)} %constant.38.clone.refs_5_) | copy-start | bytes 786436
  1.2 26.0 %collective-permute-start.18 = (bf16[128,2048]{1,0:T(8,128)(2,1)S(1)}, bf16[128,2048]{1,0:T(8,128)(2,1)S(1)}, u32[]{:S(2)}, u32[]{:S(2)}) collective-permute-start(bf16[128,2048]{1,0:T(8,128)(2,1)S(1)} %constant_dynamic-slice_fusion), channel_id=1, source_target_pairs={{0,3},{1,2},{2,1},{3,0},{4,7},{5,6},{6,5},{7,4},{8,11},{9,10},{10,... | collective-permute-start | bytes 1572872 | tf_op jit(solution)/shard_map/ppermute | solution.py:270
  5.2 23.2 %collective-permute-start.17 = (bf16[128,2048]{1,0:T(8,128)(2,1)S(1)}, bf16[128,2048]{1,0:T(8,128)(2,1)S(1)}, u32[]{:S(2)}, u32[]{:S(2)}) collective-permute-start(bf16[128,2048]{1,0:T(8,128)(2,1)S(1)} %constant_dynamic-slice_fusion), channel_id=1, source_target_pairs={{0,2},{1,3},{2,0},{3,1},{4,6},{5,7},{6,4},{7,5},{8,10},{9,11},{10,... | collective-permute-start | bytes 1572872 | tf_op jit(solution)/shard_map/ppermute | solution.py:270
  5.7 22.9 %collective-permute-start.16 = (bf16[128,2048]{1,0:T(8,128)(2,1)S(1)}, bf16[128,2048]{1,0:T(8,128)(2,1)S(1)}, u32[]{:S(2)}, u32[]{:S(2)}) collective-permute-start(bf16[128,2048]{1,0:T(8,128)(2,1)S(1)} %constant_dynamic-slice_fusion), channel_id=1, source_target_pairs={{0,1},{1,0},{2,3},{3,2},{4,5},{5,4},{6,7},{7,6},{8,9},{9,8},{10,11... | collective-permute-start | bytes 1572872 | tf_op jit(solution)/shard_map/ppermute | solution.py:270
  5.8 1.0 %copy-start.1 = (bf16[1,256,1024]{2,1,0:T(8,128)(2,1)S(1)}, bf16[1,256,1024]{2,1,0:T(8,128)(2,1)}, u32[]{:S(2)}) copy-start(bf16[1,256,1024]{2,1,0:T(8,128)(2,1)} %param.10) | copy-start | bytes 1572868
  7.2 5.0 %collective-permute-start.8 = (bf16[256,128]{1,0:T(8,128)(2,1)S(1)}, bf16[256,128]{1,0:T(8,128)(2,1)S(1)}, u32[]{:S(2)}, u32[]{:S(2)}) collective-permute-start(bf16[256,128]{1,0:T(8,128)(2,1)S(1)} %get-tuple-element.32), channel_id=1, source_target_pairs={{0,8},{4,12},{8,0},{12,4},{16,24},{20,28},{24,16},{28,20},{1,9},{5... | collective-permute-start | bytes 196616 | tf_op jit(solution)/shard_map/ppermute | solution.py:270
  9.5 5.4 %collective-permute-start = (bf16[256,128]{1,0:T(8,128)(2,1)S(1)}, bf16[256,128]{1,0:T(8,128)(2,1)S(1)}, u32[]{:S(2)}, u32[]{:S(2)}) collective-permute-start(bf16[256,128]{1,0:T(8,128)(2,1)S(1)} %get-tuple-element.24), channel_id=1, source_target_pairs={{0,8},{4,12},{8,0},{12,4},{16,24},{20,28},{24,16},{28,20},{1,9},{5... | collective-permute-start | bytes 196616 | tf_op jit(solution)/shard_map/ppermute | solution.py:270
  12.1 7.2 %collective-permute-start.1 = (bf16[256,128]{1,0:T(8,128)(2,1)S(1)}, bf16[256,128]{1,0:T(8,128)(2,1)S(1)}, u32[]{:S(2)}, u32[]{:S(2)}) collective-permute-start(bf16[256,128]{1,0:T(8,128)(2,1)S(1)} %get-tuple-element.25), channel_id=1, source_target_pairs={{0,16},{4,20},{8,24},{12,28},{16,0},{20,4},{24,8},{28,12},{1,17},{... | collective-permute-start | bytes 196616 | tf_op jit(solution)/shard_map/ppermute | solution.py:270
  14.9 6.1 %collective-permute-start.2 = (bf16[256,128]{1,0:T(8,128)(2,1)S(1)}, bf16[256,128]{1,0:T(8,128)(2,1)S(1)}, u32[]{:S(2)}, u32[]{:S(2)}) collective-permute-start(bf16[256,128]{1,0:T(8,128)(2,1)S(1)} %get-tuple-element.26), channel_id=1, source_target_pairs={{0,24},{4,28},{8,16},{12,20},{16,8},{20,12},{24,0},{28,4},{1,25},{... | collective-permute-start | bytes 196616 | tf_op jit(solution)/shard_map/ppermute | solution.py:270
  19.3 5.2 %collective-permute-start.9 = (bf16[256,128]{1,0:T(8,128)(2,1)S(1)}, bf16[256,128]{1,0:T(8,128)(2,1)S(1)}, u32[]{:S(2)}, u32[]{:S(2)}) collective-permute-start(bf16[256,128]{1,0:T(8,128)(2,1)S(1)} %get-tuple-element.33), channel_id=1, source_target_pairs={{0,16},{4,20},{8,24},{12,28},{16,0},{20,4},{24,8},{28,12},{1,17},{... | collective-permute-start | bytes 196616 | tf_op jit(solution)/shard_map/ppermute | solution.py:270
  20.9 6.1 %collective-permute-start.10 = (bf16[256,128]{1,0:T(8,128)(2,1)S(1)}, bf16[256,128]{1,0:T(8,128)(2,1)S(1)}, u32[]{:S(2)}, u32[]{:S(2)}) collective-permute-start(bf16[256,128]{1,0:T(8,128)(2,1)S(1)} %get-tuple-element.34), channel_id=1, source_target_pairs={{0,24},{4,28},{8,16},{12,20},{16,8},{20,12},{24,0},{28,4},{1,25},{... | collective-permute-start | bytes 196616 | tf_op jit(solution)/shard_map/ppermute | solution.py:270
  24.5 4.4 %collective-permute-start.3 = (bf16[4,256,128]{2,1,0:T(8,128)(2,1)S(1)}, bf16[4,256,128]{2,1,0:T(8,128)(2,1)S(1)}, u32[]{:S(2)}, u32[]{:S(2)}) collective-permute-start(bf16[4,256,128]{2,1,0:T(8,128)(2,1)S(1)} %pad_maximum_fusion), channel_id=1, source_target_pairs={{0,4},{4,0},{8,12},{12,8},{16,20},{20,16},{24,28},{28,24},{1,5},{5... | collective-permute-start | bytes 786440 | tf_op jit(solution)/shard_map/ppermute | solution.py:270
  27.1 24.6 %copy-start.2 = (bf16[1,256,2048]{2,1,0:T(8,128)(2,1)S(1)}, bf16[1,256,2048]{2,1,0:T(8,128)(2,1)}, u32[]{:S(2)}) copy-start(bf16[1,256,2048]{2,1,0:T(8,128)(2,1)} %param.11) | copy-start | bytes 3145732
  27.1 24.6 %copy-start.5 = (bf16[128,256]{1,0:T(8,128)(2,1)S(1)}, bf16[128,256]{1,0:T(8,128)(2,1)}, u32[]{:S(2)}) copy-start(bf16[128,256]{1,0:T(8,128)(2,1)} %constant.42.clone.refs_6_) | copy-start | bytes 196612
  27.1 24.6 %copy-start.6 = (bf16[128,256]{1,0:T(8,128)(2,1)S(1)}, bf16[128,256]{1,0:T(8,128)(2,1)}, u32[]{:S(2)}) copy-start(bf16[128,256]{1,0:T(8,128)(2,1)} %constant.41.clone.refs_5_) | copy-start | bytes 196612
  27.1 5.4 %collective-permute-start.11 = (bf16[4,256,128]{2,1,0:T(8,128)(2,1)S(1)}, bf16[4,256,128]{2,1,0:T(8,128)(2,1)S(1)}, u32[]{:S(2)}, u32[]{:S(2)}) collective-permute-start(bf16[4,256,128]{2,1,0:T(8,128)(2,1)S(1)} %pad_maximum_fusion.1), channel_id=1, source_target_pairs={{0,4},{4,0},{8,12},{12,8},{16,20},{20,16},{24,28},{28,24},{1,5},{5... | collective-permute-start | bytes 786440 | tf_op jit(solution)/shard_map/ppermute | solution.py:270
  27.2 25.8 %collective-permute-start.21 = (bf16[128,2048]{1,0:T(8,128)(2,1)S(1)}, bf16[128,2048]{1,0:T(8,128)(2,1)S(1)}, u32[]{:S(2)}, u32[]{:S(2)}) collective-permute-start(bf16[128,2048]{1,0:T(8,128)(2,1)S(1)} %collective-permute-done.18.refs_12_), channel_id=1, source_target_pairs={{0,4},{4,0},{8,12},{12,8},{16,20},{20,16},{24,28},{28,24},{1,5},{5... | collective-permute-start | bytes 1572872 | tf_op jit(solution)/shard_map/ppermute | solution.py:270
  28.3 24.6 %collective-permute-start.20 = (bf16[128,2048]{1,0:T(8,128)(2,1)S(1)}, bf16[128,2048]{1,0:T(8,128)(2,1)S(1)}, u32[]{:S(2)}, u32[]{:S(2)}) collective-permute-start(bf16[128,2048]{1,0:T(8,128)(2,1)S(1)} %collective-permute-done.17.refs_11_), channel_id=1, source_target_pairs={{0,4},{4,0},{8,12},{12,8},{16,20},{20,16},{24,28},{28,24},{1,5},{5... | collective-permute-start | bytes 1572872 | tf_op jit(solution)/shard_map/ppermute | solution.py:270
  28.6 24.3 %collective-permute-start.19 = (bf16[128,2048]{1,0:T(8,128)(2,1)S(1)}, bf16[128,2048]{1,0:T(8,128)(2,1)S(1)}, u32[]{:S(2)}, u32[]{:S(2)}) collective-permute-start(bf16[128,2048]{1,0:T(8,128)(2,1)S(1)} %collective-permute-done.16.refs_10_), channel_id=1, source_target_pairs={{0,4},{4,0},{8,12},{12,8},{16,20},{20,16},{24,28},{28,24},{1,5},{5... | collective-permute-start | bytes 1572872 | tf_op jit(solution)/shard_map/ppermute | solution.py:270
  30.6 22.3 %copy-start = (bf16[256,2048]{1,0:T(8,128)(2,1)S(1)}, bf16[256,2048]{1,0:T(8,128)(2,1)}, u32[]{:S(2)}) copy-start(bf16[256,2048]{1,0:T(8,128)(2,1)} %refs_9_.1) | copy-start | bytes 3145732
  30.6 22.3 %copy-start.3 = (bf16[128,256]{1,0:T(8,128)(2,1)S(1)}, bf16[128,256]{1,0:T(8,128)(2,1)}, u32[]{:S(2)}) copy-start(bf16[128,256]{1,0:T(8,128)(2,1)} %constant.44.clone.refs_6_) | copy-start | bytes 196612
  30.7 22.3 %copy-start.4 = (bf16[128,256]{1,0:T(8,128)(2,1)S(1)}, bf16[128,256]{1,0:T(8,128)(2,1)}, u32[]{:S(2)}) copy-start(bf16[128,256]{1,0:T(8,128)(2,1)} %constant.43.clone.refs_5_) | copy-start | bytes 196612
  30.7 4.4 %collective-permute-start.4 = (bf16[2,128,128]{2,1,0:T(8,128)(2,1)S(1)}, bf16[2,128,128]{2,1,0:T(8,128)(2,1)S(1)}, u32[]{:S(2)}, u32[]{:S(2)}) collective-permute-start(bf16[2,128,128]{2,1,0:T(8,128)(2,1)S(1)} %get-tuple-element.28), channel_id=1, source_target_pairs={{0,8},{4,12},{8,0},{12,4},{16,24},{20,28},{24,16},{28,20},{1,9},{5... | collective-permute-start | bytes 196616 | tf_op jit(solution)/shard_map/ppermute | solution.py:270
  34.3 5.0 %collective-permute-start.12 = (bf16[2,128,128]{2,1,0:T(8,128)(2,1)S(1)}, bf16[2,128,128]{2,1,0:T(8,128)(2,1)S(1)}, u32[]{:S(2)}, u32[]{:S(2)}) collective-permute-start(bf16[2,128,128]{2,1,0:T(8,128)(2,1)S(1)} %get-tuple-element.36), channel_id=1, source_target_pairs={{0,8},{4,12},{8,0},{12,4},{16,24},{20,28},{24,16},{28,20},{1,9},{5... | collective-permute-start | bytes 196616 | tf_op jit(solution)/shard_map/ppermute | solution.py:270
  35.0 7.4 %collective-permute-start.13 = (bf16[2,128,128]{2,1,0:T(8,128)(2,1)S(1)}, bf16[2,128,128]{2,1,0:T(8,128)(2,1)S(1)}, u32[]{:S(2)}, u32[]{:S(2)}) collective-permute-start(bf16[2,128,128]{2,1,0:T(8,128)(2,1)S(1)} %get-tuple-element.37), channel_id=1, source_target_pairs={{0,16},{4,20},{8,24},{12,28},{16,0},{20,4},{24,8},{28,12},{1,17},{... | collective-permute-start | bytes 196616 | tf_op jit(solution)/shard_map/ppermute | solution.py:270
  39.3 6.1 %collective-permute-start.14 = (bf16[2,128,128]{2,1,0:T(8,128)(2,1)S(1)}, bf16[2,128,128]{2,1,0:T(8,128)(2,1)S(1)}, u32[]{:S(2)}, u32[]{:S(2)}) collective-permute-start(bf16[2,128,128]{2,1,0:T(8,128)(2,1)S(1)} %get-tuple-element.38), channel_id=1, source_target_pairs={{0,24},{4,28},{8,16},{12,20},{16,8},{20,12},{24,0},{28,4},{1,25},{... | collective-permute-start | bytes 196616 | tf_op jit(solution)/shard_map/ppermute | solution.py:270
  42.4 6.2 %collective-permute-start.5 = (bf16[2,128,128]{2,1,0:T(8,128)(2,1)S(1)}, bf16[2,128,128]{2,1,0:T(8,128)(2,1)S(1)}, u32[]{:S(2)}, u32[]{:S(2)}) collective-permute-start(bf16[2,128,128]{2,1,0:T(8,128)(2,1)S(1)} %get-tuple-element.29), channel_id=1, source_target_pairs={{0,16},{4,20},{8,24},{12,28},{16,0},{20,4},{24,8},{28,12},{1,17},{... | collective-permute-start | bytes 196616 | tf_op jit(solution)/shard_map/ppermute | solution.py:270
  45.4 6.1 %collective-permute-start.6 = (bf16[2,128,128]{2,1,0:T(8,128)(2,1)S(1)}, bf16[2,128,128]{2,1,0:T(8,128)(2,1)S(1)}, u32[]{:S(2)}, u32[]{:S(2)}) collective-permute-start(bf16[2,128,128]{2,1,0:T(8,128)(2,1)S(1)} %get-tuple-element.30), channel_id=1, source_target_pairs={{0,24},{4,28},{8,16},{12,20},{16,8},{20,12},{24,0},{28,4},{1,25},{... | collective-permute-start | bytes 196616 | tf_op jit(solution)/shard_map/ppermute | solution.py:270
  48.6 3.0 %collective-permute-start.15 = (bf16[4,128,128]{2,1,0:T(8,128)(2,1)S(1)}, bf16[4,128,128]{2,1,0:T(8,128)(2,1)S(1)}, u32[]{:S(2)}, u32[]{:S(2)}) collective-permute-start(bf16[4,128,128]{2,1,0:T(8,128)(2,1)S(1)} %shard_map.105), channel_id=1, source_target_pairs={{0,4},{4,0},{8,12},{12,8},{16,20},{20,16},{24,28},{28,24},{1,5},{5... | collective-permute-start | bytes 393224 | tf_op jit(solution)/shard_map/ppermute | solution.py:270
  51.5 1.4 %collective-permute-start.7 = (bf16[4,128,128]{2,1,0:T(8,128)(2,1)S(1)}, bf16[4,128,128]{2,1,0:T(8,128)(2,1)S(1)}, u32[]{:S(2)}, u32[]{:S(2)}) collective-permute-start(bf16[4,128,128]{2,1,0:T(8,128)(2,1)S(1)} %shard_map.102), channel_id=1, source_target_pairs={{0,4},{4,0},{8,12},{12,8},{16,20},{20,16},{24,28},{28,24},{1,5},{5... | collective-permute-start | bytes 393224 | tf_op jit(solution)/shard_map/ppermute | solution.py:270
where the time goes:
time: 55.8 us; the launch traced here: 55.6 us
  starting transfers between devices  23.8 us (43%)
  waiting for transfers between devices  21.8 us (39%)
  Pallas kernels  7.57 us (14%)
  local copies, waits for them, and re-layouts  2.24 us (4%)
    ppermute x22, starting transfers between devices, swap(): return lax.ppermute(value, axis, [(i, i ^ bit) for i in range(size)])  23.8 us
    ppermute x22, waiting for transfers between devices, swap(): return lax.ppermute(value, axis, [(i, i ^ bit) for i in range(size)])  21.8 us
    pallas_call x2, Pallas kernels, program(): vmem_call(functools.partial(position_kernel, rows, q), [jax.ShapeDtypeStr...  3.55 us
    pallas_call x1, Pallas kernels, program(): pl.pallas_call(functools.partial(final_kernel, rows, n_col), out_shape=ja...  2.65 us
    dynamic_slice x1, local copies, waits for them, and re-layouts, program(): mine = lax.dynamic_slice_in_dim(w_proj, core * (GROUP // 2), GROUP // 2, 0)  1.15 us
  transfers between devices with their start and end apart: 22, of which 14 were waited for; matrix products, arithmetic and copies ran while one was open for 0% of the time, Pallas kernels for 9%

commit v1 on v0

--- a/solution.py
+++ b/solution.py
@@ -229,14 +229,22 @@
         opened[:, cols] = jax.nn.sigmoid(gate_ref[:, cols].astype(jnp.float32))
 
 
-def final_kernel(rows, n_col, *refs):
+def cut_kernel(w_ref, out_ref):
+    half = GROUP // 2
+    core = lax.axis_index("row") % 2
+    out_ref[...] = w_ref[pl.ds(pl.multiple_of(core * half, half), half), :]
+
+
+def relay_kernel(first, second, to_first, to_second):
+    rows = to_first.shape[0]
+    to_first[...] = second[:rows, :]
+    to_second[...] = first[rows:, :]
+
+
+def final_kernel(rows, *refs):
     chips = rows // 2
     mine, theirs, feat_hi, feat_lo, spect, opened = refs[:chips], *refs[chips : chips + 5]
-    at = chips + 5
-    w_here = refs[at]
-    w_own = refs[at + 1 : at + n_col]
-    w_other = refs[at + n_col : at + 2 * n_col - 1]
-    out_ref, lhs, result, sems = refs[at + 2 * n_col - 1 :]
+    w_here, *w_far, out_ref, lhs, result, sems = refs[chips + 5 :]
     count, width = opened.shape
     half = GROUP // 2
     row, col = lax.axis_index("row"), lax.axis_index("col")
@@ -247,17 +255,22 @@
         for h in range(2):
             spot = pl.ds(pl.multiple_of((core ^ h) * half, half), half)
             lhs[zs, :, spot] = whole[:, h * half : (h + 1) * half]
+    first, second, low, high = (w_far[i::4] for i in range(4))
     copies = []
     for t in range(width // GROUP):
         cols = slice(t * GROUP, (t + 1) * GROUP)
         total = jnp.zeros((count, GROUP), jnp.float32)
-        for s in range(n_col):
+        for s in range(4):
             if s == 0:
-                own = w_here[pl.ds(pl.multiple_of(core * half, half), half), cols]
-                other = w_here[pl.ds(pl.multiple_of((1 - core) * half, half), half), cols]
+                parts = [
+                    w_here[pl.ds(pl.multiple_of(h * half, half), half), cols]
+                    for h in (core, 1 - core)
+                ]
+            elif s < 3:
+                parts = [ref[:, cols] for ref in (first, second)[s - 1]]
             else:
-                own, other = w_own[s - 1][:, cols], w_other[s - 1][:, cols]
-            rhs = jnp.concatenate([own, other], axis=0)
+                parts = [ref[:, cols] for pair in zip(low, high) for ref in pair]
+            rhs = jnp.concatenate(parts, axis=0)
             total += jnp.dot(lhs[chip ^ col ^ s], rhs, preferred_element_type=jnp.float32)
         result[:, cols] = (opened[:, cols] * total).astype(jnp.bfloat16)
         copies.append(pltpu.make_async_copy(result.at[:, cols], out_ref.at[:, cols], sems.at[t]))
@@ -299,14 +312,7 @@
     features_of = feature_table(lanes // 2)
     feat_hi, feat_lo = split_halves(features_of)
     bf = jnp.bfloat16
-    fast = w_proj.shape[0] == GROUP and CHUNKS * lanes == GROUP and n_col == chips
-
-    if fast:
-        core = lax.axis_index("row") % 2
-        mine = lax.dynamic_slice_in_dim(w_proj, core * (GROUP // 2), GROUP // 2, 0)
-        w_own = []
-        for s in range(1, n_col):
-            w_own.append(swap(mine, "col", n_col, s))
+    fast = w_proj.shape[0] == GROUP and CHUNKS * lanes == GROUP and n_col == chips == 4
 
     arrived = []
     for q in range(CHUNKS):
@@ -318,6 +324,17 @@
             3 * count * lanes * chips * 2,
         )(tokens)
         arrived.append(across_chips(picked, rows))
+
+    if fast:
+        w_own = []
+        piece = jax.ShapeDtypeStruct((GROUP // 2, width), bf)
+        part = jax.ShapeDtypeStruct((GROUP // 4, width), bf)
+        mine = vmem_call(cut_kernel, piece, [], GROUP * width, 2 * GROUP * width)(w_proj)
+        for s in (1, 2):
+            w_own.append(swap(mine, "col", n_col, s))
+        passed = vmem_call(relay_kernel, [part] * 2, [], GROUP * width, 2 * GROUP * width)(*w_own)
+        for s in (1, 2):
+            w_own.append(swap(passed[s - 1], "col", n_col, s))
 
     spectra = []
     for q in range(CHUNKS):
@@ -338,8 +355,8 @@
 
     if fast:
         w_other = []
-        for s in range(1, n_col):
-            w_other.append(swap(w_own[s - 1], "row", rows, 1))
+        for own in w_own:
+            w_other.append(swap(own, "row", rows, 1))
     operands = []
     for q in range(CHUNKS):
         give = vmem_call(
@@ -363,9 +380,9 @@
             6 * count * width,
         )(*operands[0], feat_hi[0], feat_lo[0], gate)
         return pl.pallas_call(
-            functools.partial(final_kernel, rows, n_col),
+            functools.partial(final_kernel, rows),
             out_shape=jax.ShapeDtypeStruct((count, width), bf),
-            in_specs=[pl.BlockSpec(memory_space=pltpu.VMEM)] * (chips + 5 + 2 * n_col - 1),
+            in_specs=[pl.BlockSpec(memory_space=pltpu.VMEM)] * (chips + 14),
             out_specs=pl.BlockSpec(memory_space=pl.ANY),
             scratch_shapes=[
                 pltpu.VMEM((chips, count, GROUP), bf),

time: 55.8 us -> 55.5 us (level)
  waiting for transfers between devices: 21.8 us -> 21 us
    unnamed x20 -> x24, local copies, waits for them, and re-layouts: 1.08 us -> 2.32 us
    dynamic_slice x1 -> x0, local copies, waits for them, and re-layouts: 1.15 us -> none  [program(): mine = lax.dynamic_slice_in_dim(w_proj, core * (GROUP // 2), GROUP // 2, 0)]
    ppermute x22 -> x24, waiting for transfers between devices: 21.8 us -> 21 us  [swap(): return lax.ppermute(value, axis, [(i, i ^ bit) for i in range(size)])]
    ppermute x22 -> x24, starting transfers between devices: 23.8 us -> 24 us  [swap(): return lax.ppermute(value, axis, [(i, i ^ bit) for i in range(size)])]
    pallas_call x1 -> x3, Pallas kernels: 2.65 us -> 2.73 us  [the longest x1 2.66 us: program(): pl.pallas_call(functools.partial(final_kernel, rows), out_shape=jax.Shape...]
  transfers between devices with their start and end apart: 22 -> 24, of which waited for: 14 -> 10; matrix products, arithmetic and copies ran while one was open for 0% -> 0% of each run, Pallas kernels for 9% -> 9%
where the time goes in v1:
time: 55.5 us; the launch traced here: 55.3 us
  starting transfers between devices  24 us (43%)
  waiting for transfers between devices  21 us (38%)
  Pallas kernels  7.65 us (14%)
  local copies, waits for them, and re-layouts  2.32 us (4%)
    ppermute x24, starting transfers between devices, swap(): return lax.ppermute(value, axis, [(i, i ^ bit) for i in range(size)])  24 us
    ppermute x24, waiting for transfers between devices, swap(): return lax.ppermute(value, axis, [(i, i ^ bit) for i in range(size)])  21 us
    pallas_call x2, Pallas kernels, program(): vmem_call(functools.partial(position_kernel, rows, q), [jax.ShapeDtypeStr...  3.55 us
    pallas_call x1, Pallas kernels, program(): pl.pallas_call(functools.partial(final_kernel, rows), out_shape=jax.Shape...  2.66 us
    unnamed x24, local copies, waits for them, and re-layouts  2.32 us
  transfers between devices with their start and end apart: 24, of which 10 were waited for; matrix products, arithmetic and copies ran while one was open for 0% of the time, Pallas kernels for 9%

profile of v1, /device:TPU:0, one launch (start us, length us, event | category | flops | bytes accessed | tf_op | source)
XLA Modules:
  0.0 55.3 jit_solution(2011572130292176273)
XLA Ops:
  0.0 1.0 %copy-done.2 = bf16[1,256,1024]{2,1,0:T(8,128)(2,1)S(1)} copy-done((bf16[1,256,1024]{2,1,0:T(8,128)(2,1)S(1)}, bf16[1,256,1024]{2,1,0:T(8,128)(2,1)}, u32[]{:S(2)}) %copy-start.2) | copy-done | bytes 524312
  1.0 0.3 shard_map.100
  1.3 3.1 %collective-permute-start = (bf16[256,128]{1,0:T(8,128)(2,1)S(1)}, bf16[256,128]{1,0:T(8,128)(2,1)S(1)}, u32[]{:S(2)}, u32[]{:S(2)}) collective-permute-start(bf16[256,128]{1,0:T(8,128)(2,1)S(1)} %get-tuple-element.26), channel_id=1, source_target_pairs={{0,8},{4,12},{8,0},{12,4},{16,24},{20,28},{24,16},{28,20},{1,9},{5... | collective-permute-start | bytes 196616 | tf_op jit(solution)/shard_map/ppermute | solution.py:283
  4.5 2.6 %collective-permute-start.1 = (bf16[256,128]{1,0:T(8,128)(2,1)S(1)}, bf16[256,128]{1,0:T(8,128)(2,1)S(1)}, u32[]{:S(2)}, u32[]{:S(2)}) collective-permute-start(bf16[256,128]{1,0:T(8,128)(2,1)S(1)} %get-tuple-element.27), channel_id=1, source_target_pairs={{0,16},{4,20},{8,24},{12,28},{16,0},{20,4},{24,8},{28,12},{1,17},{... | collective-permute-start | bytes 196616 | tf_op jit(solution)/shard_map/ppermute | solution.py:283
  7.1 1.2 %copy-done = bf16[256,2048]{1,0:T(8,128)(2,1)S(1)} copy-done((bf16[256,2048]{1,0:T(8,128)(2,1)S(1)}, bf16[256,2048]{1,0:T(8,128)(2,1)}, u32[]{:S(2)}) %copy-start) | copy-done | bytes 1048600
  8.3 1.8 %collective-permute-start.17 = (bf16[128,2048]{1,0:T(8,128)(2,1)S(1)}, bf16[128,2048]{1,0:T(8,128)(2,1)S(1)}, u32[]{:S(2)}, u32[]{:S(2)}) collective-permute-start(bf16[128,2048]{1,0:T(8,128)(2,1)S(1)} %shard_map.107), channel_id=1, source_target_pairs={{0,2},{1,3},{2,0},{3,1},{4,6},{5,7},{6,4},{7,5},{8,10},{9,11},{10,... | collective-permute-start | bytes 1572872 | tf_op jit(solution)/shard_map/ppermute | solution.py:283
  10.1 1.5 %collective-permute-start.16 = (bf16[128,2048]{1,0:T(8,128)(2,1)S(1)}, bf16[128,2048]{1,0:T(8,128)(2,1)S(1)}, u32[]{:S(2)}, u32[]{:S(2)}) collective-permute-start(bf16[128,2048]{1,0:T(8,128)(2,1)S(1)} %shard_map.107), channel_id=1, source_target_pairs={{0,1},{1,0},{2,3},{3,2},{4,5},{5,4},{6,7},{7,6},{8,9},{9,8},{10,11... | collective-permute-start | bytes 1572872 | tf_op jit(solution)/shard_map/ppermute | solution.py:283
  11.6 0.3 shard_map.103
  11.9 0.7 %collective-permute-start.8 = (bf16[256,128]{1,0:T(8,128)(2,1)S(1)}, bf16[256,128]{1,0:T(8,128)(2,1)S(1)}, u32[]{:S(2)}, u32[]{:S(2)}) collective-permute-start(bf16[256,128]{1,0:T(8,128)(2,1)S(1)} %get-tuple-element.34), channel_id=1, source_target_pairs={{0,8},{4,12},{8,0},{12,4},{16,24},{20,28},{24,16},{28,20},{1,9},{5... | collective-permute-start | bytes 196616 | tf_op jit(solution)/shard_map/ppermute | solution.py:283
  12.7 3.5 %collective-permute-start.9 = (bf16[256,128]{1,0:T(8,128)(2,1)S(1)}, bf16[256,128]{1,0:T(8,128)(2,1)S(1)}, u32[]{:S(2)}, u32[]{:S(2)}) collective-permute-start(bf16[256,128]{1,0:T(8,128)(2,1)S(1)} %get-tuple-element.35), channel_id=1, source_target_pairs={{0,16},{4,20},{8,24},{12,28},{16,0},{20,4},{24,8},{28,12},{1,17},{... | collective-permute-start | bytes 196616 | tf_op jit(solution)/shard_map/ppermute | solution.py:283
  16.5 3.3 %collective-permute-done.9.refs_2_ = bf16[256,128]{1,0:T(8,128)(2,1)S(1)} collective-permute-done((bf16[256,128]{1,0:T(8,128)(2,1)S(1)}, bf16[256,128]{1,0:T(8,128)(2,1)S(1)}, u32[]{:S(2)}, u32[]{:S(2)}) %collective-permute-start.9) | collective-permute-done | bytes 65568 | tf_op jit(solution)/shard_map/ppermute | solution.py:283
  19.8 2.4 %collective-permute-done.10.refs_3_ = bf16[256,128]{1,0:T(8,128)(2,1)S(1)} collective-permute-done((bf16[256,128]{1,0:T(8,128)(2,1)S(1)}, bf16[256,128]{1,0:T(8,128)(2,1)S(1)}, u32[]{:S(2)}, u32[]{:S(2)}) %collective-permute-start.10) | collective-permute-done | bytes 65568 | tf_op jit(solution)/shard_map/ppermute | solution.py:283
  22.4 1.8 %shard_map.101 = (bf16[2,128,128]{2,1,0:T(8,128)(2,1)S(1)}, bf16[2,128,128]{2,1,0:T(8,128)(2,1)S(1)}, bf16[2,128,128]{2,1,0:T(8,128)(2,1)S(1)}, bf16[2,128,128]{2,1,0:T(8,128)(2,1)S(1)}) custom-call(bf16[256,128]{1,0:T(8,128)(2,1)S(1)} %get-tuple-element.25.refs_0_, bf16[256,128]{1,0:T(8,128)(2,1)S(1)} %collective-permute-done.refs_1_, ...), custom_call_target="tpu_custom_call" | custom-call | flops 402653184 | bytes 1048576 | tf_op jit(solution)/shard_map/pallas_call | solution.py:342
  24.3 1.3 %collective-permute-start.5 = (bf16[2,128,128]{2,1,0:T(8,128)(2,1)S(1)}, bf16[2,128,128]{2,1,0:T(8,128)(2,1)S(1)}, u32[]{:S(2)}, u32[]{:S(2)}) collective-permute-start(bf16[2,128,128]{2,1,0:T(8,128)(2,1)S(1)} %get-tuple-element.31), channel_id=1, source_target_pairs={{0,16},{4,20},{8,24},{12,28},{16,0},{20,4},{24,8},{28,12},{1,17},{... | collective-permute-start | bytes 196616 | tf_op jit(solution)/shard_map/ppermute | solution.py:283
  25.6 1.8 %shard_map.104 = (bf16[2,128,128]{2,1,0:T(8,128)(2,1)S(1)}, bf16[2,128,128]{2,1,0:T(8,128)(2,1)S(1)}, bf16[2,128,128]{2,1,0:T(8,128)(2,1)S(1)}, bf16[2,128,128]{2,1,0:T(8,128)(2,1)S(1)}) custom-call(bf16[256,128]{1,0:T(8,128)(2,1)S(1)} %get-tuple-element.33.refs_0_, bf16[256,128]{1,0:T(8,128)(2,1)S(1)} %collective-permute-done.8.refs_1_, ...), custom_call_target="tpu_custom_call" | custom-call | flops 402653184 | bytes 1048576 | tf_op jit(solution)/shard_map/pallas_call | solution.py:342
  27.4 0.8 %collective-permute-start.12 = (bf16[2,128,128]{2,1,0:T(8,128)(2,1)S(1)}, bf16[2,128,128]{2,1,0:T(8,128)(2,1)S(1)}, u32[]{:S(2)}, u32[]{:S(2)}) collective-permute-start(bf16[2,128,128]{2,1,0:T(8,128)(2,1)S(1)} %get-tuple-element.38), channel_id=1, source_target_pairs={{0,8},{4,12},{8,0},{12,4},{16,24},{20,28},{24,16},{28,20},{1,9},{5... | collective-permute-start | bytes 196616 | tf_op jit(solution)/shard_map/ppermute | solution.py:283
  28.3 0.6 %collective-permute-start.18 = (bf16[64,2048]{1,0:T(8,128)(2,1)S(1)}, bf16[64,2048]{1,0:T(8,128)(2,1)S(1)}, u32[]{:S(2)}, u32[]{:S(2)}) collective-permute-start(bf16[64,2048]{1,0:T(8,128)(2,1)S(1)} %get-tuple-element.43), channel_id=1, source_target_pairs={{0,1},{1,0},{2,3},{3,2},{4,5},{5,4},{6,7},{7,6},{8,9},{9,8},{10,11... | collective-permute-start | bytes 786440 | tf_op jit(solution)/shard_map/ppermute | solution.py:283
  28.9 1.0 %collective-permute-done.4.refs_1_ = bf16[2,128,128]{2,1,0:T(8,128)(2,1)S(1)} collective-permute-done((bf16[2,128,128]{2,1,0:T(8,128)(2,1)S(1)}, bf16[2,128,128]{2,1,0:T(8,128)(2,1)S(1)}, u32[]{:S(2)}, u32[]{:S(2)}) %collective-permute-start.4) | collective-permute-done | bytes 65568 | tf_op jit(solution)/shard_map/ppermute | solution.py:283
  29.9 0.5 collective-permute-start.19
  30.4 0.8 %collective-permute-done.5.refs_2_ = bf16[2,128,128]{2,1,0:T(8,128)(2,1)S(1)} collective-permute-done((bf16[2,128,128]{2,1,0:T(8,128)(2,1)S(1)}, bf16[2,128,128]{2,1,0:T(8,128)(2,1)S(1)}, u32[]{:S(2)}, u32[]{:S(2)}) %collective-permute-start.5) | collective-permute-done | bytes 65568 | tf_op jit(solution)/shard_map/ppermute | solution.py:283
  31.2 0.7 %collective-permute-done.12.refs_1_ = bf16[2,128,128]{2,1,0:T(8,128)(2,1)S(1)} collective-permute-done((bf16[2,128,128]{2,1,0:T(8,128)(2,1)S(1)}, bf16[2,128,128]{2,1,0:T(8,128)(2,1)S(1)}, u32[]{:S(2)}, u32[]{:S(2)}) %collective-permute-start.12) | collective-permute-done | bytes 65568 | tf_op jit(solution)/shard_map/ppermute | solution.py:283
  31.9 1.5 %collective-permute-start.13 = (bf16[2,128,128]{2,1,0:T(8,128)(2,1)S(1)}, bf16[2,128,128]{2,1,0:T(8,128)(2,1)S(1)}, u32[]{:S(2)}, u32[]{:S(2)}) collective-permute-start(bf16[2,128,128]{2,1,0:T(8,128)(2,1)S(1)} %get-tuple-element.39), channel_id=1, source_target_pairs={{0,16},{4,20},{8,24},{12,28},{16,0},{20,4},{24,8},{28,12},{1,17},{... | collective-permute-start | bytes 196616 | tf_op jit(solution)/shard_map/ppermute | solution.py:283
  33.4 4.3 %collective-permute-done.13.refs_2_ = bf16[2,128,128]{2,1,0:T(8,128)(2,1)S(1)} collective-permute-done((bf16[2,128,128]{2,1,0:T(8,128)(2,1)S(1)}, bf16[2,128,128]{2,1,0:T(8,128)(2,1)S(1)}, u32[]{:S(2)}, u32[]{:S(2)}) %collective-permute-start.13) | collective-permute-done | bytes 65568 | tf_op jit(solution)/shard_map/ppermute | solution.py:283
  37.8 2.4 %collective-permute-start.14 = (bf16[2,128,128]{2,1,0:T(8,128)(2,1)S(1)}, bf16[2,128,128]{2,1,0:T(8,128)(2,1)S(1)}, u32[]{:S(2)}, u32[]{:S(2)}) collective-permute-start(bf16[2,128,128]{2,1,0:T(8,128)(2,1)S(1)} %get-tuple-element.40), channel_id=1, source_target_pairs={{0,24},{4,28},{8,16},{12,20},{16,8},{20,12},{24,0},{28,4},{1,25},{... | collective-permute-start | bytes 196616 | tf_op jit(solution)/shard_map/ppermute | solution.py:283
  40.2 3.6 %collective-permute-done.14.refs_3_ = bf16[2,128,128]{2,1,0:T(8,128)(2,1)S(1)} collective-permute-done((bf16[2,128,128]{2,1,0:T(8,128)(2,1)S(1)}, bf16[2,128,128]{2,1,0:T(8,128)(2,1)S(1)}, u32[]{:S(2)}, u32[]{:S(2)}) %collective-permute-start.14) | collective-permute-done | bytes 65568 | tf_op jit(solution)/shard_map/ppermute | solution.py:283
  43.8 2.4 %collective-permute-start.6 = (bf16[2,128,128]{2,1,0:T(8,128)(2,1)S(1)}, bf16[2,128,128]{2,1,0:T(8,128)(2,1)S(1)}, u32[]{:S(2)}, u32[]{:S(2)}) collective-permute-start(bf16[2,128,128]{2,1,0:T(8,128)(2,1)S(1)} %get-tuple-element.32), channel_id=1, source_target_pairs={{0,24},{4,28},{8,16},{12,20},{16,8},{20,12},{24,0},{28,4},{1,25},{... | collective-permute-start | bytes 196616 | tf_op jit(solution)/shard_map/ppermute | solution.py:283
  46.3 3.6 %collective-permute-done.6.refs_3_ = bf16[2,128,128]{2,1,0:T(8,128)(2,1)S(1)} collective-permute-done((bf16[2,128,128]{2,1,0:T(8,128)(2,1)S(1)}, bf16[2,128,128]{2,1,0:T(8,128)(2,1)S(1)}, u32[]{:S(2)}, u32[]{:S(2)}) %collective-permute-start.6) | collective-permute-done | bytes 65568 | tf_op jit(solution)/shard_map/ppermute | solution.py:283
  49.9 0.5 collective-permute-start.22
  50.5 0.7 %collective-permute-done.15.refs_4_ = bf16[4,128,128]{2,1,0:T(8,128)(2,1)S(1)} collective-permute-done((bf16[4,128,128]{2,1,0:T(8,128)(2,1)S(1)}, bf16[4,128,128]{2,1,0:T(8,128)(2,1)S(1)}, u32[]{:S(2)}, u32[]{:S(2)}) %collective-permute-start.15) | collective-permute-done | bytes 131104 | tf_op jit(solution)/shard_map/ppermute | solution.py:283
  51.4 0.8 %shard_map.106 = (f32[4,256,256]{2,1,0:T(8,128)S(1)}, f32[256,2048]{1,0:T(8,128)S(1)}) custom-call(bf16[2,128,128]{2,1,0:T(8,128)(2,1)S(1)} %get-tuple-element.37.refs_0_, bf16[2,128,128]{2,1,0:T(8,128)(2,1)S(1)} %collective-permute-done.12.refs_1_, bf16[2,128,128]{2,1,0:T(8,128)(2,1)S(1)} %collective-permute-done.13.refs_2_, ...), custom_call_target="tpu_custom_call" | custom-call | flops 134217728 | bytes 3145728 | tf_op jit(solution)/shard_map/pallas_call | solution.py:372
  52.2 0.4 collective-permute-done.7.refs_4_
  52.7 2.7 %shard_map.109 = bf16[256,2048]{1,0:T(8,128)(2,1)} custom-call(bf16[2,128,128]{2,1,0:T(8,128)(2,1)S(1)} %get-tuple-element.29.refs_0_, bf16[2,128,128]{2,1,0:T(8,128)(2,1)S(1)} %collective-permute-done.4.refs_1_, bf16[2,128,128]{2,1,0:T(8,128)(2,1)S(1)} %collective-permute-done.5.refs_2_, bf16[2,128,128]{2,1,0:T(8,128)(2,1)S(1)} %collective-permute-done.6.refs_3_, ...), custom_call_target="tpu_custom_call" | custom-call | flops 1073741824 | bytes 4194304 | tf_op jit(solution)/shard_map/pallas_call | solution.py:382
  (52 shorter events, 0.9 us)
Async XLA Ops:
  1.3 10.6 %collective-permute-start = (bf16[256,128]{1,0:T(8,128)(2,1)S(1)}, bf16[256,128]{1,0:T(8,128)(2,1)S(1)}, u32[]{:S(2)}, u32[]{:S(2)}) collective-permute-start(bf16[256,128]{1,0:T(8,128)(2,1)S(1)} %get-tuple-element.26), channel_id=1, source_target_pairs={{0,8},{4,12},{8,0},{12,4},{16,24},{20,28},{24,16},{28,20},{1,9},{5... | collective-permute-start | bytes 196616 | tf_op jit(solution)/shard_map/ppermute | solution.py:283
  4.5 8.2 %collective-permute-start.1 = (bf16[256,128]{1,0:T(8,128)(2,1)S(1)}, bf16[256,128]{1,0:T(8,128)(2,1)S(1)}, u32[]{:S(2)}, u32[]{:S(2)}) collective-permute-start(bf16[256,128]{1,0:T(8,128)(2,1)S(1)} %get-tuple-element.27), channel_id=1, source_target_pairs={{0,16},{4,20},{8,24},{12,28},{16,0},{20,4},{24,8},{28,12},{1,17},{... | collective-permute-start | bytes 196616 | tf_op jit(solution)/shard_map/ppermute | solution.py:283
  7.0 9.1 %collective-permute-start.2 = (bf16[256,128]{1,0:T(8,128)(2,1)S(1)}, bf16[256,128]{1,0:T(8,128)(2,1)S(1)}, u32[]{:S(2)}, u32[]{:S(2)}) collective-permute-start(bf16[256,128]{1,0:T(8,128)(2,1)S(1)} %get-tuple-element.28), channel_id=1, source_target_pairs={{0,24},{4,28},{8,16},{12,20},{16,8},{20,12},{24,0},{28,4},{1,25},{... | collective-permute-start | bytes 196616 | tf_op jit(solution)/shard_map/ppermute | solution.py:283
  8.3 14.1 %copy-start.10 = (bf16[256,512]{1,0:T(8,128)(2,1)S(1)}, bf16[256,512]{1,0:T(8,128)(2,1)}, u32[]{:S(2)}) copy-start(bf16[256,512]{1,0:T(8,128)(2,1)} %constant.15.clone.refs_6_) | copy-start | bytes 786436
  8.3 14.1 %copy-start.11 = (bf16[256,512]{1,0:T(8,128)(2,1)S(1)}, bf16[256,512]{1,0:T(8,128)(2,1)}, u32[]{:S(2)}) copy-start(bf16[256,512]{1,0:T(8,128)(2,1)} %constant.14.clone.refs_5_) | copy-start | bytes 786436
  8.3 19.9 %collective-permute-start.17 = (bf16[128,2048]{1,0:T(8,128)(2,1)S(1)}, bf16[128,2048]{1,0:T(8,128)(2,1)S(1)}, u32[]{:S(2)}, u32[]{:S(2)}) collective-permute-start(bf16[128,2048]{1,0:T(8,128)(2,1)S(1)} %shard_map.107), channel_id=1, source_target_pairs={{0,2},{1,3},{2,0},{3,1},{4,6},{5,7},{6,4},{7,5},{8,10},{9,11},{10,... | collective-permute-start | bytes 1572872 | tf_op jit(solution)/shard_map/ppermute | solution.py:283
  10.1 18.1 %collective-permute-start.16 = (bf16[128,2048]{1,0:T(8,128)(2,1)S(1)}, bf16[128,2048]{1,0:T(8,128)(2,1)S(1)}, u32[]{:S(2)}, u32[]{:S(2)}) collective-permute-start(bf16[128,2048]{1,0:T(8,128)(2,1)S(1)} %shard_map.107), channel_id=1, source_target_pairs={{0,1},{1,0},{2,3},{3,2},{4,5},{5,4},{6,7},{7,6},{8,9},{9,8},{10,11... | collective-permute-start | bytes 1572872 | tf_op jit(solution)/shard_map/ppermute | solution.py:283
  11.9 4.5 %collective-permute-start.8 = (bf16[256,128]{1,0:T(8,128)(2,1)S(1)}, bf16[256,128]{1,0:T(8,128)(2,1)S(1)}, u32[]{:S(2)}, u32[]{:S(2)}) collective-permute-start(bf16[256,128]{1,0:T(8,128)(2,1)S(1)} %get-tuple-element.34), channel_id=1, source_target_pairs={{0,8},{4,12},{8,0},{12,4},{16,24},{20,28},{24,16},{28,20},{1,9},{5... | collective-permute-start | bytes 196616 | tf_op jit(solution)/shard_map/ppermute | solution.py:283
  12.7 7.1 %collective-permute-start.9 = (bf16[256,128]{1,0:T(8,128)(2,1)S(1)}, bf16[256,128]{1,0:T(8,128)(2,1)S(1)}, u32[]{:S(2)}, u32[]{:S(2)}) collective-permute-start(bf16[256,128]{1,0:T(8,128)(2,1)S(1)} %get-tuple-element.35), channel_id=1, source_target_pairs={{0,16},{4,20},{8,24},{12,28},{16,0},{20,4},{24,8},{28,12},{1,17},{... | collective-permute-start | bytes 196616 | tf_op jit(solution)/shard_map/ppermute | solution.py:283
  16.2 6.1 %collective-permute-start.10 = (bf16[256,128]{1,0:T(8,128)(2,1)S(1)}, bf16[256,128]{1,0:T(8,128)(2,1)S(1)}, u32[]{:S(2)}, u32[]{:S(2)}) collective-permute-start(bf16[256,128]{1,0:T(8,128)(2,1)S(1)} %get-tuple-element.36), channel_id=1, source_target_pairs={{0,24},{4,28},{8,16},{12,20},{16,8},{20,12},{24,0},{28,4},{1,25},{... | collective-permute-start | bytes 196616 | tf_op jit(solution)/shard_map/ppermute | solution.py:283
  16.4 6.0 %collective-permute-start.3 = (bf16[4,256,128]{2,1,0:T(8,128)(2,1)S(1)}, bf16[4,256,128]{2,1,0:T(8,128)(2,1)S(1)}, u32[]{:S(2)}, u32[]{:S(2)}) collective-permute-start(bf16[4,256,128]{2,1,0:T(8,128)(2,1)S(1)} %pad_maximum_fusion), channel_id=1, source_target_pairs={{0,4},{4,0},{8,12},{12,8},{16,20},{20,16},{24,28},{28,24},{1,5},{5... | collective-permute-start | bytes 786440 | tf_op jit(solution)/shard_map/ppermute | solution.py:283
  22.3 29.1 %copy-start.4 = (bf16[1,256,2048]{2,1,0:T(8,128)(2,1)S(1)}, bf16[1,256,2048]{2,1,0:T(8,128)(2,1)}, u32[]{:S(2)}) copy-start(bf16[1,256,2048]{2,1,0:T(8,128)(2,1)} %param.11) | copy-start | bytes 3145732
  22.3 29.1 %copy-start.7 = (bf16[128,256]{1,0:T(8,128)(2,1)S(1)}, bf16[128,256]{1,0:T(8,128)(2,1)}, u32[]{:S(2)}) copy-start(bf16[128,256]{1,0:T(8,128)(2,1)} %constant.18.clone.refs_6_) | copy-start | bytes 196612
  22.3 29.1 %copy-start.8 = (bf16[128,256]{1,0:T(8,128)(2,1)S(1)}, bf16[128,256]{1,0:T(8,128)(2,1)}, u32[]{:S(2)}) copy-start(bf16[128,256]{1,0:T(8,128)(2,1)} %constant.17.clone.refs_5_) | copy-start | bytes 196612
  22.3 3.3 %collective-permute-start.11 = (bf16[4,256,128]{2,1,0:T(8,128)(2,1)S(1)}, bf16[4,256,128]{2,1,0:T(8,128)(2,1)S(1)}, u32[]{:S(2)}, u32[]{:S(2)}) collective-permute-start(bf16[4,256,128]{2,1,0:T(8,128)(2,1)S(1)} %pad_maximum_fusion.1), channel_id=1, source_target_pairs={{0,4},{4,0},{8,12},{12,8},{16,20},{20,16},{24,28},{28,24},{1,5},{5... | collective-permute-start | bytes 786440 | tf_op jit(solution)/shard_map/ppermute | solution.py:283
  24.2 5.7 %collective-permute-start.4 = (bf16[2,128,128]{2,1,0:T(8,128)(2,1)S(1)}, bf16[2,128,128]{2,1,0:T(8,128)(2,1)S(1)}, u32[]{:S(2)}, u32[]{:S(2)}) collective-permute-start(bf16[2,128,128]{2,1,0:T(8,128)(2,1)S(1)} %get-tuple-element.30), channel_id=1, source_target_pairs={{0,8},{4,12},{8,0},{12,4},{16,24},{20,28},{24,16},{28,20},{1,9},{5... | collective-permute-start | bytes 196616 | tf_op jit(solution)/shard_map/ppermute | solution.py:283
  24.3 28.4 %copy-start.1 = (bf16[256,2048]{1,0:T(8,128)(2,1)S(1)}, bf16[256,2048]{1,0:T(8,128)(2,1)}, u32[]{:S(2)}) copy-start(bf16[256,2048]{1,0:T(8,128)(2,1)} %refs_9_.1) | copy-start | bytes 3145732
  24.3 28.3 %copy-start.5 = (bf16[128,256]{1,0:T(8,128)(2,1)S(1)}, bf16[128,256]{1,0:T(8,128)(2,1)}, u32[]{:S(2)}) copy-start(bf16[128,256]{1,0:T(8,128)(2,1)} %constant.20.clone.refs_6_) | copy-start | bytes 196612
  24.3 28.3 %copy-start.6 = (bf16[128,256]{1,0:T(8,128)(2,1)S(1)}, bf16[128,256]{1,0:T(8,128)(2,1)}, u32[]{:S(2)}) copy-start(bf16[128,256]{1,0:T(8,128)(2,1)} %constant.19.clone.refs_5_) | copy-start | bytes 196612
  24.3 6.9 %collective-permute-start.5 = (bf16[2,128,128]{2,1,0:T(8,128)(2,1)S(1)}, bf16[2,128,128]{2,1,0:T(8,128)(2,1)S(1)}, u32[]{:S(2)}, u32[]{:S(2)}) collective-permute-start(bf16[2,128,128]{2,1,0:T(8,128)(2,1)S(1)} %get-tuple-element.31), channel_id=1, source_target_pairs={{0,16},{4,20},{8,24},{12,28},{16,0},{20,4},{24,8},{28,12},{1,17},{... | collective-permute-start | bytes 196616 | tf_op jit(solution)/shard_map/ppermute | solution.py:283
  27.4 4.5 %collective-permute-start.12 = (bf16[2,128,128]{2,1,0:T(8,128)(2,1)S(1)}, bf16[2,128,128]{2,1,0:T(8,128)(2,1)S(1)}, u32[]{:S(2)}, u32[]{:S(2)}) collective-permute-start(bf16[2,128,128]{2,1,0:T(8,128)(2,1)S(1)} %get-tuple-element.38), channel_id=1, source_target_pairs={{0,8},{4,12},{8,0},{12,4},{16,24},{20,28},{24,16},{28,20},{1,9},{5... | collective-permute-start | bytes 196616 | tf_op jit(solution)/shard_map/ppermute | solution.py:283
  28.3 21.6 %collective-permute-start.18 = (bf16[64,2048]{1,0:T(8,128)(2,1)S(1)}, bf16[64,2048]{1,0:T(8,128)(2,1)S(1)}, u32[]{:S(2)}, u32[]{:S(2)}) collective-permute-start(bf16[64,2048]{1,0:T(8,128)(2,1)S(1)} %get-tuple-element.43), channel_id=1, source_target_pairs={{0,1},{1,0},{2,3},{3,2},{4,5},{5,4},{6,7},{7,6},{8,9},{9,8},{10,11... | collective-permute-start | bytes 786440 | tf_op jit(solution)/shard_map/ppermute | solution.py:283
  28.9 23.7 %collective-permute-start.21 = (bf16[128,2048]{1,0:T(8,128)(2,1)S(1)}, bf16[128,2048]{1,0:T(8,128)(2,1)S(1)}, u32[]{:S(2)}, u32[]{:S(2)}) collective-permute-start(bf16[128,2048]{1,0:T(8,128)(2,1)S(1)} %collective-permute-done.17.second.refs_11_), channel_id=1, source_target_pairs={{0,4},{4,0},{8,12},{12,8},{16,20},{20,16},{24,28},{28,24},{1,5},{5... | collective-permute-start | bytes 1572872 | tf_op jit(solution)/shard_map/ppermute | solution.py:283
  29.9 20.6 %collective-permute-start.19 = (bf16[64,2048]{1,0:T(8,128)(2,1)S(1)}, bf16[64,2048]{1,0:T(8,128)(2,1)S(1)}, u32[]{:S(2)}, u32[]{:S(2)}) collective-permute-start(bf16[64,2048]{1,0:T(8,128)(2,1)S(1)} %get-tuple-element.44), channel_id=1, source_target_pairs={{0,2},{1,3},{2,0},{3,1},{4,6},{5,7},{6,4},{7,5},{8,10},{9,11},{10,... | collective-permute-start | bytes 786440 | tf_op jit(solution)/shard_map/ppermute | solution.py:283
  31.2 21.4 %collective-permute-start.20 = (bf16[128,2048]{1,0:T(8,128)(2,1)S(1)}, bf16[128,2048]{1,0:T(8,128)(2,1)S(1)}, u32[]{:S(2)}, u32[]{:S(2)}) collective-permute-start(bf16[128,2048]{1,0:T(8,128)(2,1)S(1)} %collective-permute-done.16.first.refs_10_), channel_id=1, source_target_pairs={{0,4},{4,0},{8,12},{12,8},{16,20},{20,16},{24,28},{28,24},{1,5},{5... | collective-permute-start | bytes 1572872 | tf_op jit(solution)/shard_map/ppermute | solution.py:283
  31.9 5.9 %collective-permute-start.13 = (bf16[2,128,128]{2,1,0:T(8,128)(2,1)S(1)}, bf16[2,128,128]{2,1,0:T(8,128)(2,1)S(1)}, u32[]{:S(2)}, u32[]{:S(2)}) collective-permute-start(bf16[2,128,128]{2,1,0:T(8,128)(2,1)S(1)} %get-tuple-element.39), channel_id=1, source_target_pairs={{0,16},{4,20},{8,24},{12,28},{16,0},{20,4},{24,8},{28,12},{1,17},{... | collective-permute-start | bytes 196616 | tf_op jit(solution)/shard_map/ppermute | solution.py:283
  37.8 6.1 %collective-permute-start.14 = (bf16[2,128,128]{2,1,0:T(8,128)(2,1)S(1)}, bf16[2,128,128]{2,1,0:T(8,128)(2,1)S(1)}, u32[]{:S(2)}, u32[]{:S(2)}) collective-permute-start(bf16[2,128,128]{2,1,0:T(8,128)(2,1)S(1)} %get-tuple-element.40), channel_id=1, source_target_pairs={{0,24},{4,28},{8,16},{12,20},{16,8},{20,12},{24,0},{28,4},{1,25},{... | collective-permute-start | bytes 196616 | tf_op jit(solution)/shard_map/ppermute | solution.py:283
  43.8 6.1 %collective-permute-start.6 = (bf16[2,128,128]{2,1,0:T(8,128)(2,1)S(1)}, bf16[2,128,128]{2,1,0:T(8,128)(2,1)S(1)}, u32[]{:S(2)}, u32[]{:S(2)}) collective-permute-start(bf16[2,128,128]{2,1,0:T(8,128)(2,1)S(1)} %get-tuple-element.32), channel_id=1, source_target_pairs={{0,24},{4,28},{8,16},{12,20},{16,8},{20,12},{24,0},{28,4},{1,25},{... | collective-permute-start | bytes 196616 | tf_op jit(solution)/shard_map/ppermute | solution.py:283
  49.9 1.3 %collective-permute-start.15 = (bf16[4,128,128]{2,1,0:T(8,128)(2,1)S(1)}, bf16[4,128,128]{2,1,0:T(8,128)(2,1)S(1)}, u32[]{:S(2)}, u32[]{:S(2)}) collective-permute-start(bf16[4,128,128]{2,1,0:T(8,128)(2,1)S(1)} %shard_map.105), channel_id=1, source_target_pairs={{0,4},{4,0},{8,12},{12,8},{16,20},{20,16},{24,28},{28,24},{1,5},{5... | collective-permute-start | bytes 393224 | tf_op jit(solution)/shard_map/ppermute | solution.py:283
  49.9 2.7 %collective-permute-start.22 = (bf16[64,2048]{1,0:T(8,128)(2,1)S(1)}, bf16[64,2048]{1,0:T(8,128)(2,1)S(1)}, u32[]{:S(2)}, u32[]{:S(2)}) collective-permute-start(bf16[64,2048]{1,0:T(8,128)(2,1)S(1)} %collective-permute-done.18.refs_12_), channel_id=1, source_target_pairs={{0,4},{4,0},{8,12},{12,8},{16,20},{20,16},{24,28},{28,24},{1,5},{5... | collective-permute-start | bytes 786440 | tf_op jit(solution)/shard_map/ppermute | solution.py:283
  50.4 2.2 %collective-permute-start.23 = (bf16[64,2048]{1,0:T(8,128)(2,1)S(1)}, bf16[64,2048]{1,0:T(8,128)(2,1)S(1)}, u32[]{:S(2)}, u32[]{:S(2)}) collective-permute-start(bf16[64,2048]{1,0:T(8,128)(2,1)S(1)} %collective-permute-done.19.refs_13_), channel_id=1, source_target_pairs={{0,4},{4,0},{8,12},{12,8},{16,20},{20,16},{24,28},{28,24},{1,5},{5... | collective-permute-start | bytes 786440 | tf_op jit(solution)/shard_map/ppermute | solution.py:283
  51.3 1.3 %collective-permute-start.7 = (bf16[4,128,128]{2,1,0:T(8,128)(2,1)S(1)}, bf16[4,128,128]{2,1,0:T(8,128)(2,1)S(1)}, u32[]{:S(2)}, u32[]{:S(2)}) collective-permute-start(bf16[4,128,128]{2,1,0:T(8,128)(2,1)S(1)} %shard_map.102), channel_id=1, source_target_pairs={{0,4},{4,0},{8,12},{12,8},{16,20},{20,16},{24,28},{28,24},{1,5},{5... | collective-permute-start | bytes 393224 | tf_op jit(solution)/shard_map/ppermute | solution.py:283
  (4 other events, 27.0 us)

commit v2 on v1

--- a/solution.py
+++ b/solution.py
@@ -60,25 +60,52 @@
     )
 
 
-def pick_kernel(chips, q, x_ref, *outs):
-    chip = lax.axis_index("row") // 2
-    lanes = outs[0].shape[1]
+def pick_kernel(chips, fast, *refs):
+    x_ref, w_ref = refs[:2]
+    outs = refs[2 : 2 + chips]
+    halves = refs[2 + chips : -3]
+    tokens, x_sems, w_sems = refs[-3:]
+    row = lax.axis_index("row")
+    core, chip = row % 2, row // 2
+    lanes = outs[0].shape[2]
     pairs = lanes // 2
     chips_per_group = GROUP // (CHUNKS * lanes)
-    src = lax.broadcasted_iota(jnp.int32, (GROUP, lanes), 0)
-    lane = lax.broadcasted_iota(jnp.int32, (GROUP, lanes), 1)
+    loads = []
     for zs in range(chips):
-        dest = chip ^ zs
-        group = dest // chips_per_group
-        part = (dest % chips_per_group) * CHUNKS + q
-        j = lane - pairs
+        group = (chip ^ zs) // chips_per_group
+        columns = pl.ds(pl.multiple_of(group * GROUP, GROUP), GROUP)
+        loads.append(pltpu.make_async_copy(x_ref.at[:, columns], tokens.at[zs], x_sems.at[zs]))
+    order = [*send_order(chips), 0]
+    for zs in order:
+        loads[zs].start()
+    fetches = []
+    if fast:
+        half = GROUP // 2
+        for i, h in enumerate((core, 1 - core)):
+            part = w_ref.at[pl.ds(pl.multiple_of(h * half, half), half), :]
+            fetches.append(pltpu.make_async_copy(part, halves[i], w_sems.at[i]))
+            fetches[-1].start()
+    src = lax.broadcasted_iota(jnp.int32, (GROUP, CHUNKS * lanes), 0)
+    column = lax.broadcasted_iota(jnp.int32, (GROUP, CHUNKS * lanes), 1)
+    lane, j = column % lanes, column % lanes - pairs
+    for zs in order:
+        part = ((chip ^ zs) % chips_per_group) * CHUNKS + column // lanes
         mirrored = jnp.where((j == 0) & (part == 0), GROUP // 2, GROUP - pairs * part - j)
         wanted = jnp.where(lane < pairs, pairs * part + lane, mirrored)
         choose = (src == wanted).astype(jnp.bfloat16)
-        block = x_ref[:, pl.ds(pl.multiple_of(group * GROUP, GROUP), GROUP)]
-        outs[zs][...] = jnp.dot(block, choose, preferred_element_type=jnp.float32).astype(
-            jnp.bfloat16
-        )
+        loads[zs].wait()
+        got = jnp.dot(tokens[zs], choose, preferred_element_type=jnp.float32).astype(jnp.bfloat16)
+        for q in range(CHUNKS):
+            outs[zs][q] = got[:, q * lanes : (q + 1) * lanes]
+    for fetch in fetches:
+        fetch.wait()
+
+
+def stack_kernel(*refs):
+    pieces, outs = refs[:-CHUNKS], refs[-CHUNKS:]
+    for q, out in enumerate(outs):
+        for zs, piece in enumerate(pieces):
+            out[zs] = piece[q]
 
 
 def complex_dft(values):
@@ -106,9 +133,8 @@
     chips = rows // 2
     mine, theirs = refs[:chips], refs[chips]
     table_hi, table_lo, twist = refs[chips + 1 : chips + 4]
-    outs = refs[chips + 4 : 2 * chips + 4]
-    folded, z_hi, z_lo, spect = refs[2 * chips + 4 :]
-    inner, lanes = mine[0].shape
+    *outs, folded, z_hi, z_lo, spect = refs[chips + 4 :]
+    inner, lanes = mine[0].shape[1:]
     pairs = lanes // 2
     row = lax.axis_index("row")
     core, chip = row % 2, row // 2
@@ -132,7 +158,7 @@
         return value * own + turned * other
 
     for zs in range(chips):
-        folded[row ^ (2 * zs)] = fold(mine[zs][...])
+        folded[row ^ (2 * zs)] = fold(mine[zs][q])
         folded[row ^ (2 * zs + 1)] = fold(theirs[zs])
 
     odd_core = core == 1
@@ -183,9 +209,12 @@
         for rel in range(2):
             dest = row ^ (2 * zs + rel)
             for j in range(half):
-                outs[zs][rel, j * per : (j + 1) * per, :] = spect[
-                    j, pl.ds(pl.multiple_of(dest * per, per), per), :
-                ].astype(jnp.bfloat16)
+                piece = spect[j, pl.ds(pl.multiple_of(dest * per, per), per), :]
+                lines = slice(j * per, (j + 1) * per)
+                if q == 0:
+                    outs[zs][rel, lines, :] = piece.astype(jnp.bfloat16)
+                else:
+                    outs[rel][zs, lines, :] = piece.astype(jnp.bfloat16)
 
 
 def order_rows(rows, count):
@@ -203,14 +232,18 @@
         out[zs] = ref[1]
 
 
-def channel_part(order, mine, theirs, feat_hi, feat_lo):
+def join_kernel(keep, got, *outs):
+    for zs, out in enumerate(outs):
+        out[0] = keep[zs]
+        out[1] = got[zs]
+
+
+def channel_part(order, pieces, feat_hi, feat_lo):
     lanes = feat_hi.shape[0]
-    got = jnp.concatenate(
-        [jnp.concatenate([m[0], theirs[zs]], axis=0) for zs, m in enumerate(mine)], axis=1
-    )
+    got = jnp.concatenate([jnp.concatenate(piece, axis=0) for piece in pieces], axis=1)
     got = jnp.dot(order, got, preferred_element_type=jnp.float32).astype(jnp.bfloat16)
     parts = []
-    for zs in range(len(mine)):
+    for zs in range(len(pieces)):
         piece = got[:, zs * lanes : (zs + 1) * lanes]
         part = jnp.dot(piece, feat_hi, preferred_element_type=jnp.float32)
         parts.append(part + jnp.dot(piece, feat_lo, preferred_element_type=jnp.float32))
@@ -222,19 +255,14 @@
     mine, theirs, feat_hi, feat_lo, gate_ref = refs[:chips], *refs[chips : chips + 4]
     spect, opened = refs[chips + 4 :]
     order = order_rows(rows, gate_ref.shape[0])
-    for zs, part in enumerate(channel_part(order, mine, theirs, feat_hi[...], feat_lo[...])):
+    pieces = [(ref[0], theirs[zs]) for zs, ref in enumerate(mine)]
+    for zs, part in enumerate(channel_part(order, pieces, feat_hi[...], feat_lo[...])):
         spect[zs] = part
     for start in range(0, gate_ref.shape[1], GROUP):
         cols = slice(start, start + GROUP)
         opened[:, cols] = jax.nn.sigmoid(gate_ref[:, cols].astype(jnp.float32))
 
 
-def cut_kernel(w_ref, out_ref):
-    half = GROUP // 2
-    core = lax.axis_index("row") % 2
-    out_ref[...] = w_ref[pl.ds(pl.multiple_of(core * half, half), half), :]
-
-
 def relay_kernel(first, second, to_first, to_second):
     rows = to_first.shape[0]
     to_first[...] = second[:rows, :]
@@ -243,14 +271,15 @@
 
 def final_kernel(rows, *refs):
     chips = rows // 2
-    mine, theirs, feat_hi, feat_lo, spect, opened = refs[:chips], *refs[chips : chips + 5]
-    w_here, *w_far, out_ref, lhs, result, sems = refs[chips + 5 :]
+    mine, feat_hi, feat_lo, spect, opened = refs[:chips], *refs[chips : chips + 4]
+    w_mine, w_rest, *w_far, out_ref, lhs, result, sems = refs[chips + 4 :]
     count, width = opened.shape
     half = GROUP // 2
     row, col = lax.axis_index("row"), lax.axis_index("col")
     core, chip = row % 2, row // 2
     order = order_rows(rows, count)
-    for zs, part in enumerate(channel_part(order, mine, theirs, feat_hi[...], feat_lo[...])):
+    pieces = [(ref[0], ref[1]) for ref in mine]
+    for zs, part in enumerate(channel_part(order, pieces, feat_hi[...], feat_lo[...])):
         whole = (part + spect[zs]).astype(jnp.bfloat16)
         for h in range(2):
             spot = pl.ds(pl.multiple_of((core ^ h) * half, half), half)
@@ -262,10 +291,7 @@
         total = jnp.zeros((count, GROUP), jnp.float32)
         for s in range(4):
             if s == 0:
-                parts = [
-                    w_here[pl.ds(pl.multiple_of(h * half, half), half), cols]
-                    for h in (core, 1 - core)
-                ]
+                parts = [w_mine[:, cols], w_rest[:, cols]]
             elif s < 3:
                 parts = [ref[:, cols] for ref in (first, second)[s - 1]]
             else:
@@ -314,60 +340,73 @@
     bf = jnp.bfloat16
     fast = w_proj.shape[0] == GROUP and CHUNKS * lanes == GROUP and n_col == chips == 4
 
-    arrived = []
-    for q in range(CHUNKS):
-        picked = vmem_call(
-            functools.partial(pick_kernel, chips, q),
-            [jax.ShapeDtypeStruct((count, lanes), bf)] * chips,
-            [],
-            2 * count * GROUP * lanes * chips,
-            3 * count * lanes * chips * 2,
-        )(tokens)
-        arrived.append(across_chips(picked, rows))
+    half_w = jax.ShapeDtypeStruct((GROUP // 2, width), bf)
+    picked = pl.pallas_call(
+        functools.partial(pick_kernel, chips, fast),
+        out_shape=[jax.ShapeDtypeStruct((CHUNKS, count, lanes), bf)] * chips
+        + [half_w] * (2 * fast),
+        in_specs=[pl.BlockSpec(memory_space=pl.ANY)] * 2,
+        out_specs=[pl.BlockSpec(memory_space=pltpu.VMEM)] * (chips + 2 * fast),
+        scratch_shapes=[
+            pltpu.VMEM((chips, count, GROUP), bf),
+            pltpu.SemaphoreType.DMA((chips,)),
+            pltpu.SemaphoreType.DMA((2,)),
+        ],
+        compiler_params=pltpu.CompilerParams(vmem_limit_bytes=24 * MIB),
+        cost_estimate=pl.CostEstimate(
+            flops=2 * count * GROUP * features, bytes_accessed=MIB, transcendentals=0
+        ),
+    )(tokens, w_proj)
+    arrived = across_chips(picked[:chips], rows)
 
     if fast:
+        mine, rest = picked[chips:]
         w_own = []
-        piece = jax.ShapeDtypeStruct((GROUP // 2, width), bf)
         part = jax.ShapeDtypeStruct((GROUP // 4, width), bf)
-        mine = vmem_call(cut_kernel, piece, [], GROUP * width, 2 * GROUP * width)(w_proj)
         for s in (1, 2):
             w_own.append(swap(mine, "col", n_col, s))
         passed = vmem_call(relay_kernel, [part] * 2, [], GROUP * width, 2 * GROUP * width)(*w_own)
         for s in (1, 2):
             w_own.append(swap(passed[s - 1], "col", n_col, s))
-
-    spectra = []
-    for q in range(CHUNKS):
-        theirs = swap(jnp.stack(arrived[q]), "row", rows, 1)
-        sent = vmem_call(
-            functools.partial(position_kernel, rows, q),
-            [jax.ShapeDtypeStruct((2, half * (count // rows), lanes), bf)] * chips,
-            [
-                pltpu.VMEM((rows, count, lanes), jnp.float32),
-                pltpu.VMEM((2 * count, half * lanes), bf),
-                pltpu.VMEM((2 * count, half * lanes), bf),
-                pltpu.VMEM((half, count, lanes), jnp.float32),
-            ],
-            12 * count * count * half * lanes,
-            rows * count * lanes * 4,
-        )(*arrived[q], theirs, table_hi, table_lo, twist)
-        spectra.append(across_chips(sent, rows))
-
-    if fast:
         w_other = []
         for own in w_own:
             w_other.append(swap(own, "row", rows, 1))
-    operands = []
+
+    stacks = vmem_call(
+        stack_kernel,
+        [jax.ShapeDtypeStruct((chips, count, lanes), bf)] * CHUNKS,
+        [],
+        count * features,
+        4 * count * features,
+    )(*arrived)
+    lines = half * (count // rows)
+    piece = jax.ShapeDtypeStruct((2, lines, lanes), bf)
+    stacked = jax.ShapeDtypeStruct((chips, lines, lanes), bf)
+    small = (count * features // 4, count * features)
+    sent = []
     for q in range(CHUNKS):
-        give = vmem_call(
-            give_kernel,
-            jax.ShapeDtypeStruct((chips, half * (count // rows), lanes), bf),
-            [],
-            count * lanes * chips,
-            2 * count * lanes * chips,
-        )(*spectra[q])
-        theirs = swap(give, "row", rows, 1)
-        operands.append([*spectra[q], theirs])
+        theirs = swap(stacks[q], "row", rows, 1)
+        sent.append(
+            vmem_call(
+                functools.partial(position_kernel, rows, q),
+                [piece] * chips if q == 0 else [stacked] * 2,
+                [
+                    pltpu.VMEM((rows, count, lanes), jnp.float32),
+                    pltpu.VMEM((2 * count, half * lanes), bf),
+                    pltpu.VMEM((2 * count, half * lanes), bf),
+                    pltpu.VMEM((half, count, lanes), jnp.float32),
+                ],
+                12 * count * count * half * lanes,
+                rows * count * lanes * 4,
+            )(*arrived, theirs, table_hi, table_lo, twist)
+        )
+    early = across_chips(sent[0], rows)
+    give = vmem_call(give_kernel, stacked, [], *small)(*early)
+    early.append(swap(give, "row", rows, 1))
+    keep, give = sent[1]
+    got = swap(give, "row", rows, 1)
+    joined = vmem_call(join_kernel, [piece] * chips, [], *small)(keep, got)
+    late = across_chips(joined, rows)
     if fast:
         spect, opened = vmem_call(
             functools.partial(prepare_kernel, rows),
@@ -378,7 +417,7 @@
             [],
             2 * count * features * GROUP,
             6 * count * width,
-        )(*operands[0], feat_hi[0], feat_lo[0], gate)
+        )(*early, feat_hi[0], feat_lo[0], gate)
         return pl.pallas_call(
             functools.partial(final_kernel, rows),
             out_shape=jax.ShapeDtypeStruct((count, width), bf),
@@ -395,7 +434,7 @@
                 bytes_accessed=2 * features * width,
                 transcendentals=0,
             ),
-        )(*operands[1], feat_hi[1], feat_lo[1], spect, opened, w_proj, *w_own, *w_other)
+        )(*late, feat_hi[1], feat_lo[1], spect, opened, mine, rest, *w_own, *w_other)
 
     weights = lax.all_gather(w_proj, "col", axis=0, tiled=True).reshape(-1, GROUP, width)
     order = order_rows(rows, count)
@@ -405,12 +444,11 @@
     spectrum = jnp.zeros((count, weights.shape[0], GROUP), jnp.float32)
     here = chip ^ jnp.arange(chips)
     for q in range(CHUNKS):
-        got = jnp.stack(
-            [
-                jnp.concatenate([operands[q][zs][0], operands[q][chips][zs]], axis=0)
-                for zs in range(chips)
-            ]
-        )[here]
+        if q == 0:
+            parts = [(early[zs][0], early[chips][zs]) for zs in range(chips)]
+        else:
+            parts = [(ref[0], ref[1]) for ref in late]
+        got = jnp.stack([jnp.concatenate(pair, axis=0) for pair in parts])[here]
         got = jnp.einsum("kr,zrl->kzl", order, got, preferred_element_type=jnp.float32)
         spectrum += jnp.einsum(
             "kgtl,tlm->kgm",

time: 55.5 us -> 59.8 us (1.077)
  waiting for transfers between devices: 21 us -> 28.9 us
  starting transfers between devices: 24 us -> 20 us
    ppermute x24 -> x21, waiting for transfers between devices: 21 us -> 28.9 us  [swap(): return lax.ppermute(value, axis, [(i, i ^ bit) for i in range(size)])]
    ppermute x24 -> x21, starting transfers between devices: 24 us -> 20 us  [swap(): return lax.ppermute(value, axis, [(i, i ^ bit) for i in range(size)])]
    pallas_call x7 -> x6, Pallas kernels: 4.18 us -> 4.71 us  [the longest x2 3.55 us: program(): vmem_call(functools.partial(position_kernel, rows, q), [piece] * chips if...]
    unnamed x24 -> x20, local copies, waits for them, and re-layouts: 2.32 us -> 2.3 us
  transfers between devices with their start and end apart: 24 -> 21, of which waited for: 10 -> 9; matrix products, arithmetic and copies ran while one was open for 0% -> 0% of each run, Pallas kernels for 9% -> 7%
where the time goes in v2:
time: 59.8 us; the launch traced here: 59.6 us
  waiting for transfers between devices  28.9 us (48%)
  starting transfers between devices  20 us (33%)
  Pallas kernels  8.17 us (14%)
  local copies, waits for them, and re-layouts  2.3 us (4%)
    ppermute x21, waiting for transfers between devices, swap(): return lax.ppermute(value, axis, [(i, i ^ bit) for i in range(size)])  28.9 us
    ppermute x21, starting transfers between devices, swap(): return lax.ppermute(value, axis, [(i, i ^ bit) for i in range(size)])  20 us
    pallas_call x2, Pallas kernels, program(): vmem_call(functools.partial(position_kernel, rows, q), [piece] * chips if...  3.55 us
    pallas_call x1, Pallas kernels, program(): pl.pallas_call(functools.partial(final_kernel, rows), out_shape=jax.Shape...  2.66 us
    unnamed x20, local copies, waits for them, and re-layouts  2.3 us
  transfers between devices with their start and end apart: 21, of which 9 were waited for; matrix products, arithmetic and copies ran while one was open for 0% of the time, Pallas kernels for 7%

profile of v2, /device:TPU:0, one launch (start us, length us, event | category | flops | bytes accessed | tf_op | source)
XLA Modules:
  0.0 59.6 jit_solution(12885825620563226496)
XLA Ops:
  0.0 1.2 %copy-done = bf16[256,2048]{1,0:T(8,128)(2,1)S(1)} copy-done((bf16[256,2048]{1,0:T(8,128)(2,1)S(1)}, bf16[256,2048]{1,0:T(8,128)(2,1)}, u32[]{:S(2)}) %copy-start) | copy-done | bytes 1048600
  1.2 1.0 %copy-done.5 = bf16[1,256,1024]{2,1,0:T(8,128)(2,1)S(1)} copy-done((bf16[1,256,1024]{2,1,0:T(8,128)(2,1)S(1)}, bf16[1,256,1024]{2,1,0:T(8,128)(2,1)}, u32[]{:S(2)}) %copy-start.5) | copy-done | bytes 524312
  2.3 1.1 %shard_map.100 = (bf16[2,256,128]{2,1,0:T(8,128)(2,1)S(1)}, bf16[2,256,128]{2,1,0:T(8,128)(2,1)S(1)}, bf16[2,256,128]{2,1,0:T(8,128)(2,1)S(1)}, bf16[2,256,128]{...) custom-call(bf16[256,1024]{1,0:T(8,128)(2,1)S(1)} %bitcast.4, ...), custom_call_target="tpu_custom_call" | custom-call | flops 134217728 | bytes 1048576 | tf_op jit(solution)/shard_map/pallas_call | solution.py:344
  3.4 3.1 %collective-permute-start.14 = (bf16[128,2048]{1,0:T(8,128)(2,1)S(1)}, bf16[128,2048]{1,0:T(8,128)(2,1)S(1)}, u32[]{:S(2)}, u32[]{:S(2)}) collective-permute-start(bf16[128,2048]{1,0:T(8,128)(2,1)S(1)} %get-tuple-element.45.refs_8_), channel_id=1, source_target_pairs={{0,2},{1,3},{2,0},{3,1},{4,6},{5,7},{6,4},{7,5},{8,10},{9,11},{10,... | collective-permute-start | bytes 1572872 | tf_op jit(solution)/shard_map/ppermute | solution.py:309
  6.4 1.5 %collective-permute-start.13 = (bf16[128,2048]{1,0:T(8,128)(2,1)S(1)}, bf16[128,2048]{1,0:T(8,128)(2,1)S(1)}, u32[]{:S(2)}, u32[]{:S(2)}) collective-permute-start(bf16[128,2048]{1,0:T(8,128)(2,1)S(1)} %get-tuple-element.45.refs_8_), channel_id=1, source_target_pairs={{0,1},{1,0},{2,3},{3,2},{4,5},{5,4},{6,7},{7,6},{8,9},{9,8},{10,11... | collective-permute-start | bytes 1572872 | tf_op jit(solution)/shard_map/ppermute | solution.py:309
  7.9 1.6 %collective-permute-start = (bf16[2,256,128]{2,1,0:T(8,128)(2,1)S(1)}, bf16[2,256,128]{2,1,0:T(8,128)(2,1)S(1)}, u32[]{:S(2)}, u32[]{:S(2)}) collective-permute-start(bf16[2,256,128]{2,1,0:T(8,128)(2,1)S(1)} %get-tuple-element.28), channel_id=1, source_target_pairs={{0,8},{4,12},{8,0},{12,4},{16,24},{20,28},{24,16},{28,20},{1,9},{5... | collective-permute-start | bytes 393224 | tf_op jit(solution)/shard_map/ppermute | solution.py:309
  9.5 2.6 %collective-permute-start.1 = (bf16[2,256,128]{2,1,0:T(8,128)(2,1)S(1)}, bf16[2,256,128]{2,1,0:T(8,128)(2,1)S(1)}, u32[]{:S(2)}, u32[]{:S(2)}) collective-permute-start(bf16[2,256,128]{2,1,0:T(8,128)(2,1)S(1)} %get-tuple-element.29), channel_id=1, source_target_pairs={{0,16},{4,20},{8,24},{12,28},{16,0},{20,4},{24,8},{28,12},{1,17},{... | collective-permute-start | bytes 393224 | tf_op jit(solution)/shard_map/ppermute | solution.py:309
  12.1 0.2 collective-permute-start.2
  12.3 2.1 %collective-permute-done.refs_1_ = bf16[2,256,128]{2,1,0:T(8,128)(2,1)S(1)} collective-permute-done((bf16[2,256,128]{2,1,0:T(8,128)(2,1)S(1)}, bf16[2,256,128]{2,1,0:T(8,128)(2,1)S(1)}, u32[]{:S(2)}, u32[]{:S(2)}) %collective-permute-start) | collective-permute-done | bytes 131104 | tf_op jit(solution)/shard_map/ppermute | solution.py:309
  14.4 7.5 %collective-permute-done.1.refs_2_ = bf16[2,256,128]{2,1,0:T(8,128)(2,1)S(1)} collective-permute-done((bf16[2,256,128]{2,1,0:T(8,128)(2,1)S(1)}, bf16[2,256,128]{2,1,0:T(8,128)(2,1)S(1)}, u32[]{:S(2)}, u32[]{:S(2)}) %collective-permute-start.1) | collective-permute-done | bytes 131104 | tf_op jit(solution)/shard_map/ppermute | solution.py:309
  22.0 0.5 collective-permute-start.3
  22.5 1.0 %collective-permute-done.8.refs_4_ = bf16[4,256,128]{2,1,0:T(8,128)(2,1)S(1)} collective-permute-done((bf16[4,256,128]{2,1,0:T(8,128)(2,1)S(1)}, bf16[4,256,128]{2,1,0:T(8,128)(2,1)S(1)}, u32[]{:S(2)}, u32[]{:S(2)}) %collective-permute-start.8) | collective-permute-done | bytes 262176 | tf_op jit(solution)/shard_map/ppermute | solution.py:309
  23.5 1.8 %shard_map.104 = (bf16[2,128,128]{2,1,0:T(8,128)(2,1)S(1)}, bf16[2,128,128]{2,1,0:T(8,128)(2,1)S(1)}, bf16[2,128,128]{2,1,0:T(8,128)(2,1)S(1)}, bf16[2,128,128]{2,1,0:T(8,128)(2,1)S(1)}) custom-call(bf16[2,256,128]{2,1,0:T(8,128)(2,1)S(1)} %get-tuple-element.27.refs_0_, bf16[2,256,128]{2,1,0:T(8,128)(2,1)S(1)} %collective-permute-done.refs_1_, ...), custom_call_target="tpu_custom_call" | custom-call | flops 402653184 | bytes 1048576 | tf_op jit(solution)/shard_map/pallas_call | solution.py:390
  25.3 2.0 %collective-permute-start.9 = (bf16[2,128,128]{2,1,0:T(8,128)(2,1)S(1)}, bf16[2,128,128]{2,1,0:T(8,128)(2,1)S(1)}, u32[]{:S(2)}, u32[]{:S(2)}) collective-permute-start(bf16[2,128,128]{2,1,0:T(8,128)(2,1)S(1)} %get-tuple-element.40), channel_id=1, source_target_pairs={{0,8},{4,12},{8,0},{12,4},{16,24},{20,28},{24,16},{28,20},{1,9},{5... | collective-permute-start | bytes 196616 | tf_op jit(solution)/shard_map/ppermute | solution.py:309
  27.4 1.1 %collective-permute-start.10 = (bf16[2,128,128]{2,1,0:T(8,128)(2,1)S(1)}, bf16[2,128,128]{2,1,0:T(8,128)(2,1)S(1)}, u32[]{:S(2)}, u32[]{:S(2)}) collective-permute-start(bf16[2,128,128]{2,1,0:T(8,128)(2,1)S(1)} %get-tuple-element.41), channel_id=1, source_target_pairs={{0,16},{4,20},{8,24},{12,28},{16,0},{20,4},{24,8},{28,12},{1,17},{... | collective-permute-start | bytes 196616 | tf_op jit(solution)/shard_map/ppermute | solution.py:309
  28.5 1.8 %shard_map.102 = (bf16[4,128,128]{2,1,0:T(8,128)(2,1)S(1)}, bf16[4,128,128]{2,1,0:T(8,128)(2,1)S(1)}) custom-call(bf16[2,256,128]{2,1,0:T(8,128)(2,1)S(1)} %get-tuple-element.27.refs_0_, bf16[2,256,128]{2,1,0:T(8,128)(2,1)S(1)} %collective-permute-done.refs_1_, bf16[2,256,128]{2,1,0:T(8,128)(2,1)S(1)} %collective-permute-done.1.refs_2_, ...), custom_call_target="tpu_custom_call" | custom-call | flops 402653184 | bytes 1048576 | tf_op jit(solution)/shard_map/pallas_call | solution.py:390
  30.2 0.1 collective-permute-start.4
  30.4 0.6 %collective-permute-start.15 = (bf16[64,2048]{1,0:T(8,128)(2,1)S(1)}, bf16[64,2048]{1,0:T(8,128)(2,1)S(1)}, u32[]{:S(2)}, u32[]{:S(2)}) collective-permute-start(bf16[64,2048]{1,0:T(8,128)(2,1)S(1)} %get-tuple-element.47), channel_id=1, source_target_pairs={{0,1},{1,0},{2,3},{3,2},{4,5},{5,4},{6,7},{7,6},{8,9},{9,8},{10,11... | collective-permute-start | bytes 786440 | tf_op jit(solution)/shard_map/ppermute | solution.py:309
  31.0 0.2 collective-permute-start.18
  31.2 0.5 collective-permute-start.16
  31.7 1.9 %collective-permute-done.10.refs_2_ = bf16[2,128,128]{2,1,0:T(8,128)(2,1)S(1)} collective-permute-done((bf16[2,128,128]{2,1,0:T(8,128)(2,1)S(1)}, bf16[2,128,128]{2,1,0:T(8,128)(2,1)S(1)}, u32[]{:S(2)}, u32[]{:S(2)}) %collective-permute-start.10) | collective-permute-done | bytes 65568 | tf_op jit(solution)/shard_map/ppermute | solution.py:309
  33.6 2.3 %collective-permute-start.11 = (bf16[2,128,128]{2,1,0:T(8,128)(2,1)S(1)}, bf16[2,128,128]{2,1,0:T(8,128)(2,1)S(1)}, u32[]{:S(2)}, u32[]{:S(2)}) collective-permute-start(bf16[2,128,128]{2,1,0:T(8,128)(2,1)S(1)} %get-tuple-element.42), channel_id=1, source_target_pairs={{0,24},{4,28},{8,16},{12,20},{16,8},{20,12},{24,0},{28,4},{1,25},{... | collective-permute-start | bytes 196616 | tf_op jit(solution)/shard_map/ppermute | solution.py:309
  35.9 4.0 %collective-permute-done.11.refs_3_ = bf16[2,128,128]{2,1,0:T(8,128)(2,1)S(1)} collective-permute-done((bf16[2,128,128]{2,1,0:T(8,128)(2,1)S(1)}, bf16[2,128,128]{2,1,0:T(8,128)(2,1)S(1)}, u32[]{:S(2)}, u32[]{:S(2)}) %collective-permute-start.11) | collective-permute-done | bytes 65568 | tf_op jit(solution)/shard_map/ppermute | solution.py:309
  39.9 4.3 %collective-permute-done.5.refs_1_ = bf16[2,128,128]{2,1,0:T(8,128)(2,1)S(1)} collective-permute-done((bf16[2,128,128]{2,1,0:T(8,128)(2,1)S(1)}, bf16[2,128,128]{2,1,0:T(8,128)(2,1)S(1)}, u32[]{:S(2)}, u32[]{:S(2)}) %collective-permute-start.5) | collective-permute-done | bytes 65568 | tf_op jit(solution)/shard_map/ppermute | solution.py:309
  44.1 0.9 %collective-permute-start.6 = (bf16[2,128,128]{2,1,0:T(8,128)(2,1)S(1)}, bf16[2,128,128]{2,1,0:T(8,128)(2,1)S(1)}, u32[]{:S(2)}, u32[]{:S(2)}) collective-permute-start(bf16[2,128,128]{2,1,0:T(8,128)(2,1)S(1)} %get-tuple-element.36), channel_id=1, source_target_pairs={{0,16},{4,20},{8,24},{12,28},{16,0},{20,4},{24,8},{28,12},{1,17},{... | collective-permute-start | bytes 196616 | tf_op jit(solution)/shard_map/ppermute | solution.py:309
  45.0 0.5 collective-permute-start.20
  45.5 3.9 %collective-permute-done.6.refs_2_ = bf16[2,128,128]{2,1,0:T(8,128)(2,1)S(1)} collective-permute-done((bf16[2,128,128]{2,1,0:T(8,128)(2,1)S(1)}, bf16[2,128,128]{2,1,0:T(8,128)(2,1)S(1)}, u32[]{:S(2)}, u32[]{:S(2)}) %collective-permute-start.6) | collective-permute-done | bytes 65568 | tf_op jit(solution)/shard_map/ppermute | solution.py:309
  49.5 1.3 %collective-permute-done.12.refs_4_ = bf16[4,128,128]{2,1,0:T(8,128)(2,1)S(1)} collective-permute-done((bf16[4,128,128]{2,1,0:T(8,128)(2,1)S(1)}, bf16[4,128,128]{2,1,0:T(8,128)(2,1)S(1)}, u32[]{:S(2)}, u32[]{:S(2)}) %collective-permute-start.12) | collective-permute-done | bytes 131104 | tf_op jit(solution)/shard_map/ppermute | solution.py:309
  50.8 2.3 %collective-permute-start.7 = (bf16[2,128,128]{2,1,0:T(8,128)(2,1)S(1)}, bf16[2,128,128]{2,1,0:T(8,128)(2,1)S(1)}, u32[]{:S(2)}, u32[]{:S(2)}) collective-permute-start(bf16[2,128,128]{2,1,0:T(8,128)(2,1)S(1)} %get-tuple-element.37), channel_id=1, source_target_pairs={{0,24},{4,28},{8,16},{12,20},{16,8},{20,12},{24,0},{28,4},{1,25},{... | collective-permute-start | bytes 196616 | tf_op jit(solution)/shard_map/ppermute | solution.py:309
  53.1 0.8 %shard_map.106 = (f32[4,256,256]{2,1,0:T(8,128)S(1)}, f32[256,2048]{1,0:T(8,128)S(1)}) custom-call(bf16[2,128,128]{2,1,0:T(8,128)(2,1)S(1)} %get-tuple-element.39.refs_0_, bf16[2,128,128]{2,1,0:T(8,128)(2,1)S(1)} %collective-permute-done.9.refs_1_, bf16[2,128,128]{2,1,0:T(8,128)(2,1)S(1)} %collective-permute-done.10.refs_2_, ...), custom_call_target="tpu_custom_call" | custom-call | flops 134217728 | bytes 3145728 | tf_op jit(solution)/shard_map/pallas_call | solution.py:411
  53.9 3.0 %collective-permute-done.7.refs_3_ = bf16[2,128,128]{2,1,0:T(8,128)(2,1)S(1)} collective-permute-done((bf16[2,128,128]{2,1,0:T(8,128)(2,1)S(1)}, bf16[2,128,128]{2,1,0:T(8,128)(2,1)S(1)}, u32[]{:S(2)}, u32[]{:S(2)}) %collective-permute-start.7) | collective-permute-done | bytes 65568 | tf_op jit(solution)/shard_map/ppermute | solution.py:309
  56.9 2.7 %shard_map.108 = bf16[256,2048]{1,0:T(8,128)(2,1)} custom-call(bf16[2,128,128]{2,1,0:T(8,128)(2,1)S(1)} %get-tuple-element.34.refs_0_, bf16[2,128,128]{2,1,0:T(8,128)(2,1)S(1)} %collective-permute-done.5.refs_1_, bf16[2,128,128]{2,1,0:T(8,128)(2,1)S(1)} %collective-permute-done.6.refs_2_, bf16[2,128,128]{2,1,0:T(8,128)(2,1)S(1)} %collective-permute-done.7.refs_3_, ...), custom_call_target="tpu_custom_call" | custom-call | flops 1073741824 | bytes 4194304 | tf_op jit(solution)/shard_map/pallas_call | solution.py:421
  (39 shorter events, 0.3 us)
Async XLA Ops:
  0.0 1.2 %copy-start = (bf16[256,2048]{1,0:T(8,128)(2,1)S(1)}, bf16[256,2048]{1,0:T(8,128)(2,1)}, u32[]{:S(2)}) copy-start(bf16[256,2048]{1,0:T(8,128)(2,1)} %refs_1_.1) | copy-start | bytes 3145732
  1.2 1.0 %copy-start.5 = (bf16[1,256,1024]{2,1,0:T(8,128)(2,1)S(1)}, bf16[1,256,1024]{2,1,0:T(8,128)(2,1)}, u32[]{:S(2)}) copy-start(bf16[1,256,1024]{2,1,0:T(8,128)(2,1)} %param.10) | copy-start | bytes 1572868
  2.3 21.3 %copy-start.2 = (f32[2,256,8]{2,1,0:T(8,128)S(1)}, f32[2,256,8]{2,1,0:T(8,128)}, u32[]{:S(2)}) copy-start(f32[2,256,8]{2,1,0:T(8,128)} %constant.16.clone.refs_7_) | copy-start | bytes 49156
  2.3 21.3 %copy-start.3 = (bf16[256,512]{1,0:T(8,128)(2,1)S(1)}, bf16[256,512]{1,0:T(8,128)(2,1)}, u32[]{:S(2)}) copy-start(bf16[256,512]{1,0:T(8,128)(2,1)} %constant.15.clone.refs_6_) | copy-start | bytes 786436
  2.3 21.3 %copy-start.4 = (bf16[256,512]{1,0:T(8,128)(2,1)S(1)}, bf16[256,512]{1,0:T(8,128)(2,1)}, u32[]{:S(2)}) copy-start(bf16[256,512]{1,0:T(8,128)(2,1)} %constant.14.clone.refs_5_) | copy-start | bytes 786436
  3.4 26.9 %collective-permute-start.14 = (bf16[128,2048]{1,0:T(8,128)(2,1)S(1)}, bf16[128,2048]{1,0:T(8,128)(2,1)S(1)}, u32[]{:S(2)}, u32[]{:S(2)}) collective-permute-start(bf16[128,2048]{1,0:T(8,128)(2,1)S(1)} %get-tuple-element.45.refs_8_), channel_id=1, source_target_pairs={{0,2},{1,3},{2,0},{3,1},{4,6},{5,7},{6,4},{7,5},{8,10},{9,11},{10,... | collective-permute-start | bytes 1572872 | tf_op jit(solution)/shard_map/ppermute | solution.py:309
  6.4 23.9 %collective-permute-start.13 = (bf16[128,2048]{1,0:T(8,128)(2,1)S(1)}, bf16[128,2048]{1,0:T(8,128)(2,1)S(1)}, u32[]{:S(2)}, u32[]{:S(2)}) collective-permute-start(bf16[128,2048]{1,0:T(8,128)(2,1)S(1)} %get-tuple-element.45.refs_8_), channel_id=1, source_target_pairs={{0,1},{1,0},{2,3},{3,2},{4,5},{5,4},{6,7},{7,6},{8,9},{9,8},{10,11... | collective-permute-start | bytes 1572872 | tf_op jit(solution)/shard_map/ppermute | solution.py:309
  7.9 6.5 %collective-permute-start = (bf16[2,256,128]{2,1,0:T(8,128)(2,1)S(1)}, bf16[2,256,128]{2,1,0:T(8,128)(2,1)S(1)}, u32[]{:S(2)}, u32[]{:S(2)}) collective-permute-start(bf16[2,256,128]{2,1,0:T(8,128)(2,1)S(1)} %get-tuple-element.28), channel_id=1, source_target_pairs={{0,8},{4,12},{8,0},{12,4},{16,24},{20,28},{24,16},{28,20},{1,9},{5... | collective-permute-start | bytes 393224 | tf_op jit(solution)/shard_map/ppermute | solution.py:309
  9.5 12.4 %collective-permute-start.1 = (bf16[2,256,128]{2,1,0:T(8,128)(2,1)S(1)}, bf16[2,256,128]{2,1,0:T(8,128)(2,1)S(1)}, u32[]{:S(2)}, u32[]{:S(2)}) collective-permute-start(bf16[2,256,128]{2,1,0:T(8,128)(2,1)S(1)} %get-tuple-element.29), channel_id=1, source_target_pairs={{0,16},{4,20},{8,24},{12,28},{16,0},{20,4},{24,8},{28,12},{1,17},{... | collective-permute-start | bytes 393224 | tf_op jit(solution)/shard_map/ppermute | solution.py:309
  12.1 9.8 %collective-permute-start.2 = (bf16[2,256,128]{2,1,0:T(8,128)(2,1)S(1)}, bf16[2,256,128]{2,1,0:T(8,128)(2,1)S(1)}, u32[]{:S(2)}, u32[]{:S(2)}) collective-permute-start(bf16[2,256,128]{2,1,0:T(8,128)(2,1)S(1)} %get-tuple-element.30), channel_id=1, source_target_pairs={{0,24},{4,28},{8,16},{12,20},{16,8},{20,12},{24,0},{28,4},{1,25},{... | collective-permute-start | bytes 393224 | tf_op jit(solution)/shard_map/ppermute | solution.py:309
  21.9 1.6 %collective-permute-start.8 = (bf16[4,256,128]{2,1,0:T(8,128)(2,1)S(1)}, bf16[4,256,128]{2,1,0:T(8,128)(2,1)S(1)}, u32[]{:S(2)}, u32[]{:S(2)}) collective-permute-start(bf16[4,256,128]{2,1,0:T(8,128)(2,1)S(1)} %get-tuple-element.38), channel_id=1, source_target_pairs={{0,4},{4,0},{8,12},{12,8},{16,20},{20,16},{24,28},{28,24},{1,5},{5... | collective-permute-start | bytes 786440 | tf_op jit(solution)/shard_map/ppermute | solution.py:309
  22.0 31.1 %copy-start.1 = (bf16[1,256,2048]{2,1,0:T(8,128)(2,1)S(1)}, bf16[1,256,2048]{2,1,0:T(8,128)(2,1)}, u32[]{:S(2)}) copy-start(bf16[1,256,2048]{2,1,0:T(8,128)(2,1)} %param.11) | copy-start | bytes 3145732
  22.0 31.1 %copy-start.8 = (bf16[128,256]{1,0:T(8,128)(2,1)S(1)}, bf16[128,256]{1,0:T(8,128)(2,1)}, u32[]{:S(2)}) copy-start(bf16[128,256]{1,0:T(8,128)(2,1)} %constant.18.clone.refs_6_) | copy-start | bytes 196612
  22.0 31.1 %copy-start.9 = (bf16[128,256]{1,0:T(8,128)(2,1)S(1)}, bf16[128,256]{1,0:T(8,128)(2,1)}, u32[]{:S(2)}) copy-start(bf16[128,256]{1,0:T(8,128)(2,1)} %constant.17.clone.refs_5_) | copy-start | bytes 196612
  22.0 6.4 %collective-permute-start.3 = (bf16[4,256,128]{2,1,0:T(8,128)(2,1)S(1)}, bf16[4,256,128]{2,1,0:T(8,128)(2,1)S(1)}, u32[]{:S(2)}, u32[]{:S(2)}) collective-permute-start(bf16[4,256,128]{2,1,0:T(8,128)(2,1)S(1)} %get-tuple-element.31), channel_id=1, source_target_pairs={{0,4},{4,0},{8,12},{12,8},{16,20},{20,16},{24,28},{28,24},{1,5},{5... | collective-permute-start | bytes 786440 | tf_op jit(solution)/shard_map/ppermute | solution.py:309
  25.3 5.9 %collective-permute-start.9 = (bf16[2,128,128]{2,1,0:T(8,128)(2,1)S(1)}, bf16[2,128,128]{2,1,0:T(8,128)(2,1)S(1)}, u32[]{:S(2)}, u32[]{:S(2)}) collective-permute-start(bf16[2,128,128]{2,1,0:T(8,128)(2,1)S(1)} %get-tuple-element.40), channel_id=1, source_target_pairs={{0,8},{4,12},{8,0},{12,4},{16,24},{20,28},{24,16},{28,20},{1,9},{5... | collective-permute-start | bytes 196616 | tf_op jit(solution)/shard_map/ppermute | solution.py:309
  27.4 29.5 %copy-start.6 = (bf16[128,256]{1,0:T(8,128)(2,1)S(1)}, bf16[128,256]{1,0:T(8,128)(2,1)}, u32[]{:S(2)}) copy-start(bf16[128,256]{1,0:T(8,128)(2,1)} %constant.20.clone.refs_5_) | copy-start | bytes 196612
  27.4 29.5 %copy-start.7 = (bf16[128,256]{1,0:T(8,128)(2,1)S(1)}, bf16[128,256]{1,0:T(8,128)(2,1)}, u32[]{:S(2)}) copy-start(bf16[128,256]{1,0:T(8,128)(2,1)} %constant.19.clone.refs_4_) | copy-start | bytes 196612
  27.4 6.2 %collective-permute-start.10 = (bf16[2,128,128]{2,1,0:T(8,128)(2,1)S(1)}, bf16[2,128,128]{2,1,0:T(8,128)(2,1)S(1)}, u32[]{:S(2)}, u32[]{:S(2)}) collective-permute-start(bf16[2,128,128]{2,1,0:T(8,128)(2,1)S(1)} %get-tuple-element.41), channel_id=1, source_target_pairs={{0,16},{4,20},{8,24},{12,28},{16,0},{20,4},{24,8},{28,12},{1,17},{... | collective-permute-start | bytes 196616 | tf_op jit(solution)/shard_map/ppermute | solution.py:309
  30.2 3.3 %collective-permute-start.4 = (bf16[4,128,128]{2,1,0:T(8,128)(2,1)S(1)}, bf16[4,128,128]{2,1,0:T(8,128)(2,1)S(1)}, u32[]{:S(2)}, u32[]{:S(2)}) collective-permute-start(bf16[4,128,128]{2,1,0:T(8,128)(2,1)S(1)} %get-tuple-element.33), channel_id=1, source_target_pairs={{0,4},{4,0},{8,12},{12,8},{16,20},{20,16},{24,28},{28,24},{1,5},{5... | collective-permute-start | bytes 393224 | tf_op jit(solution)/shard_map/ppermute | solution.py:309
  30.4 14.6 %collective-permute-start.15 = (bf16[64,2048]{1,0:T(8,128)(2,1)S(1)}, bf16[64,2048]{1,0:T(8,128)(2,1)S(1)}, u32[]{:S(2)}, u32[]{:S(2)}) collective-permute-start(bf16[64,2048]{1,0:T(8,128)(2,1)S(1)} %get-tuple-element.47), channel_id=1, source_target_pairs={{0,1},{1,0},{2,3},{3,2},{4,5},{5,4},{6,7},{7,6},{8,9},{9,8},{10,11... | collective-permute-start | bytes 786440 | tf_op jit(solution)/shard_map/ppermute | solution.py:309
  31.0 25.9 %collective-permute-start.18 = (bf16[128,2048]{1,0:T(8,128)(2,1)S(1)}, bf16[128,2048]{1,0:T(8,128)(2,1)S(1)}, u32[]{:S(2)}, u32[]{:S(2)}) collective-permute-start(bf16[128,2048]{1,0:T(8,128)(2,1)S(1)} %collective-permute-done.14.second.refs_11_), channel_id=1, source_target_pairs={{0,4},{4,0},{8,12},{12,8},{16,20},{20,16},{24,28},{28,24},{1,5},{5... | collective-permute-start | bytes 1572872 | tf_op jit(solution)/shard_map/ppermute | solution.py:309
  31.2 13.8 %collective-permute-start.16 = (bf16[64,2048]{1,0:T(8,128)(2,1)S(1)}, bf16[64,2048]{1,0:T(8,128)(2,1)S(1)}, u32[]{:S(2)}, u32[]{:S(2)}) collective-permute-start(bf16[64,2048]{1,0:T(8,128)(2,1)S(1)} %get-tuple-element.48), channel_id=1, source_target_pairs={{0,2},{1,3},{2,0},{3,1},{4,6},{5,7},{6,4},{7,5},{8,10},{9,11},{10,... | collective-permute-start | bytes 786440 | tf_op jit(solution)/shard_map/ppermute | solution.py:309
  33.6 23.3 %collective-permute-start.17 = (bf16[128,2048]{1,0:T(8,128)(2,1)S(1)}, bf16[128,2048]{1,0:T(8,128)(2,1)S(1)}, u32[]{:S(2)}, u32[]{:S(2)}) collective-permute-start(bf16[128,2048]{1,0:T(8,128)(2,1)S(1)} %collective-permute-done.13.first.refs_10_), channel_id=1, source_target_pairs={{0,4},{4,0},{8,12},{12,8},{16,20},{20,16},{24,28},{28,24},{1,5},{5... | collective-permute-start | bytes 1572872 | tf_op jit(solution)/shard_map/ppermute | solution.py:309
  33.6 6.3 %collective-permute-start.11 = (bf16[2,128,128]{2,1,0:T(8,128)(2,1)S(1)}, bf16[2,128,128]{2,1,0:T(8,128)(2,1)S(1)}, u32[]{:S(2)}, u32[]{:S(2)}) collective-permute-start(bf16[2,128,128]{2,1,0:T(8,128)(2,1)S(1)} %get-tuple-element.42), channel_id=1, source_target_pairs={{0,24},{4,28},{8,16},{12,20},{16,8},{20,12},{24,0},{28,4},{1,25},{... | collective-permute-start | bytes 196616 | tf_op jit(solution)/shard_map/ppermute | solution.py:309
  39.9 4.3 %collective-permute-start.5 = (bf16[2,128,128]{2,1,0:T(8,128)(2,1)S(1)}, bf16[2,128,128]{2,1,0:T(8,128)(2,1)S(1)}, u32[]{:S(2)}, u32[]{:S(2)}) collective-permute-start(bf16[2,128,128]{2,1,0:T(8,128)(2,1)S(1)} %get-tuple-element.35), channel_id=1, source_target_pairs={{0,8},{4,12},{8,0},{12,4},{16,24},{20,28},{24,16},{28,20},{1,9},{5... | collective-permute-start | bytes 196616 | tf_op jit(solution)/shard_map/ppermute | solution.py:309
  44.1 5.3 %collective-permute-start.6 = (bf16[2,128,128]{2,1,0:T(8,128)(2,1)S(1)}, bf16[2,128,128]{2,1,0:T(8,128)(2,1)S(1)}, u32[]{:S(2)}, u32[]{:S(2)}) collective-permute-start(bf16[2,128,128]{2,1,0:T(8,128)(2,1)S(1)} %get-tuple-element.36), channel_id=1, source_target_pairs={{0,16},{4,20},{8,24},{12,28},{16,0},{20,4},{24,8},{28,12},{1,17},{... | collective-permute-start | bytes 196616 | tf_op jit(solution)/shard_map/ppermute | solution.py:309
  45.0 11.9 %collective-permute-start.19 = (bf16[64,2048]{1,0:T(8,128)(2,1)S(1)}, bf16[64,2048]{1,0:T(8,128)(2,1)S(1)}, u32[]{:S(2)}, u32[]{:S(2)}) collective-permute-start(bf16[64,2048]{1,0:T(8,128)(2,1)S(1)} %collective-permute-done.15.refs_12_), channel_id=1, source_target_pairs={{0,4},{4,0},{8,12},{12,8},{16,20},{20,16},{24,28},{28,24},{1,5},{5... | collective-permute-start | bytes 786440 | tf_op jit(solution)/shard_map/ppermute | solution.py:309
  45.0 11.8 %collective-permute-start.20 = (bf16[64,2048]{1,0:T(8,128)(2,1)S(1)}, bf16[64,2048]{1,0:T(8,128)(2,1)S(1)}, u32[]{:S(2)}, u32[]{:S(2)}) collective-permute-start(bf16[64,2048]{1,0:T(8,128)(2,1)S(1)} %collective-permute-done.16.refs_13_), channel_id=1, source_target_pairs={{0,4},{4,0},{8,12},{12,8},{16,20},{20,16},{24,28},{28,24},{1,5},{5... | collective-permute-start | bytes 786440 | tf_op jit(solution)/shard_map/ppermute | solution.py:309
  49.5 1.3 %collective-permute-start.12 = (bf16[4,128,128]{2,1,0:T(8,128)(2,1)S(1)}, bf16[4,128,128]{2,1,0:T(8,128)(2,1)S(1)}, u32[]{:S(2)}, u32[]{:S(2)}) collective-permute-start(bf16[4,128,128]{2,1,0:T(8,128)(2,1)S(1)} %shard_map.105), channel_id=1, source_target_pairs={{0,4},{4,0},{8,12},{12,8},{16,20},{20,16},{24,28},{28,24},{1,5},{5... | collective-permute-start | bytes 393224 | tf_op jit(solution)/shard_map/ppermute | solution.py:309
  50.8 6.1 %collective-permute-start.7 = (bf16[2,128,128]{2,1,0:T(8,128)(2,1)S(1)}, bf16[2,128,128]{2,1,0:T(8,128)(2,1)S(1)}, u32[]{:S(2)}, u32[]{:S(2)}) collective-permute-start(bf16[2,128,128]{2,1,0:T(8,128)(2,1)S(1)} %get-tuple-element.37), channel_id=1, source_target_pairs={{0,24},{4,28},{8,16},{12,20},{16,8},{20,12},{24,0},{28,4},{1,25},{... | collective-permute-start | bytes 196616 | tf_op jit(solution)/shard_map/ppermute | solution.py:309

commit v3 on v2

--- a/solution.py
+++ b/solution.py
@@ -62,12 +62,12 @@
 
 def pick_kernel(chips, fast, *refs):
     x_ref, w_ref = refs[:2]
-    outs = refs[2 : 2 + chips]
-    halves = refs[2 + chips : -3]
+    outs = [refs[2 + q * chips : 2 + (q + 1) * chips] for q in range(CHUNKS)]
+    halves = refs[2 + CHUNKS * chips : -3]
     tokens, x_sems, w_sems = refs[-3:]
     row = lax.axis_index("row")
     core, chip = row % 2, row // 2
-    lanes = outs[0].shape[2]
+    lanes = outs[0][0].shape[1]
     pairs = lanes // 2
     chips_per_group = GROUP // (CHUNKS * lanes)
     loads = []
@@ -96,16 +96,14 @@
         loads[zs].wait()
         got = jnp.dot(tokens[zs], choose, preferred_element_type=jnp.float32).astype(jnp.bfloat16)
         for q in range(CHUNKS):
-            outs[zs][q] = got[:, q * lanes : (q + 1) * lanes]
+            outs[q][zs][...] = got[:, q * lanes : (q + 1) * lanes]
     for fetch in fetches:
         fetch.wait()
 
 
 def stack_kernel(*refs):
-    pieces, outs = refs[:-CHUNKS], refs[-CHUNKS:]
-    for q, out in enumerate(outs):
-        for zs, piece in enumerate(pieces):
-            out[zs] = piece[q]
+    for zs, piece in enumerate(refs[:-1]):
+        refs[-1][zs] = piece[...]
 
 
 def complex_dft(values):
@@ -132,9 +130,9 @@
 def position_kernel(rows, q, *refs):
     chips = rows // 2
     mine, theirs = refs[:chips], refs[chips]
-    table_hi, table_lo, twist = refs[chips + 1 : chips + 4]
-    *outs, folded, z_hi, z_lo, spect = refs[chips + 4 :]
-    inner, lanes = mine[0].shape[1:]
+    table, twist = refs[chips + 1 : chips + 3]
+    *outs, folded, turned_z, spect = refs[chips + 3 :]
+    inner, lanes = mine[0].shape
     pairs = lanes // 2
     row = lax.axis_index("row")
     core, chip = row % 2, row // 2
@@ -158,7 +156,7 @@
         return value * own + turned * other
 
     for zs in range(chips):
-        folded[row ^ (2 * zs)] = fold(mine[zs][q])
+        folded[row ^ (2 * zs)] = fold(mine[zs][...])
         folded[row ^ (2 * zs + 1)] = fold(theirs[zs])
 
     odd_core = core == 1
@@ -187,20 +185,14 @@
             b = jnp.where(cosine, im, re)
             c, s = tw[:, j : j + 1], tw[:, half + j : half + j + 1]
             for where, z in ((at, a * c + b * s), (low_at, b * c - a * s)):
-                head = z.astype(jnp.bfloat16)
-                cols = slice(j * lanes, (j + 1) * lanes)
-                z_hi[where, cols] = head
-                z_lo[where, cols] = (z - head.astype(jnp.float32)).astype(jnp.bfloat16)
+                turned_z[where, j * lanes : (j + 1) * lanes] = z.astype(jnp.bfloat16)
         return carry
 
     lax.fori_loop(0, inner // tile, step, 0)
-    dot = functools.partial(jnp.dot, preferred_element_type=jnp.float32)
     width = min(half * lanes, 256)
     for start in range(0, half * lanes, width):
         cols = slice(start, start + width)
-        value = dot(table_hi[...], z_hi[:, cols])
-        value += dot(table_hi[...], z_lo[:, cols])
-        value += dot(table_lo[...], z_hi[:, cols])
+        value = jnp.dot(table[...], turned_z[:, cols], preferred_element_type=jnp.float32)
         for j in range(start // lanes, (start + width) // lanes):
             piece = value[:, j * lanes - start : (j + 1) * lanes - start]
             spect[j] = piece
@@ -210,11 +202,7 @@
             dest = row ^ (2 * zs + rel)
             for j in range(half):
                 piece = spect[j, pl.ds(pl.multiple_of(dest * per, per), per), :]
-                lines = slice(j * per, (j + 1) * per)
-                if q == 0:
-                    outs[zs][rel, lines, :] = piece.astype(jnp.bfloat16)
-                else:
-                    outs[rel][zs, lines, :] = piece.astype(jnp.bfloat16)
+                outs[zs][rel, j * per : (j + 1) * per, :] = piece.astype(jnp.bfloat16)
 
 
 def order_rows(rows, count):
@@ -232,10 +220,9 @@
         out[zs] = ref[1]
 
 
-def join_kernel(keep, got, *outs):
-    for zs, out in enumerate(outs):
-        out[0] = keep[zs]
-        out[1] = got[zs]
+def join_kernel(first, second, out):
+    out[0] = first[...]
+    out[1] = second[...]
 
 
 def channel_part(order, pieces, feat_hi, feat_lo):
@@ -263,40 +250,33 @@
         opened[:, cols] = jax.nn.sigmoid(gate_ref[:, cols].astype(jnp.float32))
 
 
-def relay_kernel(first, second, to_first, to_second):
-    rows = to_first.shape[0]
-    to_first[...] = second[:rows, :]
-    to_second[...] = first[rows:, :]
-
-
 def final_kernel(rows, *refs):
     chips = rows // 2
-    mine, feat_hi, feat_lo, spect, opened = refs[:chips], *refs[chips : chips + 4]
-    w_mine, w_rest, *w_far, out_ref, lhs, result, sems = refs[chips + 4 :]
+    mine, theirs, feat_hi, feat_lo, spect, opened = refs[:chips], *refs[chips : chips + 5]
+    w_mine, w_rest, w_a, w_b, v_a, v_b, out_ref, lhs, result, sems = refs[chips + 5 :]
     count, width = opened.shape
     half = GROUP // 2
     row, col = lax.axis_index("row"), lax.axis_index("col")
     core, chip = row % 2, row // 2
     order = order_rows(rows, count)
-    pieces = [(ref[0], ref[1]) for ref in mine]
+    pieces = [(ref[0], theirs[zs]) for zs, ref in enumerate(mine)]
     for zs, part in enumerate(channel_part(order, pieces, feat_hi[...], feat_lo[...])):
         whole = (part + spect[zs]).astype(jnp.bfloat16)
         for h in range(2):
             spot = pl.ds(pl.multiple_of((core ^ h) * half, half), half)
             lhs[zs, :, spot] = whole[:, h * half : (h + 1) * half]
-    first, second, low, high = (w_far[i::4] for i in range(4))
+    weights = (
+        (0, lambda at: (w_mine[:, at], w_rest[:, at])),
+        (1 + core, lambda at: (w_a[:, at], v_b[0, :, at])),
+        (2 - core, lambda at: (w_b[0, :, at], v_a[:, at])),
+        (3, lambda at: (w_b[1, :, at], v_b[1, :, at])),
+    )
     copies = []
     for t in range(width // GROUP):
         cols = slice(t * GROUP, (t + 1) * GROUP)
         total = jnp.zeros((count, GROUP), jnp.float32)
-        for s in range(4):
-            if s == 0:
-                parts = [w_mine[:, cols], w_rest[:, cols]]
-            elif s < 3:
-                parts = [ref[:, cols] for ref in (first, second)[s - 1]]
-            else:
-                parts = [ref[:, cols] for pair in zip(low, high) for ref in pair]
-            rhs = jnp.concatenate(parts, axis=0)
+        for s, halves in weights:
+            rhs = jnp.concatenate(halves(cols), axis=0)
             total += jnp.dot(lhs[chip ^ col ^ s], rhs, preferred_element_type=jnp.float32)
         result[:, cols] = (opened[:, cols] * total).astype(jnp.bfloat16)
         copies.append(pltpu.make_async_copy(result.at[:, cols], out_ref.at[:, cols], sems.at[t]))
@@ -307,6 +287,15 @@
 
 def swap(value, axis, size, bit):
     return lax.ppermute(value, axis, [(i, i ^ bit) for i in range(size)])
+
+
+def turn_swap(value, rows, n_col, bits):
+    turn = [
+        (row * n_col + col, row * n_col + (col ^ bits[row % 2]))
+        for row in range(rows)
+        for col in range(n_col)
+    ]
+    return lax.ppermute(value, ("row", "col"), turn)
 
 
 def send_order(chips):
@@ -333,7 +322,7 @@
     half = rows // 2
     width = w_proj.shape[1]
     scale = 1.0 / math.sqrt(count * rows * GROUP)
-    table_hi, table_lo = split_halves(position_table(count, scale))
+    table = position_table(count, scale).astype(jnp.bfloat16)
     twist = twist_table(rows, count)
     features_of = feature_table(lanes // 2)
     feat_hi, feat_lo = split_halves(features_of)
@@ -343,10 +332,10 @@
     half_w = jax.ShapeDtypeStruct((GROUP // 2, width), bf)
     picked = pl.pallas_call(
         functools.partial(pick_kernel, chips, fast),
-        out_shape=[jax.ShapeDtypeStruct((CHUNKS, count, lanes), bf)] * chips
+        out_shape=[jax.ShapeDtypeStruct((count, lanes), bf)] * (CHUNKS * chips)
         + [half_w] * (2 * fast),
-        in_specs=[pl.BlockSpec(memory_space=pl.ANY)] * 2,
-        out_specs=[pl.BlockSpec(memory_space=pltpu.VMEM)] * (chips + 2 * fast),
+        in_specs=[pl.BlockSpec(memory_space=pltpu.HBM)] * 2,
+        out_specs=[pl.BlockSpec(memory_space=pltpu.VMEM)] * (CHUNKS * chips + 2 * fast),
         scratch_shapes=[
             pltpu.VMEM((chips, count, GROUP), bf),
             pltpu.SemaphoreType.DMA((chips,)),
@@ -356,57 +345,50 @@
         cost_estimate=pl.CostEstimate(
             flops=2 * count * GROUP * features, bytes_accessed=MIB, transcendentals=0
         ),
-    )(tokens, w_proj)
-    arrived = across_chips(picked[:chips], rows)
+    )(*(pltpu.with_memory_space_constraint(v, pltpu.HBM) for v in (tokens, w_proj)))
+    arrived = [across_chips(picked[q * chips : (q + 1) * chips], rows) for q in range(CHUNKS)]
 
     if fast:
-        mine, rest = picked[chips:]
-        w_own = []
-        part = jax.ShapeDtypeStruct((GROUP // 4, width), bf)
-        for s in (1, 2):
-            w_own.append(swap(mine, "col", n_col, s))
-        passed = vmem_call(relay_kernel, [part] * 2, [], GROUP * width, 2 * GROUP * width)(*w_own)
-        for s in (1, 2):
-            w_own.append(swap(passed[s - 1], "col", n_col, s))
-        w_other = []
-        for own in w_own:
-            w_other.append(swap(own, "row", rows, 1))
-
-    stacks = vmem_call(
-        stack_kernel,
-        [jax.ShapeDtypeStruct((chips, count, lanes), bf)] * CHUNKS,
-        [],
-        count * features,
-        4 * count * features,
-    )(*arrived)
+        mine, rest = picked[CHUNKS * chips :]
+        w_a = turn_swap(mine, rows, n_col, (1, 2))
+        pair = vmem_call(
+            join_kernel,
+            jax.ShapeDtypeStruct((2, GROUP // 2, width), bf),
+            [],
+            GROUP * width,
+            4 * GROUP * width,
+        )(mine, w_a)
+        w_b = turn_swap(pair, rows, n_col, (2, 1))
+        v_a = swap(w_a, "row", rows, 1)
+        v_b = swap(w_b, "row", rows, 1)
+
     lines = half * (count // rows)
     piece = jax.ShapeDtypeStruct((2, lines, lanes), bf)
-    stacked = jax.ShapeDtypeStruct((chips, lines, lanes), bf)
     small = (count * features // 4, count * features)
-    sent = []
+    received = []
     for q in range(CHUNKS):
-        theirs = swap(stacks[q], "row", rows, 1)
-        sent.append(
-            vmem_call(
-                functools.partial(position_kernel, rows, q),
-                [piece] * chips if q == 0 else [stacked] * 2,
-                [
-                    pltpu.VMEM((rows, count, lanes), jnp.float32),
-                    pltpu.VMEM((2 * count, half * lanes), bf),
-                    pltpu.VMEM((2 * count, half * lanes), bf),
-                    pltpu.VMEM((half, count, lanes), jnp.float32),
-                ],
-                12 * count * count * half * lanes,
-                rows * count * lanes * 4,
-            )(*arrived, theirs, table_hi, table_lo, twist)
-        )
-    early = across_chips(sent[0], rows)
-    give = vmem_call(give_kernel, stacked, [], *small)(*early)
-    early.append(swap(give, "row", rows, 1))
-    keep, give = sent[1]
-    got = swap(give, "row", rows, 1)
-    joined = vmem_call(join_kernel, [piece] * chips, [], *small)(keep, got)
-    late = across_chips(joined, rows)
+        stack = vmem_call(
+            stack_kernel, jax.ShapeDtypeStruct((chips, count, lanes), bf), [], *small
+        )(*arrived[q])
+        theirs = swap(stack, "row", rows, 1)
+        sent = vmem_call(
+            functools.partial(position_kernel, rows, q),
+            [piece] * chips,
+            [
+                pltpu.VMEM((rows, count, lanes), jnp.float32),
+                pltpu.VMEM((2 * count, half * lanes), bf),
+                pltpu.VMEM((half, count, lanes), jnp.float32),
+            ],
+            4 * count * count * half * lanes,
+            rows * count * lanes * 4,
+        )(*arrived[q], theirs, table, twist)
+        got = across_chips(sent, rows)
+        give = vmem_call(
+            give_kernel, jax.ShapeDtypeStruct((chips, lines, lanes), bf), [], *small
+        )(*got)
+        got.append(swap(give, "row", rows, 1))
+        received.append(got)
+    early, late = received
     if fast:
         spect, opened = vmem_call(
             functools.partial(prepare_kernel, rows),
@@ -421,7 +403,7 @@
         return pl.pallas_call(
             functools.partial(final_kernel, rows),
             out_shape=jax.ShapeDtypeStruct((count, width), bf),
-            in_specs=[pl.BlockSpec(memory_space=pltpu.VMEM)] * (chips + 14),
+            in_specs=[pl.BlockSpec(memory_space=pltpu.VMEM)] * (chips + 11),
             out_specs=pl.BlockSpec(memory_space=pl.ANY),
             scratch_shapes=[
                 pltpu.VMEM((chips, count, GROUP), bf),
@@ -434,7 +416,7 @@
                 bytes_accessed=2 * features * width,
                 transcendentals=0,
             ),
-        )(*late, feat_hi[1], feat_lo[1], spect, opened, mine, rest, *w_own, *w_other)
+        )(*late, feat_hi[1], feat_lo[1], spect, opened, mine, rest, w_a, w_b, v_a, v_b)
 
     weights = lax.all_gather(w_proj, "col", axis=0, tiled=True).reshape(-1, GROUP, width)
     order = order_rows(rows, count)
@@ -444,10 +426,7 @@
     spectrum = jnp.zeros((count, weights.shape[0], GROUP), jnp.float32)
     here = chip ^ jnp.arange(chips)
     for q in range(CHUNKS):
-        if q == 0:
-            parts = [(early[zs][0], early[chips][zs]) for zs in range(chips)]
-        else:
-            parts = [(ref[0], ref[1]) for ref in late]
+        parts = [(received[q][zs][0], received[q][chips][zs]) for zs in range(chips)]
         got = jnp.stack([jnp.concatenate(pair, axis=0) for pair in parts])[here]
         got = jnp.einsum("kr,zrl->kzl", order, got, preferred_element_type=jnp.float32)
         spectrum += jnp.einsum(

time: 59.8 us -> 66.6 us (1.11)
  starting transfers between devices: 20 us -> 26.9 us
  local copies, waits for them, and re-layouts: 2.3 us -> 0.04 us
  waiting for transfers between devices: 28.9 us -> 30.9 us
    ppermute x0 -> x2, waiting for transfers between devices: none -> 19.9 us  [turn_swap(): return lax.ppermute(value, ('row', 'col'), turn)]
    ppermute x21 -> x18, waiting for transfers between devices: 28.9 us -> 11 us  [swap(): return lax.ppermute(value, axis, [(i, i ^ bit) for i in range(size)])]
    ppermute x0 -> x2, starting transfers between devices: none -> 5.14 us  [turn_swap(): return lax.ppermute(value, ('row', 'col'), turn)]
    unnamed x20 -> x14, local copies, waits for them, and re-layouts: 2.3 us -> 0.04 us
    ppermute x21 -> x18, starting transfers between devices: 20 us -> 21.8 us  [swap(): return lax.ppermute(value, axis, [(i, i ^ bit) for i in range(size)])]
    pallas_call x1, Pallas kernels: 1.1 us -> 1.88 us  [program(): pl.pallas_call(functools.partial(pick_kernel, chips, fast), out_shape=[ja...]
    pallas_call x6 -> x7, Pallas kernels: 3.64 us -> 3.08 us  [the longest x2 2.95 us: program(): vmem_call(functools.partial(position_kernel, rows, q), [piece] * chips, [...]
  transfers between devices with their start and end apart: 21 -> 20, of which waited for: 9 -> 9; matrix products, arithmetic and copies ran while one was open for 0% -> 0% of each run, Pallas kernels for 7% -> 6%
where the time goes in v3:
time: 66.6 us; the launch traced here: 66.5 us
  waiting for transfers between devices  30.9 us (46%)
  starting transfers between devices  26.9 us (40%)
  Pallas kernels  8.38 us (13%)
    ppermute x18, starting transfers between devices, swap(): return lax.ppermute(value, axis, [(i, i ^ bit) for i in range(size)])  21.8 us
    ppermute x2, waiting for transfers between devices, turn_swap(): return lax.ppermute(value, ('row', 'col'), turn)  19.9 us
    ppermute x18, waiting for transfers between devices, swap(): return lax.ppermute(value, axis, [(i, i ^ bit) for i in range(size)])  11 us
    ppermute x2, starting transfers between devices, turn_swap(): return lax.ppermute(value, ('row', 'col'), turn)  5.14 us
    pallas_call x2, Pallas kernels, program(): vmem_call(functools.partial(position_kernel, rows, q), [piece] * chips, [...  2.95 us
    pallas_call x1, Pallas kernels, program(): pl.pallas_call(functools.partial(final_kernel, rows), out_shape=jax.Shape...  2.65 us
    pallas_call x1, Pallas kernels, program(): pl.pallas_call(functools.partial(pick_kernel, chips, fast), out_shape=[ja...  1.88 us
  transfers between devices with their start and end apart: 20, of which 9 were waited for; matrix products, arithmetic and copies ran while one was open for 0% of the time, Pallas kernels for 6%

profile of v3, /device:TPU:0, one launch (start us, length us, event | category | flops | bytes accessed | tf_op | source)
XLA Modules:
  0.0 66.5 jit_solution(3248446797479083055)
XLA Ops:
  0.0 1.9 %shard_map.91 = (bf16[256,128]{1,0:T(8,128)(2,1)S(1)}, bf16[256,128]{1,0:T(8,128)(2,1)S(1)}, bf16[256,128]{1,0:T(8,128)(2,1)S(1)}, bf16[256,128]{1,0:T(8,128)(2,...) custom-call(bf16[256,1024]{1,0:T(8,128)(2,1)} %bitcast.4, ...), custom_call_target="tpu_custom_call" | custom-call | flops 134217728 | bytes 1048576 | tf_op jit(solution)/shard_map/pallas_call | solution.py:333
  1.9 3.0 %collective-permute-start.16 = (bf16[128,2048]{1,0:T(8,128)(2,1)S(1)}, bf16[128,2048]{1,0:T(8,128)(2,1)S(1)}, u32[]{:S(2)}, u32[]{:S(2)}) collective-permute-start(bf16[128,2048]{1,0:T(8,128)(2,1)S(1)} %get-tuple-element.43.first.refs_9_), channel_id=1, source_target_pairs={{0,1},{1,0},{2,3},{3,2},{4,6},{5,7},{6,4},{7,5},{8,9},{9,8},{10,11... | collective-permute-start | bytes 1572872 | tf_op jit(solution)/shard_map/ppermute | solution.py:298
  4.9 7.2 %collective-permute-done.16.second.refs_11_ = bf16[128,2048]{1,0:T(8,128)(2,1)S(1)} collective-permute-done((bf16[128,2048]{1,0:T(8,128)(2,1)S(1)}, bf16[128,2048]{1,0:T(8,128)(2,1)S(1)}, u32[]{:S(2)}, u32[]{:S(2)}) %collective-permute-start.16) | collective-permute-done | bytes 524320 | tf_op jit(solution)/shard_map/ppermute | solution.py:298
  12.2 2.1 %collective-permute-start.17 = (bf16[2,128,2048]{2,1,0:T(8,128)(2,1)S(1)}, bf16[2,128,2048]{2,1,0:T(8,128)(2,1)S(1)}, u32[]{:S(2)}, u32[]{:S(2)}) collective-permute-start(bf16[2,128,2048]{2,1,0:T(8,128)(2,1)S(1)} %shard_map.99), channel_id=1, source_target_pairs={{0,2},{1,3},{2,0},{3,1},{4,5},{5,4},{6,7},{7,6},{8,10},{9,11},{10,... | collective-permute-start | bytes 3145736 | tf_op jit(solution)/shard_map/ppermute | solution.py:298
  14.3 12.8 %collective-permute-done.17.refs_12_ = bf16[2,128,2048]{2,1,0:T(8,128)(2,1)S(1)} collective-permute-done((bf16[2,128,2048]{2,1,0:T(8,128)(2,1)S(1)}, bf16[2,128,2048]{2,1,0:T(8,128)(2,1)S(1)}, u32[]{:S(2)}, u32[]{:S(2)}) %collective-permute-start.17) | collective-permute-done | bytes 1048608 | tf_op jit(solution)/shard_map/ppermute | solution.py:298
  27.1 2.1 %collective-permute-start.8 = (bf16[256,128]{1,0:T(8,128)(2,1)S(1)}, bf16[256,128]{1,0:T(8,128)(2,1)S(1)}, u32[]{:S(2)}, u32[]{:S(2)}) collective-permute-start(bf16[256,128]{1,0:T(8,128)(2,1)S(1)} %get-tuple-element.34), channel_id=1, source_target_pairs={{0,8},{4,12},{8,0},{12,4},{16,24},{20,28},{24,16},{28,20},{1,9},{5... | collective-permute-start | bytes 196616 | tf_op jit(solution)/shard_map/ppermute | solution.py:289
  29.2 2.6 %collective-permute-start.9 = (bf16[256,128]{1,0:T(8,128)(2,1)S(1)}, bf16[256,128]{1,0:T(8,128)(2,1)S(1)}, u32[]{:S(2)}, u32[]{:S(2)}) collective-permute-start(bf16[256,128]{1,0:T(8,128)(2,1)S(1)} %get-tuple-element.35), channel_id=1, source_target_pairs={{0,16},{4,20},{8,24},{12,28},{16,0},{20,4},{24,8},{28,12},{1,17},{... | collective-permute-start | bytes 196616 | tf_op jit(solution)/shard_map/ppermute | solution.py:289
  31.8 0.9 %collective-permute-start = (bf16[256,128]{1,0:T(8,128)(2,1)S(1)}, bf16[256,128]{1,0:T(8,128)(2,1)S(1)}, u32[]{:S(2)}, u32[]{:S(2)}) collective-permute-start(bf16[256,128]{1,0:T(8,128)(2,1)S(1)} %get-tuple-element.26), channel_id=1, source_target_pairs={{0,8},{4,12},{8,0},{12,4},{16,24},{20,28},{24,16},{28,20},{1,9},{5... | collective-permute-start | bytes 196616 | tf_op jit(solution)/shard_map/ppermute | solution.py:289
  32.7 3.5 %collective-permute-start.1 = (bf16[256,128]{1,0:T(8,128)(2,1)S(1)}, bf16[256,128]{1,0:T(8,128)(2,1)S(1)}, u32[]{:S(2)}, u32[]{:S(2)}) collective-permute-start(bf16[256,128]{1,0:T(8,128)(2,1)S(1)} %get-tuple-element.27), channel_id=1, source_target_pairs={{0,16},{4,20},{8,24},{12,28},{16,0},{20,4},{24,8},{28,12},{1,17},{... | collective-permute-start | bytes 196616 | tf_op jit(solution)/shard_map/ppermute | solution.py:289
  36.2 0.1 collective-permute-done.9.refs_2_
  36.2 4.5 %collective-permute-start.2 = (bf16[256,128]{1,0:T(8,128)(2,1)S(1)}, bf16[256,128]{1,0:T(8,128)(2,1)S(1)}, u32[]{:S(2)}, u32[]{:S(2)}) collective-permute-start(bf16[256,128]{1,0:T(8,128)(2,1)S(1)} %get-tuple-element.28), channel_id=1, source_target_pairs={{0,24},{4,28},{8,16},{12,20},{16,8},{20,12},{24,0},{28,4},{1,25},{... | collective-permute-start | bytes 196616 | tf_op jit(solution)/shard_map/ppermute | solution.py:289
  40.7 0.1 collective-permute-start.11
  40.8 2.3 %collective-permute-done.1.refs_2_ = bf16[256,128]{1,0:T(8,128)(2,1)S(1)} collective-permute-done((bf16[256,128]{1,0:T(8,128)(2,1)S(1)}, bf16[256,128]{1,0:T(8,128)(2,1)S(1)}, u32[]{:S(2)}, u32[]{:S(2)}) %collective-permute-start.1) | collective-permute-done | bytes 65568 | tf_op jit(solution)/shard_map/ppermute | solution.py:289
  43.2 0.1 collective-permute-start.3
  43.3 0.5 collective-permute-start.18
  43.8 1.5 %shard_map.96 = (bf16[2,128,128]{2,1,0:T(8,128)(2,1)S(1)}, bf16[2,128,128]{2,1,0:T(8,128)(2,1)S(1)}, bf16[2,128,128]{2,1,0:T(8,128)(2,1)S(1)}, bf16[2,128,128]{2,1,0:T(8,128)(2,1)S(1)}) custom-call(bf16[256,128]{1,0:T(8,128)(2,1)S(1)} %get-tuple-element.33.refs_0_, bf16[256,128]{1,0:T(8,128)(2,1)S(1)} %collective-permute-done.8.refs_1_, ...), custom_call_target="tpu_custom_call" | custom-call | flops 134217728 | bytes 1048576 | tf_op jit(solution)/shard_map/pallas_call | solution.py:374
  45.3 1.6 %collective-permute-start.12 = (bf16[2,128,128]{2,1,0:T(8,128)(2,1)S(1)}, bf16[2,128,128]{2,1,0:T(8,128)(2,1)S(1)}, u32[]{:S(2)}, u32[]{:S(2)}) collective-permute-start(bf16[2,128,128]{2,1,0:T(8,128)(2,1)S(1)} %get-tuple-element.38), channel_id=1, source_target_pairs={{0,8},{4,12},{8,0},{12,4},{16,24},{20,28},{24,16},{28,20},{1,9},{5... | collective-permute-start | bytes 196616 | tf_op jit(solution)/shard_map/ppermute | solution.py:289
  46.9 2.6 %collective-permute-start.13 = (bf16[2,128,128]{2,1,0:T(8,128)(2,1)S(1)}, bf16[2,128,128]{2,1,0:T(8,128)(2,1)S(1)}, u32[]{:S(2)}, u32[]{:S(2)}) collective-permute-start(bf16[2,128,128]{2,1,0:T(8,128)(2,1)S(1)} %get-tuple-element.39), channel_id=1, source_target_pairs={{0,16},{4,20},{8,24},{12,28},{16,0},{20,4},{24,8},{28,12},{1,17},{... | collective-permute-start | bytes 196616 | tf_op jit(solution)/shard_map/ppermute | solution.py:289
  49.5 0.2 collective-permute-start.14
  49.8 1.5 %shard_map.93 = (bf16[2,128,128]{2,1,0:T(8,128)(2,1)S(1)}, bf16[2,128,128]{2,1,0:T(8,128)(2,1)S(1)}, bf16[2,128,128]{2,1,0:T(8,128)(2,1)S(1)}, bf16[2,128,128]{2,1,0:T(8,128)(2,1)S(1)}) custom-call(bf16[256,128]{1,0:T(8,128)(2,1)S(1)} %get-tuple-element.25.refs_0_, bf16[256,128]{1,0:T(8,128)(2,1)S(1)} %collective-permute-done.refs_1_, ...), custom_call_target="tpu_custom_call" | custom-call | flops 134217728 | bytes 1048576 | tf_op jit(solution)/shard_map/pallas_call | solution.py:374
  51.2 0.7 %collective-permute-start.4 = (bf16[2,128,128]{2,1,0:T(8,128)(2,1)S(1)}, bf16[2,128,128]{2,1,0:T(8,128)(2,1)S(1)}, u32[]{:S(2)}, u32[]{:S(2)}) collective-permute-start(bf16[2,128,128]{2,1,0:T(8,128)(2,1)S(1)} %get-tuple-element.30), channel_id=1, source_target_pairs={{0,8},{4,12},{8,0},{12,4},{16,24},{20,28},{24,16},{28,20},{1,9},{5... | collective-permute-start | bytes 196616 | tf_op jit(solution)/shard_map/ppermute | solution.py:289
  52.0 2.6 %collective-permute-done.13.refs_2_ = bf16[2,128,128]{2,1,0:T(8,128)(2,1)S(1)} collective-permute-done((bf16[2,128,128]{2,1,0:T(8,128)(2,1)S(1)}, bf16[2,128,128]{2,1,0:T(8,128)(2,1)S(1)}, u32[]{:S(2)}, u32[]{:S(2)}) %collective-permute-start.13) | collective-permute-done | bytes 65568 | tf_op jit(solution)/shard_map/ppermute | solution.py:289
  54.5 0.9 %collective-permute-start.5 = (bf16[2,128,128]{2,1,0:T(8,128)(2,1)S(1)}, bf16[2,128,128]{2,1,0:T(8,128)(2,1)S(1)}, u32[]{:S(2)}, u32[]{:S(2)}) collective-permute-start(bf16[2,128,128]{2,1,0:T(8,128)(2,1)S(1)} %get-tuple-element.31), channel_id=1, source_target_pairs={{0,16},{4,20},{8,24},{12,28},{16,0},{20,4},{24,8},{28,12},{1,17},{... | collective-permute-start | bytes 196616 | tf_op jit(solution)/shard_map/ppermute | solution.py:289
  55.5 0.7 %collective-permute-done.14.refs_3_ = bf16[2,128,128]{2,1,0:T(8,128)(2,1)S(1)} collective-permute-done((bf16[2,128,128]{2,1,0:T(8,128)(2,1)S(1)}, bf16[2,128,128]{2,1,0:T(8,128)(2,1)S(1)}, u32[]{:S(2)}, u32[]{:S(2)}) %collective-permute-start.14) | collective-permute-done | bytes 65568 | tf_op jit(solution)/shard_map/ppermute | solution.py:289
  56.2 1.4 %collective-permute-start.6 = (bf16[2,128,128]{2,1,0:T(8,128)(2,1)S(1)}, bf16[2,128,128]{2,1,0:T(8,128)(2,1)S(1)}, u32[]{:S(2)}, u32[]{:S(2)}) collective-permute-start(bf16[2,128,128]{2,1,0:T(8,128)(2,1)S(1)} %get-tuple-element.32), channel_id=1, source_target_pairs={{0,24},{4,28},{8,16},{12,20},{16,8},{20,12},{24,0},{28,4},{1,25},{... | collective-permute-start | bytes 196616 | tf_op jit(solution)/shard_map/ppermute | solution.py:289
  57.6 0.1 collective-permute-start.15
  57.7 3.0 %collective-permute-done.5.refs_2_ = bf16[2,128,128]{2,1,0:T(8,128)(2,1)S(1)} collective-permute-done((bf16[2,128,128]{2,1,0:T(8,128)(2,1)S(1)}, bf16[2,128,128]{2,1,0:T(8,128)(2,1)S(1)}, u32[]{:S(2)}, u32[]{:S(2)}) %collective-permute-start.5) | collective-permute-done | bytes 65568 | tf_op jit(solution)/shard_map/ppermute | solution.py:289
  60.7 1.7 %collective-permute-done.6.refs_3_ = bf16[2,128,128]{2,1,0:T(8,128)(2,1)S(1)} collective-permute-done((bf16[2,128,128]{2,1,0:T(8,128)(2,1)S(1)}, bf16[2,128,128]{2,1,0:T(8,128)(2,1)S(1)}, u32[]{:S(2)}, u32[]{:S(2)}) %collective-permute-start.6) | collective-permute-done | bytes 65568 | tf_op jit(solution)/shard_map/ppermute | solution.py:289
  62.4 0.1 collective-permute-start.7
  62.5 0.8 %shard_map.98 = (f32[4,256,256]{2,1,0:T(8,128)S(1)}, f32[256,2048]{1,0:T(8,128)S(1)}) custom-call(bf16[2,128,128]{2,1,0:T(8,128)(2,1)S(1)} %get-tuple-element.37.refs_0_, bf16[2,128,128]{2,1,0:T(8,128)(2,1)S(1)} %collective-permute-done.12.refs_1_, bf16[2,128,128]{2,1,0:T(8,128)(2,1)S(1)} %collective-permute-done.13.refs_2_, ...), custom_call_target="tpu_custom_call" | custom-call | flops 134217728 | bytes 3145728 | tf_op jit(solution)/shard_map/pallas_call | solution.py:393
  63.3 0.5 collective-permute-done.7.refs_4_
  63.8 2.7 %shard_map.100 = bf16[256,2048]{1,0:T(8,128)(2,1)} custom-call(bf16[2,128,128]{2,1,0:T(8,128)(2,1)S(1)} %get-tuple-element.29.refs_0_, bf16[2,128,128]{2,1,0:T(8,128)(2,1)S(1)} %collective-permute-done.4.refs_1_, bf16[2,128,128]{2,1,0:T(8,128)(2,1)S(1)} %collective-permute-done.5.refs_2_, bf16[2,128,128]{2,1,0:T(8,128)(2,1)S(1)} %collective-permute-done.6.refs_3_, ...), custom_call_target="tpu_custom_call" | custom-call | flops 1073741824 | bytes 4194304 | tf_op jit(solution)/shard_map/pallas_call | solution.py:403
  (32 shorter events, 0.2 us)
Async XLA Ops:
  0.0 43.8 %copy-start.1 = (f32[2,256,8]{2,1,0:T(8,128)S(1)}, f32[2,256,8]{2,1,0:T(8,128)}, u32[]{:S(2)}) copy-start(f32[2,256,8]{2,1,0:T(8,128)} %constant.13.clone.refs_6_) | copy-start | bytes 49156
  0.0 43.8 %copy-start.2 = (bf16[256,512]{1,0:T(8,128)(2,1)S(1)}, bf16[256,512]{1,0:T(8,128)(2,1)}, u32[]{:S(2)}) copy-start(bf16[256,512]{1,0:T(8,128)(2,1)} %constant.12.clone.refs_5_) | copy-start | bytes 786436
  1.9 10.2 %collective-permute-start.16 = (bf16[128,2048]{1,0:T(8,128)(2,1)S(1)}, bf16[128,2048]{1,0:T(8,128)(2,1)S(1)}, u32[]{:S(2)}, u32[]{:S(2)}) collective-permute-start(bf16[128,2048]{1,0:T(8,128)(2,1)S(1)} %get-tuple-element.43.first.refs_9_), channel_id=1, source_target_pairs={{0,1},{1,0},{2,3},{3,2},{4,6},{5,7},{6,4},{7,5},{8,9},{9,8},{10,11... | collective-permute-start | bytes 1572872 | tf_op jit(solution)/shard_map/ppermute | solution.py:298
  12.2 50.3 %copy-start = (bf16[1,256,2048]{2,1,0:T(8,128)(2,1)S(1)}, bf16[1,256,2048]{2,1,0:T(8,128)(2,1)}, u32[]{:S(2)}) copy-start(bf16[1,256,2048]{2,1,0:T(8,128)(2,1)} %param.10) | copy-start | bytes 3145732
  12.2 50.3 %copy-start.5 = (bf16[128,256]{1,0:T(8,128)(2,1)S(1)}, bf16[128,256]{1,0:T(8,128)(2,1)}, u32[]{:S(2)}) copy-start(bf16[128,256]{1,0:T(8,128)(2,1)} %constant.15.clone.refs_6_) | copy-start | bytes 196612
  12.2 50.3 %copy-start.6 = (bf16[128,256]{1,0:T(8,128)(2,1)S(1)}, bf16[128,256]{1,0:T(8,128)(2,1)}, u32[]{:S(2)}) copy-start(bf16[128,256]{1,0:T(8,128)(2,1)} %constant.14.clone.refs_5_) | copy-start | bytes 196612
  12.2 14.9 %collective-permute-start.17 = (bf16[2,128,2048]{2,1,0:T(8,128)(2,1)S(1)}, bf16[2,128,2048]{2,1,0:T(8,128)(2,1)S(1)}, u32[]{:S(2)}, u32[]{:S(2)}) collective-permute-start(bf16[2,128,2048]{2,1,0:T(8,128)(2,1)S(1)} %shard_map.99), channel_id=1, source_target_pairs={{0,2},{1,3},{2,0},{3,1},{4,5},{5,4},{6,7},{7,6},{8,10},{9,11},{10,... | collective-permute-start | bytes 3145736 | tf_op jit(solution)/shard_map/ppermute | solution.py:298
  27.1 36.7 %collective-permute-start.19 = (bf16[2,128,2048]{2,1,0:T(8,128)(2,1)S(1)}, bf16[2,128,2048]{2,1,0:T(8,128)(2,1)S(1)}, u32[]{:S(2)}, u32[]{:S(2)}) collective-permute-start(bf16[2,128,2048]{2,1,0:T(8,128)(2,1)S(1)} %collective-permute-done.17.refs_12_), channel_id=1, source_target_pairs={{0,4},{4,0},{8,12},{12,8},{16,20},{20,16},{24,28},{28,24},{1,5},{5... | collective-permute-start | bytes 3145736 | tf_op jit(solution)/shard_map/ppermute | solution.py:289
  27.1 5.6 %collective-permute-start.8 = (bf16[256,128]{1,0:T(8,128)(2,1)S(1)}, bf16[256,128]{1,0:T(8,128)(2,1)S(1)}, u32[]{:S(2)}, u32[]{:S(2)}) collective-permute-start(bf16[256,128]{1,0:T(8,128)(2,1)S(1)} %get-tuple-element.34), channel_id=1, source_target_pairs={{0,8},{4,12},{8,0},{12,4},{16,24},{20,28},{24,16},{28,20},{1,9},{5... | collective-permute-start | bytes 196616 | tf_op jit(solution)/shard_map/ppermute | solution.py:289
  29.2 7.1 %collective-permute-start.9 = (bf16[256,128]{1,0:T(8,128)(2,1)S(1)}, bf16[256,128]{1,0:T(8,128)(2,1)S(1)}, u32[]{:S(2)}, u32[]{:S(2)}) collective-permute-start(bf16[256,128]{1,0:T(8,128)(2,1)S(1)} %get-tuple-element.35), channel_id=1, source_target_pairs={{0,16},{4,20},{8,24},{12,28},{16,0},{20,4},{24,8},{28,12},{1,17},{... | collective-permute-start | bytes 196616 | tf_op jit(solution)/shard_map/ppermute | solution.py:289
  31.8 9.0 %collective-permute-start.10 = (bf16[256,128]{1,0:T(8,128)(2,1)S(1)}, bf16[256,128]{1,0:T(8,128)(2,1)S(1)}, u32[]{:S(2)}, u32[]{:S(2)}) collective-permute-start(bf16[256,128]{1,0:T(8,128)(2,1)S(1)} %get-tuple-element.36), channel_id=1, source_target_pairs={{0,24},{4,28},{8,16},{12,20},{16,8},{20,12},{24,0},{28,4},{1,25},{... | collective-permute-start | bytes 196616 | tf_op jit(solution)/shard_map/ppermute | solution.py:289
  31.8 9.1 %collective-permute-start = (bf16[256,128]{1,0:T(8,128)(2,1)S(1)}, bf16[256,128]{1,0:T(8,128)(2,1)S(1)}, u32[]{:S(2)}, u32[]{:S(2)}) collective-permute-start(bf16[256,128]{1,0:T(8,128)(2,1)S(1)} %get-tuple-element.26), channel_id=1, source_target_pairs={{0,8},{4,12},{8,0},{12,4},{16,24},{20,28},{24,16},{28,20},{1,9},{5... | collective-permute-start | bytes 196616 | tf_op jit(solution)/shard_map/ppermute | solution.py:289
  32.7 10.5 %collective-permute-start.1 = (bf16[256,128]{1,0:T(8,128)(2,1)S(1)}, bf16[256,128]{1,0:T(8,128)(2,1)S(1)}, u32[]{:S(2)}, u32[]{:S(2)}) collective-permute-start(bf16[256,128]{1,0:T(8,128)(2,1)S(1)} %get-tuple-element.27), channel_id=1, source_target_pairs={{0,16},{4,20},{8,24},{12,28},{16,0},{20,4},{24,8},{28,12},{1,17},{... | collective-permute-start | bytes 196616 | tf_op jit(solution)/shard_map/ppermute | solution.py:289
  36.2 6.9 %collective-permute-start.2 = (bf16[256,128]{1,0:T(8,128)(2,1)S(1)}, bf16[256,128]{1,0:T(8,128)(2,1)S(1)}, u32[]{:S(2)}, u32[]{:S(2)}) collective-permute-start(bf16[256,128]{1,0:T(8,128)(2,1)S(1)} %get-tuple-element.28), channel_id=1, source_target_pairs={{0,24},{4,28},{8,16},{12,20},{16,8},{20,12},{24,0},{28,4},{1,25},{... | collective-permute-start | bytes 196616 | tf_op jit(solution)/shard_map/ppermute | solution.py:289
  40.7 3.1 %collective-permute-start.11 = (bf16[4,256,128]{2,1,0:T(8,128)(2,1)S(1)}, bf16[4,256,128]{2,1,0:T(8,128)(2,1)S(1)}, u32[]{:S(2)}, u32[]{:S(2)}) collective-permute-start(bf16[4,256,128]{2,1,0:T(8,128)(2,1)S(1)} %shard_map.95), channel_id=1, source_target_pairs={{0,4},{4,0},{8,12},{12,8},{16,20},{20,16},{24,28},{28,24},{1,5},{5... | collective-permute-start | bytes 786440 | tf_op jit(solution)/shard_map/ppermute | solution.py:289
  43.2 20.6 %copy-start.3 = (bf16[128,256]{1,0:T(8,128)(2,1)S(1)}, bf16[128,256]{1,0:T(8,128)(2,1)}, u32[]{:S(2)}) copy-start(bf16[128,256]{1,0:T(8,128)(2,1)} %constant.17.clone.refs_6_) | copy-start | bytes 196612
  43.2 20.6 %copy-start.4 = (bf16[128,256]{1,0:T(8,128)(2,1)S(1)}, bf16[128,256]{1,0:T(8,128)(2,1)}, u32[]{:S(2)}) copy-start(bf16[128,256]{1,0:T(8,128)(2,1)} %constant.16.clone.refs_5_) | copy-start | bytes 196612
  43.2 6.3 %collective-permute-start.3 = (bf16[4,256,128]{2,1,0:T(8,128)(2,1)S(1)}, bf16[4,256,128]{2,1,0:T(8,128)(2,1)S(1)}, u32[]{:S(2)}, u32[]{:S(2)}) collective-permute-start(bf16[4,256,128]{2,1,0:T(8,128)(2,1)S(1)} %shard_map.92), channel_id=1, source_target_pairs={{0,4},{4,0},{8,12},{12,8},{16,20},{20,16},{24,28},{28,24},{1,5},{5... | collective-permute-start | bytes 786440 | tf_op jit(solution)/shard_map/ppermute | solution.py:289
  43.3 20.5 %collective-permute-start.18 = (bf16[128,2048]{1,0:T(8,128)(2,1)S(1)}, bf16[128,2048]{1,0:T(8,128)(2,1)S(1)}, u32[]{:S(2)}, u32[]{:S(2)}) collective-permute-start(bf16[128,2048]{1,0:T(8,128)(2,1)S(1)} %collective-permute-done.16.second.refs_11_), channel_id=1, source_target_pairs={{0,4},{4,0},{8,12},{12,8},{16,20},{20,16},{24,28},{28,24},{1,5},{5... | collective-permute-start | bytes 1572872 | tf_op jit(solution)/shard_map/ppermute | solution.py:289
  45.3 5.9 %collective-permute-start.12 = (bf16[2,128,128]{2,1,0:T(8,128)(2,1)S(1)}, bf16[2,128,128]{2,1,0:T(8,128)(2,1)S(1)}, u32[]{:S(2)}, u32[]{:S(2)}) collective-permute-start(bf16[2,128,128]{2,1,0:T(8,128)(2,1)S(1)} %get-tuple-element.38), channel_id=1, source_target_pairs={{0,8},{4,12},{8,0},{12,4},{16,24},{20,28},{24,16},{28,20},{1,9},{5... | collective-permute-start | bytes 196616 | tf_op jit(solution)/shard_map/ppermute | solution.py:289
  46.9 7.6 %collective-permute-start.13 = (bf16[2,128,128]{2,1,0:T(8,128)(2,1)S(1)}, bf16[2,128,128]{2,1,0:T(8,128)(2,1)S(1)}, u32[]{:S(2)}, u32[]{:S(2)}) collective-permute-start(bf16[2,128,128]{2,1,0:T(8,128)(2,1)S(1)} %get-tuple-element.39), channel_id=1, source_target_pairs={{0,16},{4,20},{8,24},{12,28},{16,0},{20,4},{24,8},{28,12},{1,17},{... | collective-permute-start | bytes 196616 | tf_op jit(solution)/shard_map/ppermute | solution.py:289
  49.5 6.7 %collective-permute-start.14 = (bf16[2,128,128]{2,1,0:T(8,128)(2,1)S(1)}, bf16[2,128,128]{2,1,0:T(8,128)(2,1)S(1)}, u32[]{:S(2)}, u32[]{:S(2)}) collective-permute-start(bf16[2,128,128]{2,1,0:T(8,128)(2,1)S(1)} %get-tuple-element.40), channel_id=1, source_target_pairs={{0,24},{4,28},{8,16},{12,20},{16,8},{20,12},{24,0},{28,4},{1,25},{... | collective-permute-start | bytes 196616 | tf_op jit(solution)/shard_map/ppermute | solution.py:289
  51.2 6.3 %collective-permute-start.4 = (bf16[2,128,128]{2,1,0:T(8,128)(2,1)S(1)}, bf16[2,128,128]{2,1,0:T(8,128)(2,1)S(1)}, u32[]{:S(2)}, u32[]{:S(2)}) collective-permute-start(bf16[2,128,128]{2,1,0:T(8,128)(2,1)S(1)} %get-tuple-element.30), channel_id=1, source_target_pairs={{0,8},{4,12},{8,0},{12,4},{16,24},{20,28},{24,16},{28,20},{1,9},{5... | collective-permute-start | bytes 196616 | tf_op jit(solution)/shard_map/ppermute | solution.py:289
  54.5 6.1 %collective-permute-start.5 = (bf16[2,128,128]{2,1,0:T(8,128)(2,1)S(1)}, bf16[2,128,128]{2,1,0:T(8,128)(2,1)S(1)}, u32[]{:S(2)}, u32[]{:S(2)}) collective-permute-start(bf16[2,128,128]{2,1,0:T(8,128)(2,1)S(1)} %get-tuple-element.31), channel_id=1, source_target_pairs={{0,16},{4,20},{8,24},{12,28},{16,0},{20,4},{24,8},{28,12},{1,17},{... | collective-permute-start | bytes 196616 | tf_op jit(solution)/shard_map/ppermute | solution.py:289
  56.2 6.2 %collective-permute-start.6 = (bf16[2,128,128]{2,1,0:T(8,128)(2,1)S(1)}, bf16[2,128,128]{2,1,0:T(8,128)(2,1)S(1)}, u32[]{:S(2)}, u32[]{:S(2)}) collective-permute-start(bf16[2,128,128]{2,1,0:T(8,128)(2,1)S(1)} %get-tuple-element.32), channel_id=1, source_target_pairs={{0,24},{4,28},{8,16},{12,20},{16,8},{20,12},{24,0},{28,4},{1,25},{... | collective-permute-start | bytes 196616 | tf_op jit(solution)/shard_map/ppermute | solution.py:289
  57.6 4.9 %collective-permute-start.15 = (bf16[4,128,128]{2,1,0:T(8,128)(2,1)S(1)}, bf16[4,128,128]{2,1,0:T(8,128)(2,1)S(1)}, u32[]{:S(2)}, u32[]{:S(2)}) collective-permute-start(bf16[4,128,128]{2,1,0:T(8,128)(2,1)S(1)} %shard_map.97), channel_id=1, source_target_pairs={{0,4},{4,0},{8,12},{12,8},{16,20},{20,16},{24,28},{28,24},{1,5},{5... | collective-permute-start | bytes 393224 | tf_op jit(solution)/shard_map/ppermute | solution.py:289
  62.4 1.4 %collective-permute-start.7 = (bf16[4,128,128]{2,1,0:T(8,128)(2,1)S(1)}, bf16[4,128,128]{2,1,0:T(8,128)(2,1)S(1)}, u32[]{:S(2)}, u32[]{:S(2)}) collective-permute-start(bf16[4,128,128]{2,1,0:T(8,128)(2,1)S(1)} %shard_map.94), channel_id=1, source_target_pairs={{0,4},{4,0},{8,12},{12,8},{16,20},{20,16},{24,28},{28,24},{1,5},{5... | collective-permute-start | bytes 393224 | tf_op jit(solution)/shard_map/ppermute | solution.py:289

commit v4 on v3

--- a/solution.py
+++ b/solution.py
@@ -88,11 +88,13 @@
     src = lax.broadcasted_iota(jnp.int32, (GROUP, CHUNKS * lanes), 0)
     column = lax.broadcasted_iota(jnp.int32, (GROUP, CHUNKS * lanes), 1)
     lane, j = column % lanes, column % lanes - pairs
+    choose = None
     for zs in order:
-        part = ((chip ^ zs) % chips_per_group) * CHUNKS + column // lanes
-        mirrored = jnp.where((j == 0) & (part == 0), GROUP // 2, GROUP - pairs * part - j)
-        wanted = jnp.where(lane < pairs, pairs * part + lane, mirrored)
-        choose = (src == wanted).astype(jnp.bfloat16)
+        if choose is None or chips_per_group > 1:
+            part = ((chip ^ zs) % chips_per_group) * CHUNKS + column // lanes
+            mirrored = jnp.where((j == 0) & (part == 0), GROUP // 2, GROUP - pairs * part - j)
+            wanted = jnp.where(lane < pairs, pairs * part + lane, mirrored)
+            choose = (src == wanted).astype(jnp.bfloat16)
         loads[zs].wait()
         got = jnp.dot(tokens[zs], choose, preferred_element_type=jnp.float32).astype(jnp.bfloat16)
         for q in range(CHUNKS):
@@ -130,8 +132,8 @@
 def position_kernel(rows, q, *refs):
     chips = rows // 2
     mine, theirs = refs[:chips], refs[chips]
-    table, twist = refs[chips + 1 : chips + 3]
-    *outs, folded, turned_z, spect = refs[chips + 3 :]
+    table_hi, table_lo, twist = refs[chips + 1 : chips + 4]
+    *outs, folded, turned_z, spect = refs[chips + 4 :]
     inner, lanes = mine[0].shape
     pairs = lanes // 2
     row = lax.axis_index("row")
@@ -147,29 +149,29 @@
     other = jnp.where(lone_low | lone_high, 0.0, 1.0).astype(jnp.float32)
     cosine = (lane < pairs) | lone_high
 
-    def fold(block):
-        value = block.astype(jnp.float32)
-        if lanes % 128 == 0:
-            turned = pltpu.roll(value, pairs, 1)
-        else:
-            turned = jnp.concatenate([value[:, pairs:], value[:, :pairs]], axis=1)
-        return value * own + turned * other
-
-    for zs in range(chips):
-        folded[row ^ (2 * zs)] = fold(mine[zs][...])
-        folded[row ^ (2 * zs + 1)] = fold(theirs[zs])
-
     odd_core = core == 1
     sign = jnp.where(odd_core, -1.0, 1.0).astype(jnp.float32)
+    upper = row >= half
+    near, far = jnp.where(upper, sign, 1.0), jnp.where(upper, 1.0, sign)
+
+    def block(s):
+        value = mine[s // 2][...] if s % 2 == 0 else theirs[s // 2]
+        return value.astype(jnp.float32)
+
+    for s in range(half):
+        value = near * block(s) + far * block(s ^ half)
+        if lanes % 128 == 0:
+            rolled = pltpu.roll(value, pairs, 1)
+        else:
+            rolled = jnp.concatenate([value[:, pairs:], value[:, :pairs]], axis=1)
+        folded[(row % half) ^ s] = value * own + rolled * other
+
     turns = []
     for n in range(half):
         angle = 2 * math.pi * n / rows
-        turns.append(
-            (
-                jnp.where(odd_core, math.cos(angle), 1.0).astype(jnp.float32),
-                jnp.where(odd_core, -math.sin(angle), 0.0).astype(jnp.float32),
-            )
-        )
+        c = jnp.where(odd_core, math.cos(angle), 1.0).astype(jnp.float32)
+        d = jnp.where(odd_core, math.sin(angle), 0.0).astype(jnp.float32)
+        turns.append((jnp.where(cosine, c, d), jnp.where(cosine, -d, c)))
     tile = min(inner, 32)
 
     def step(i, carry):
@@ -177,22 +179,22 @@
         low_at = pl.ds(pl.multiple_of(inner + i * tile, tile), tile)
         values = []
         for n in range(half):
-            v = folded[n, at, :] + sign * folded[n + half, at, :]
+            v = folded[n, at, :]
             values.append((v * turns[n][0], v * turns[n][1]))
         tw = twist[core, at, :]
-        for j, (re, im) in enumerate(complex_dft(values)):
-            a = jnp.where(cosine, re, -im)
-            b = jnp.where(cosine, im, re)
+        for j, (a, b) in enumerate(complex_dft(values)):
             c, s = tw[:, j : j + 1], tw[:, half + j : half + j + 1]
-            for where, z in ((at, a * c + b * s), (low_at, b * c - a * s)):
-                turned_z[where, j * lanes : (j + 1) * lanes] = z.astype(jnp.bfloat16)
+            cols = slice(j * lanes, (j + 1) * lanes)
+            turned_z[at, cols] = (a * c + b * s).astype(jnp.bfloat16)
+            turned_z[low_at, cols] = (b * c - a * s).astype(jnp.bfloat16)
         return carry
 
     lax.fori_loop(0, inner // tile, step, 0)
     width = min(half * lanes, 256)
     for start in range(0, half * lanes, width):
         cols = slice(start, start + width)
-        value = jnp.dot(table[...], turned_z[:, cols], preferred_element_type=jnp.float32)
+        value = jnp.dot(table_hi[...], turned_z[:, cols], preferred_element_type=jnp.float32)
+        value += jnp.dot(table_lo[...], turned_z[:, cols], preferred_element_type=jnp.float32)
         for j in range(start // lanes, (start + width) // lanes):
             piece = value[:, j * lanes - start : (j + 1) * lanes - start]
             spect[j] = piece
@@ -202,7 +204,11 @@
             dest = row ^ (2 * zs + rel)
             for j in range(half):
                 piece = spect[j, pl.ds(pl.multiple_of(dest * per, per), per), :]
-                outs[zs][rel, j * per : (j + 1) * per, :] = piece.astype(jnp.bfloat16)
+                lines = slice(j * per, (j + 1) * per)
+                if q == 0:
+                    outs[zs][rel, lines, :] = piece.astype(jnp.bfloat16)
+                else:
+                    outs[rel][zs, lines, :] = piece.astype(jnp.bfloat16)
 
 
 def order_rows(rows, count):
@@ -220,9 +226,10 @@
         out[zs] = ref[1]
 
 
-def join_kernel(first, second, out):
-    out[0] = first[...]
-    out[1] = second[...]
+def join_kernel(keep, got, *outs):
+    for zs, out in enumerate(outs):
+        out[0] = keep[zs]
+        out[1] = got[zs]
 
 
 def channel_part(order, pieces, feat_hi, feat_lo):
@@ -252,31 +259,31 @@
 
 def final_kernel(rows, *refs):
     chips = rows // 2
-    mine, theirs, feat_hi, feat_lo, spect, opened = refs[:chips], *refs[chips : chips + 5]
-    w_mine, w_rest, w_a, w_b, v_a, v_b, out_ref, lhs, result, sems = refs[chips + 5 :]
+    mine, feat_hi, feat_lo, spect, opened = refs[:chips], *refs[chips : chips + 4]
+    w_mine, w_rest, w_a, w_b, w_c, v_a, v_b, v_c, out_ref, lhs, result, sems = refs[chips + 4 :]
     count, width = opened.shape
     half = GROUP // 2
     row, col = lax.axis_index("row"), lax.axis_index("col")
     core, chip = row % 2, row // 2
     order = order_rows(rows, count)
-    pieces = [(ref[0], theirs[zs]) for zs, ref in enumerate(mine)]
+    pieces = [(ref[0], ref[1]) for ref in mine]
     for zs, part in enumerate(channel_part(order, pieces, feat_hi[...], feat_lo[...])):
         whole = (part + spect[zs]).astype(jnp.bfloat16)
         for h in range(2):
             spot = pl.ds(pl.multiple_of((core ^ h) * half, half), half)
             lhs[zs, :, spot] = whole[:, h * half : (h + 1) * half]
     weights = (
-        (0, lambda at: (w_mine[:, at], w_rest[:, at])),
-        (1 + core, lambda at: (w_a[:, at], v_b[0, :, at])),
-        (2 - core, lambda at: (w_b[0, :, at], v_a[:, at])),
-        (3, lambda at: (w_b[1, :, at], v_b[1, :, at])),
+        (0, w_mine, w_rest),
+        (1 + core, w_a, v_b),
+        (2 - core, w_b, v_a),
+        (3, w_c, v_c),
     )
     copies = []
     for t in range(width // GROUP):
         cols = slice(t * GROUP, (t + 1) * GROUP)
         total = jnp.zeros((count, GROUP), jnp.float32)
-        for s, halves in weights:
-            rhs = jnp.concatenate(halves(cols), axis=0)
+        for s, w_here, w_there in weights:
+            rhs = jnp.concatenate([w_here[:, cols], w_there[:, cols]], axis=0)
             total += jnp.dot(lhs[chip ^ col ^ s], rhs, preferred_element_type=jnp.float32)
         result[:, cols] = (opened[:, cols] * total).astype(jnp.bfloat16)
         copies.append(pltpu.make_async_copy(result.at[:, cols], out_ref.at[:, cols], sems.at[t]))
@@ -322,7 +329,7 @@
     half = rows // 2
     width = w_proj.shape[1]
     scale = 1.0 / math.sqrt(count * rows * GROUP)
-    table = position_table(count, scale).astype(jnp.bfloat16)
+    table_hi, table_lo = split_halves(position_table(count, scale))
     twist = twist_table(rows, count)
     features_of = feature_table(lanes // 2)
     feat_hi, feat_lo = split_halves(features_of)
@@ -351,44 +358,42 @@
     if fast:
         mine, rest = picked[CHUNKS * chips :]
         w_a = turn_swap(mine, rows, n_col, (1, 2))
-        pair = vmem_call(
-            join_kernel,
-            jax.ShapeDtypeStruct((2, GROUP // 2, width), bf),
-            [],
-            GROUP * width,
-            4 * GROUP * width,
-        )(mine, w_a)
-        w_b = turn_swap(pair, rows, n_col, (2, 1))
-        v_a = swap(w_a, "row", rows, 1)
-        v_b = swap(w_b, "row", rows, 1)
+        w_b = turn_swap(mine, rows, n_col, (2, 1))
+        w_c = turn_swap(w_a, rows, n_col, (2, 1))
+        others = []
+        for own in (w_a, w_b, w_c):
+            others.append(swap(own, "row", rows, 1))
 
     lines = half * (count // rows)
     piece = jax.ShapeDtypeStruct((2, lines, lanes), bf)
     small = (count * features // 4, count * features)
-    received = []
+    stacked = jax.ShapeDtypeStruct((chips, lines, lanes), bf)
+    sent = []
     for q in range(CHUNKS):
         stack = vmem_call(
             stack_kernel, jax.ShapeDtypeStruct((chips, count, lanes), bf), [], *small
         )(*arrived[q])
         theirs = swap(stack, "row", rows, 1)
-        sent = vmem_call(
-            functools.partial(position_kernel, rows, q),
-            [piece] * chips,
-            [
-                pltpu.VMEM((rows, count, lanes), jnp.float32),
-                pltpu.VMEM((2 * count, half * lanes), bf),
-                pltpu.VMEM((half, count, lanes), jnp.float32),
-            ],
-            4 * count * count * half * lanes,
-            rows * count * lanes * 4,
-        )(*arrived[q], theirs, table, twist)
-        got = across_chips(sent, rows)
-        give = vmem_call(
-            give_kernel, jax.ShapeDtypeStruct((chips, lines, lanes), bf), [], *small
-        )(*got)
-        got.append(swap(give, "row", rows, 1))
-        received.append(got)
-    early, late = received
+        sent.append(
+            vmem_call(
+                functools.partial(position_kernel, rows, q),
+                [piece] * chips if q == 0 else [stacked] * 2,
+                [
+                    pltpu.VMEM((half, count, lanes), jnp.float32),
+                    pltpu.VMEM((2 * count, half * lanes), bf),
+                    pltpu.VMEM((half, count, lanes), jnp.float32),
+                ],
+                8 * count * count * half * lanes,
+                rows * count * lanes * 4,
+            )(*arrived[q], theirs, table_hi, table_lo, twist)
+        )
+    early = across_chips(sent[0], rows)
+    give = vmem_call(give_kernel, stacked, [], *small)(*early)
+    early.append(swap(give, "row", rows, 1))
+    keep, give = sent[1]
+    got = swap(give, "row", rows, 1)
+    joined = vmem_call(join_kernel, [piece] * chips, [], *small)(keep, got)
+    late = across_chips(joined, rows)
     if fast:
         spect, opened = vmem_call(
             functools.partial(prepare_kernel, rows),
@@ -403,7 +408,7 @@
         return pl.pallas_call(
             functools.partial(final_kernel, rows),
             out_shape=jax.ShapeDtypeStruct((count, width), bf),
-            in_specs=[pl.BlockSpec(memory_space=pltpu.VMEM)] * (chips + 11),
+            in_specs=[pl.BlockSpec(memory_space=pltpu.VMEM)] * (chips + 12),
             out_specs=pl.BlockSpec(memory_space=pl.ANY),
             scratch_shapes=[
                 pltpu.VMEM((chips, count, GROUP), bf),
@@ -416,7 +421,7 @@
                 bytes_accessed=2 * features * width,
                 transcendentals=0,
             ),
-        )(*late, feat_hi[1], feat_lo[1], spect, opened, mine, rest, w_a, w_b, v_a, v_b)
+        )(*late, feat_hi[1], feat_lo[1], spect, opened, mine, rest, w_a, w_b, w_c, *others)
 
     weights = lax.all_gather(w_proj, "col", axis=0, tiled=True).reshape(-1, GROUP, width)
     order = order_rows(rows, count)
@@ -426,7 +431,10 @@
     spectrum = jnp.zeros((count, weights.shape[0], GROUP), jnp.float32)
     here = chip ^ jnp.arange(chips)
     for q in range(CHUNKS):
-        parts = [(received[q][zs][0], received[q][chips][zs]) for zs in range(chips)]
+        if q == 0:
+            parts = [(early[zs][0], early[chips][zs]) for zs in range(chips)]
+        else:
+            parts = [(ref[0], ref[1]) for ref in late]
         got = jnp.stack([jnp.concatenate(pair, axis=0) for pair in parts])[here]
         got = jnp.einsum("kr,zrl->kzl", order, got, preferred_element_type=jnp.float32)
         spectrum += jnp.einsum(

time: 66.6 us -> 66.1 us (level)
  starting transfers between devices: 26.9 us -> 24 us
  waiting for transfers between devices: 30.9 us -> 33.1 us
    ppermute x18 -> x19, waiting for transfers between devices: 11 us -> 22.4 us  [swap(): return lax.ppermute(value, axis, [(i, i ^ bit) for i in range(size)])]
    ppermute x2 -> x3, waiting for transfers between devices: 19.9 us -> 10.7 us  [turn_swap(): return lax.ppermute(value, ('row', 'col'), turn)]
    ppermute x18 -> x19, starting transfers between devices: 21.8 us -> 17.9 us  [swap(): return lax.ppermute(value, axis, [(i, i ^ bit) for i in range(size)])]
    ppermute x2 -> x3, starting transfers between devices: 5.14 us -> 6.12 us  [turn_swap(): return lax.ppermute(value, ('row', 'col'), turn)]
    pallas_call x5 -> x4, Pallas kernels: 3.04 us -> 3.23 us  [the longest x2 3.2 us: program(): vmem_call(functools.partial(position_kernel, rows, q), [piece] * chips if...]
  transfers between devices with their start and end apart: 20 -> 22, of which waited for: 9 -> 9; matrix products, arithmetic and copies ran while one was open for 0% -> 0% of each run, Pallas kernels for 6% -> 6%
where the time goes in v4:
time: 66.1 us; the launch traced here: 65.9 us
  waiting for transfers between devices  33.1 us (50%)
  starting transfers between devices  24 us (36%)
  Pallas kernels  8.61 us (13%)
    ppermute x19, waiting for transfers between devices, swap(): return lax.ppermute(value, axis, [(i, i ^ bit) for i in range(size)])  22.4 us
    ppermute x19, starting transfers between devices, swap(): return lax.ppermute(value, axis, [(i, i ^ bit) for i in range(size)])  17.9 us
    ppermute x3, waiting for transfers between devices, turn_swap(): return lax.ppermute(value, ('row', 'col'), turn)  10.7 us
    ppermute x3, starting transfers between devices, turn_swap(): return lax.ppermute(value, ('row', 'col'), turn)  6.12 us
    pallas_call x2, Pallas kernels, program(): vmem_call(functools.partial(position_kernel, rows, q), [piece] * chips if...  3.2 us
    pallas_call x1, Pallas kernels, program(): pl.pallas_call(functools.partial(final_kernel, rows), out_shape=jax.Shape...  2.67 us
    pallas_call x1, Pallas kernels, program(): pl.pallas_call(functools.partial(pick_kernel, chips, fast), out_shape=[ja...  1.9 us
  transfers between devices with their start and end apart: 22, of which 9 were waited for; matrix products, arithmetic and copies ran while one was open for 0% of the time, Pallas kernels for 6%

profile of v4, /device:TPU:0, one launch (start us, length us, event | category | flops | bytes accessed | tf_op | source)
XLA Modules:
  0.0 65.9 jit_solution(17562993774783399935)
XLA Ops:
  0.0 1.9 %shard_map.100 = (bf16[256,128]{1,0:T(8,128)(2,1)S(1)}, bf16[256,128]{1,0:T(8,128)(2,1)S(1)}, bf16[256,128]{1,0:T(8,128)(2,1)S(1)}, bf16[256,128]{1,0:T(8,128)(2...) custom-call(bf16[256,1024]{1,0:T(8,128)(2,1)} %bitcast.4, ...), custom_call_target="tpu_custom_call" | custom-call | flops 134217728 | bytes 1048576 | tf_op jit(solution)/shard_map/pallas_call | solution.py:340
  1.9 3.0 %collective-permute-start.16 = (bf16[128,2048]{1,0:T(8,128)(2,1)S(1)}, bf16[128,2048]{1,0:T(8,128)(2,1)S(1)}, u32[]{:S(2)}, u32[]{:S(2)}) collective-permute-start(bf16[128,2048]{1,0:T(8,128)(2,1)S(1)} %get-tuple-element.47.refs_8_), channel_id=1, source_target_pairs={{0,1},{1,0},{2,3},{3,2},{4,6},{5,7},{6,4},{7,5},{8,9},{9,8},{10,11... | collective-permute-start | bytes 1572872 | tf_op jit(solution)/shard_map/ppermute | solution.py:305
  4.9 1.5 %collective-permute-start.17 = (bf16[128,2048]{1,0:T(8,128)(2,1)S(1)}, bf16[128,2048]{1,0:T(8,128)(2,1)S(1)}, u32[]{:S(2)}, u32[]{:S(2)}) collective-permute-start(bf16[128,2048]{1,0:T(8,128)(2,1)S(1)} %get-tuple-element.47.refs_8_), channel_id=1, source_target_pairs={{0,2},{1,3},{2,0},{3,1},{4,5},{5,4},{6,7},{7,6},{8,10},{9,11},{10,... | collective-permute-start | bytes 1572872 | tf_op jit(solution)/shard_map/ppermute | solution.py:305
  6.5 10.7 %collective-permute-done.16.refs_10_ = bf16[128,2048]{1,0:T(8,128)(2,1)S(1)} collective-permute-done((bf16[128,2048]{1,0:T(8,128)(2,1)S(1)}, bf16[128,2048]{1,0:T(8,128)(2,1)S(1)}, u32[]{:S(2)}, u32[]{:S(2)}) %collective-permute-start.16) | collective-permute-done | bytes 524320 | tf_op jit(solution)/shard_map/ppermute | solution.py:305
  17.2 1.6 %collective-permute-start.18 = (bf16[128,2048]{1,0:T(8,128)(2,1)S(1)}, bf16[128,2048]{1,0:T(8,128)(2,1)S(1)}, u32[]{:S(2)}, u32[]{:S(2)}) collective-permute-start(bf16[128,2048]{1,0:T(8,128)(2,1)S(1)} %collective-permute-done.16.refs_10_), channel_id=1, source_target_pairs={{0,2},{1,3},{2,0},{3,1},{4,5},{5,4},{6,7},{7,6},{8,10},{9,11},{10,... | collective-permute-start | bytes 1572872 | tf_op jit(solution)/shard_map/ppermute | solution.py:305
  18.7 1.7 %collective-permute-start.8 = (bf16[256,128]{1,0:T(8,128)(2,1)S(1)}, bf16[256,128]{1,0:T(8,128)(2,1)S(1)}, u32[]{:S(2)}, u32[]{:S(2)}) collective-permute-start(bf16[256,128]{1,0:T(8,128)(2,1)S(1)} %get-tuple-element.38), channel_id=1, source_target_pairs={{0,8},{4,12},{8,0},{12,4},{16,24},{20,28},{24,16},{28,20},{1,9},{5... | collective-permute-start | bytes 196616 | tf_op jit(solution)/shard_map/ppermute | solution.py:296
  20.4 2.6 %collective-permute-start.9 = (bf16[256,128]{1,0:T(8,128)(2,1)S(1)}, bf16[256,128]{1,0:T(8,128)(2,1)S(1)}, u32[]{:S(2)}, u32[]{:S(2)}) collective-permute-start(bf16[256,128]{1,0:T(8,128)(2,1)S(1)} %get-tuple-element.39), channel_id=1, source_target_pairs={{0,16},{4,20},{8,24},{12,28},{16,0},{20,4},{24,8},{28,12},{1,17},{... | collective-permute-start | bytes 196616 | tf_op jit(solution)/shard_map/ppermute | solution.py:296
  23.0 0.1 collective-permute-start.10
  23.1 2.3 %collective-permute-start = (bf16[256,128]{1,0:T(8,128)(2,1)S(1)}, bf16[256,128]{1,0:T(8,128)(2,1)S(1)}, u32[]{:S(2)}, u32[]{:S(2)}) collective-permute-start(bf16[256,128]{1,0:T(8,128)(2,1)S(1)} %get-tuple-element.28), channel_id=1, source_target_pairs={{0,8},{4,12},{8,0},{12,4},{16,24},{20,28},{24,16},{28,20},{1,9},{5... | collective-permute-start | bytes 196616 | tf_op jit(solution)/shard_map/ppermute | solution.py:296
  25.4 1.9 %collective-permute-done.9.refs_2_ = bf16[256,128]{1,0:T(8,128)(2,1)S(1)} collective-permute-done((bf16[256,128]{1,0:T(8,128)(2,1)S(1)}, bf16[256,128]{1,0:T(8,128)(2,1)S(1)}, u32[]{:S(2)}, u32[]{:S(2)}) %collective-permute-start.9) | collective-permute-done | bytes 65568 | tf_op jit(solution)/shard_map/ppermute | solution.py:296
  27.3 1.9 %collective-permute-start.1 = (bf16[256,128]{1,0:T(8,128)(2,1)S(1)}, bf16[256,128]{1,0:T(8,128)(2,1)S(1)}, u32[]{:S(2)}, u32[]{:S(2)}) collective-permute-start(bf16[256,128]{1,0:T(8,128)(2,1)S(1)} %get-tuple-element.29), channel_id=1, source_target_pairs={{0,16},{4,20},{8,24},{12,28},{16,0},{20,4},{24,8},{28,12},{1,17},{... | collective-permute-start | bytes 196616 | tf_op jit(solution)/shard_map/ppermute | solution.py:296
  29.2 1.3 %collective-permute-start.2 = (bf16[256,128]{1,0:T(8,128)(2,1)S(1)}, bf16[256,128]{1,0:T(8,128)(2,1)S(1)}, u32[]{:S(2)}, u32[]{:S(2)}) collective-permute-start(bf16[256,128]{1,0:T(8,128)(2,1)S(1)} %get-tuple-element.30), channel_id=1, source_target_pairs={{0,24},{4,28},{8,16},{12,20},{16,8},{20,12},{24,0},{28,4},{1,25},{... | collective-permute-start | bytes 196616 | tf_op jit(solution)/shard_map/ppermute | solution.py:296
  30.6 0.1 collective-permute-start.11
  30.6 2.3 %collective-permute-done.1.refs_2_ = bf16[256,128]{1,0:T(8,128)(2,1)S(1)} collective-permute-done((bf16[256,128]{1,0:T(8,128)(2,1)S(1)}, bf16[256,128]{1,0:T(8,128)(2,1)S(1)}, u32[]{:S(2)}, u32[]{:S(2)}) %collective-permute-start.1) | collective-permute-done | bytes 65568 | tf_op jit(solution)/shard_map/ppermute | solution.py:296
  33.0 2.3 %collective-permute-done.2.refs_3_ = bf16[256,128]{1,0:T(8,128)(2,1)S(1)} collective-permute-done((bf16[256,128]{1,0:T(8,128)(2,1)S(1)}, bf16[256,128]{1,0:T(8,128)(2,1)S(1)}, u32[]{:S(2)}, u32[]{:S(2)}) %collective-permute-start.2) | collective-permute-done | bytes 65568 | tf_op jit(solution)/shard_map/ppermute | solution.py:296
  35.4 0.5 collective-permute-start.19
  35.9 0.1 collective-permute-start.20
  36.0 0.4 collective-permute-start.21
  36.4 1.6 %shard_map.105 = (bf16[2,128,128]{2,1,0:T(8,128)(2,1)S(1)}, bf16[2,128,128]{2,1,0:T(8,128)(2,1)S(1)}, bf16[2,128,128]{2,1,0:T(8,128)(2,1)S(1)}, bf16[2,128,128]{2,1,0:T(8,128)(2,1)S(1)}) custom-call(bf16[256,128]{1,0:T(8,128)(2,1)S(1)} %get-tuple-element.37.refs_0_, bf16[256,128]{1,0:T(8,128)(2,1)S(1)} %collective-permute-done.8.refs_1_, ...), custom_call_target="tpu_custom_call" | custom-call | flops 268435456 | bytes 1048576 | tf_op jit(solution)/shard_map/pallas_call | solution.py:378
  38.1 0.1 collective-permute-start.12
  38.2 2.0 %collective-permute-start.13 = (bf16[2,128,128]{2,1,0:T(8,128)(2,1)S(1)}, bf16[2,128,128]{2,1,0:T(8,128)(2,1)S(1)}, u32[]{:S(2)}, u32[]{:S(2)}) collective-permute-start(bf16[2,128,128]{2,1,0:T(8,128)(2,1)S(1)} %get-tuple-element.43), channel_id=1, source_target_pairs={{0,16},{4,20},{8,24},{12,28},{16,0},{20,4},{24,8},{28,12},{1,17},{... | collective-permute-start | bytes 196616 | tf_op jit(solution)/shard_map/ppermute | solution.py:296
  40.1 1.6 %shard_map.102 = (bf16[4,128,128]{2,1,0:T(8,128)(2,1)S(1)}, bf16[4,128,128]{2,1,0:T(8,128)(2,1)S(1)}) custom-call(bf16[256,128]{1,0:T(8,128)(2,1)S(1)} %get-tuple-element.27.refs_0_, bf16[256,128]{1,0:T(8,128)(2,1)S(1)} %collective-permute-done.refs_1_, bf16[256,128]{1,0:T(8,128)(2,1)S(1)} %collective-permute-done.1.refs_2_, ...), custom_call_target="tpu_custom_call" | custom-call | flops 268435456 | bytes 1048576 | tf_op jit(solution)/shard_map/pallas_call | solution.py:378
  41.7 1.7 %collective-permute-done.12.refs_1_ = bf16[2,128,128]{2,1,0:T(8,128)(2,1)S(1)} collective-permute-done((bf16[2,128,128]{2,1,0:T(8,128)(2,1)S(1)}, bf16[2,128,128]{2,1,0:T(8,128)(2,1)S(1)}, u32[]{:S(2)}, u32[]{:S(2)}) %collective-permute-start.12) | collective-permute-done | bytes 65568 | tf_op jit(solution)/shard_map/ppermute | solution.py:296
  43.5 1.3 %collective-permute-done.13.refs_2_ = bf16[2,128,128]{2,1,0:T(8,128)(2,1)S(1)} collective-permute-done((bf16[2,128,128]{2,1,0:T(8,128)(2,1)S(1)}, bf16[2,128,128]{2,1,0:T(8,128)(2,1)S(1)}, u32[]{:S(2)}, u32[]{:S(2)}) %collective-permute-start.13) | collective-permute-done | bytes 65568 | tf_op jit(solution)/shard_map/ppermute | solution.py:296
  44.8 2.0 %collective-permute-start.14 = (bf16[2,128,128]{2,1,0:T(8,128)(2,1)S(1)}, bf16[2,128,128]{2,1,0:T(8,128)(2,1)S(1)}, u32[]{:S(2)}, u32[]{:S(2)}) collective-permute-start(bf16[2,128,128]{2,1,0:T(8,128)(2,1)S(1)} %get-tuple-element.44), channel_id=1, source_target_pairs={{0,24},{4,28},{8,16},{12,20},{16,8},{20,12},{24,0},{28,4},{1,25},{... | collective-permute-start | bytes 196616 | tf_op jit(solution)/shard_map/ppermute | solution.py:296
  46.8 4.0 %collective-permute-done.14.refs_3_ = bf16[2,128,128]{2,1,0:T(8,128)(2,1)S(1)} collective-permute-done((bf16[2,128,128]{2,1,0:T(8,128)(2,1)S(1)}, bf16[2,128,128]{2,1,0:T(8,128)(2,1)S(1)}, u32[]{:S(2)}, u32[]{:S(2)}) %collective-permute-start.14) | collective-permute-done | bytes 65568 | tf_op jit(solution)/shard_map/ppermute | solution.py:296
  51.1 4.5 %collective-permute-done.5.refs_1_ = bf16[2,128,128]{2,1,0:T(8,128)(2,1)S(1)} collective-permute-done((bf16[2,128,128]{2,1,0:T(8,128)(2,1)S(1)}, bf16[2,128,128]{2,1,0:T(8,128)(2,1)S(1)}, u32[]{:S(2)}, u32[]{:S(2)}) %collective-permute-start.5) | collective-permute-done | bytes 65568 | tf_op jit(solution)/shard_map/ppermute | solution.py:296
  55.5 0.8 %collective-permute-start.6 = (bf16[2,128,128]{2,1,0:T(8,128)(2,1)S(1)}, bf16[2,128,128]{2,1,0:T(8,128)(2,1)S(1)}, u32[]{:S(2)}, u32[]{:S(2)}) collective-permute-start(bf16[2,128,128]{2,1,0:T(8,128)(2,1)S(1)} %get-tuple-element.35), channel_id=1, source_target_pairs={{0,16},{4,20},{8,24},{12,28},{16,0},{20,4},{24,8},{28,12},{1,17},{... | collective-permute-start | bytes 196616 | tf_op jit(solution)/shard_map/ppermute | solution.py:296
  56.4 1.8 %collective-permute-start.7 = (bf16[2,128,128]{2,1,0:T(8,128)(2,1)S(1)}, bf16[2,128,128]{2,1,0:T(8,128)(2,1)S(1)}, u32[]{:S(2)}, u32[]{:S(2)}) collective-permute-start(bf16[2,128,128]{2,1,0:T(8,128)(2,1)S(1)} %get-tuple-element.36), channel_id=1, source_target_pairs={{0,24},{4,28},{8,16},{12,20},{16,8},{20,12},{24,0},{28,4},{1,25},{... | collective-permute-start | bytes 196616 | tf_op jit(solution)/shard_map/ppermute | solution.py:296
  58.2 0.8 %shard_map.107 = (f32[4,256,256]{2,1,0:T(8,128)S(1)}, f32[256,2048]{1,0:T(8,128)S(1)}) custom-call(bf16[2,128,128]{2,1,0:T(8,128)(2,1)S(1)} %get-tuple-element.41.refs_0_, bf16[2,128,128]{2,1,0:T(8,128)(2,1)S(1)} %collective-permute-done.12.refs_1_, bf16[2,128,128]{2,1,0:T(8,128)(2,1)S(1)} %collective-permute-done.13.refs_2_, ...), custom_call_target="tpu_custom_call" | custom-call | flops 134217728 | bytes 3145728 | tf_op jit(solution)/shard_map/pallas_call | solution.py:398
  59.0 4.3 %collective-permute-done.6.refs_2_ = bf16[2,128,128]{2,1,0:T(8,128)(2,1)S(1)} collective-permute-done((bf16[2,128,128]{2,1,0:T(8,128)(2,1)S(1)}, bf16[2,128,128]{2,1,0:T(8,128)(2,1)S(1)}, u32[]{:S(2)}, u32[]{:S(2)}) %collective-permute-start.6) | collective-permute-done | bytes 65568 | tf_op jit(solution)/shard_map/ppermute | solution.py:296
  63.3 2.7 %shard_map.108 = bf16[256,2048]{1,0:T(8,128)(2,1)} custom-call(bf16[2,128,128]{2,1,0:T(8,128)(2,1)S(1)} %get-tuple-element.33.refs_0_, bf16[2,128,128]{2,1,0:T(8,128)(2,1)S(1)} %collective-permute-done.5.refs_1_, bf16[2,128,128]{2,1,0:T(8,128)(2,1)S(1)} %collective-permute-done.6.refs_2_, bf16[2,128,128]{2,1,0:T(8,128)(2,1)S(1)} %collective-permute-done.7.refs_3_, ...), custom_call_target="tpu_custom_call" | custom-call | flops 1073741824 | bytes 4194304 | tf_op jit(solution)/shard_map/pallas_call | solution.py:408
  (37 shorter events, 0.4 us)
Async XLA Ops:
  0.0 36.4 %copy-start = (f32[2,256,8]{2,1,0:T(8,128)S(1)}, f32[2,256,8]{2,1,0:T(8,128)}, u32[]{:S(2)}) copy-start(f32[2,256,8]{2,1,0:T(8,128)} %constant.16.clone.refs_7_) | copy-start | bytes 49156
  0.0 36.4 %copy-start.1 = (bf16[256,512]{1,0:T(8,128)(2,1)S(1)}, bf16[256,512]{1,0:T(8,128)(2,1)}, u32[]{:S(2)}) copy-start(bf16[256,512]{1,0:T(8,128)(2,1)} %constant.15.clone.refs_6_) | copy-start | bytes 786436
  0.0 36.4 %copy-start.2 = (bf16[256,512]{1,0:T(8,128)(2,1)S(1)}, bf16[256,512]{1,0:T(8,128)(2,1)}, u32[]{:S(2)}) copy-start(bf16[256,512]{1,0:T(8,128)(2,1)} %constant.14.clone.refs_5_) | copy-start | bytes 786436
  1.9 15.2 %collective-permute-start.16 = (bf16[128,2048]{1,0:T(8,128)(2,1)S(1)}, bf16[128,2048]{1,0:T(8,128)(2,1)S(1)}, u32[]{:S(2)}, u32[]{:S(2)}) collective-permute-start(bf16[128,2048]{1,0:T(8,128)(2,1)S(1)} %get-tuple-element.47.refs_8_), channel_id=1, source_target_pairs={{0,1},{1,0},{2,3},{3,2},{4,6},{5,7},{6,4},{7,5},{8,9},{9,8},{10,11... | collective-permute-start | bytes 1572872 | tf_op jit(solution)/shard_map/ppermute | solution.py:305
  4.9 30.9 %collective-permute-start.17 = (bf16[128,2048]{1,0:T(8,128)(2,1)S(1)}, bf16[128,2048]{1,0:T(8,128)(2,1)S(1)}, u32[]{:S(2)}, u32[]{:S(2)}) collective-permute-start(bf16[128,2048]{1,0:T(8,128)(2,1)S(1)} %get-tuple-element.47.refs_8_), channel_id=1, source_target_pairs={{0,2},{1,3},{2,0},{3,1},{4,5},{5,4},{6,7},{7,6},{8,10},{9,11},{10,... | collective-permute-start | bytes 1572872 | tf_op jit(solution)/shard_map/ppermute | solution.py:305
  17.2 18.8 %collective-permute-start.18 = (bf16[128,2048]{1,0:T(8,128)(2,1)S(1)}, bf16[128,2048]{1,0:T(8,128)(2,1)S(1)}, u32[]{:S(2)}, u32[]{:S(2)}) collective-permute-start(bf16[128,2048]{1,0:T(8,128)(2,1)S(1)} %collective-permute-done.16.refs_10_), channel_id=1, source_target_pairs={{0,2},{1,3},{2,0},{3,1},{4,5},{5,4},{6,7},{7,6},{8,10},{9,11},{10,... | collective-permute-start | bytes 1572872 | tf_op jit(solution)/shard_map/ppermute | solution.py:305
  18.7 4.4 %collective-permute-start.8 = (bf16[256,128]{1,0:T(8,128)(2,1)S(1)}, bf16[256,128]{1,0:T(8,128)(2,1)S(1)}, u32[]{:S(2)}, u32[]{:S(2)}) collective-permute-start(bf16[256,128]{1,0:T(8,128)(2,1)S(1)} %get-tuple-element.38), channel_id=1, source_target_pairs={{0,8},{4,12},{8,0},{12,4},{16,24},{20,28},{24,16},{28,20},{1,9},{5... | collective-permute-start | bytes 196616 | tf_op jit(solution)/shard_map/ppermute | solution.py:296
  20.4 6.9 %collective-permute-start.9 = (bf16[256,128]{1,0:T(8,128)(2,1)S(1)}, bf16[256,128]{1,0:T(8,128)(2,1)S(1)}, u32[]{:S(2)}, u32[]{:S(2)}) collective-permute-start(bf16[256,128]{1,0:T(8,128)(2,1)S(1)} %get-tuple-element.39), channel_id=1, source_target_pairs={{0,16},{4,20},{8,24},{12,28},{16,0},{20,4},{24,8},{28,12},{1,17},{... | collective-permute-start | bytes 196616 | tf_op jit(solution)/shard_map/ppermute | solution.py:296
  23.0 6.2 %collective-permute-start.10 = (bf16[256,128]{1,0:T(8,128)(2,1)S(1)}, bf16[256,128]{1,0:T(8,128)(2,1)S(1)}, u32[]{:S(2)}, u32[]{:S(2)}) collective-permute-start(bf16[256,128]{1,0:T(8,128)(2,1)S(1)} %get-tuple-element.40), channel_id=1, source_target_pairs={{0,24},{4,28},{8,16},{12,20},{16,8},{20,12},{24,0},{28,4},{1,25},{... | collective-permute-start | bytes 196616 | tf_op jit(solution)/shard_map/ppermute | solution.py:296
  23.1 7.5 %collective-permute-start = (bf16[256,128]{1,0:T(8,128)(2,1)S(1)}, bf16[256,128]{1,0:T(8,128)(2,1)S(1)}, u32[]{:S(2)}, u32[]{:S(2)}) collective-permute-start(bf16[256,128]{1,0:T(8,128)(2,1)S(1)} %get-tuple-element.28), channel_id=1, source_target_pairs={{0,8},{4,12},{8,0},{12,4},{16,24},{20,28},{24,16},{28,20},{1,9},{5... | collective-permute-start | bytes 196616 | tf_op jit(solution)/shard_map/ppermute | solution.py:296
  27.3 5.7 %collective-permute-start.1 = (bf16[256,128]{1,0:T(8,128)(2,1)S(1)}, bf16[256,128]{1,0:T(8,128)(2,1)S(1)}, u32[]{:S(2)}, u32[]{:S(2)}) collective-permute-start(bf16[256,128]{1,0:T(8,128)(2,1)S(1)} %get-tuple-element.29), channel_id=1, source_target_pairs={{0,16},{4,20},{8,24},{12,28},{16,0},{20,4},{24,8},{28,12},{1,17},{... | collective-permute-start | bytes 196616 | tf_op jit(solution)/shard_map/ppermute | solution.py:296
  29.2 6.1 %collective-permute-start.2 = (bf16[256,128]{1,0:T(8,128)(2,1)S(1)}, bf16[256,128]{1,0:T(8,128)(2,1)S(1)}, u32[]{:S(2)}, u32[]{:S(2)}) collective-permute-start(bf16[256,128]{1,0:T(8,128)(2,1)S(1)} %get-tuple-element.30), channel_id=1, source_target_pairs={{0,24},{4,28},{8,16},{12,20},{16,8},{20,12},{24,0},{28,4},{1,25},{... | collective-permute-start | bytes 196616 | tf_op jit(solution)/shard_map/ppermute | solution.py:296
  30.5 27.7 %copy-start.3 = (bf16[1,256,2048]{2,1,0:T(8,128)(2,1)S(1)}, bf16[1,256,2048]{2,1,0:T(8,128)(2,1)}, u32[]{:S(2)}) copy-start(bf16[1,256,2048]{2,1,0:T(8,128)(2,1)} %param.11) | copy-start | bytes 3145732
  30.5 27.7 %copy-start.6 = (bf16[128,256]{1,0:T(8,128)(2,1)S(1)}, bf16[128,256]{1,0:T(8,128)(2,1)}, u32[]{:S(2)}) copy-start(bf16[128,256]{1,0:T(8,128)(2,1)} %constant.18.clone.refs_6_) | copy-start | bytes 196612
  30.5 27.7 %copy-start.7 = (bf16[128,256]{1,0:T(8,128)(2,1)S(1)}, bf16[128,256]{1,0:T(8,128)(2,1)}, u32[]{:S(2)}) copy-start(bf16[128,256]{1,0:T(8,128)(2,1)} %constant.17.clone.refs_5_) | copy-start | bytes 196612
  30.6 5.8 %collective-permute-start.11 = (bf16[4,256,128]{2,1,0:T(8,128)(2,1)S(1)}, bf16[4,256,128]{2,1,0:T(8,128)(2,1)S(1)}, u32[]{:S(2)}, u32[]{:S(2)}) collective-permute-start(bf16[4,256,128]{2,1,0:T(8,128)(2,1)S(1)} %shard_map.104), channel_id=1, source_target_pairs={{0,4},{4,0},{8,12},{12,8},{16,20},{20,16},{24,28},{28,24},{1,5},{5... | collective-permute-start | bytes 786440 | tf_op jit(solution)/shard_map/ppermute | solution.py:296
  35.3 2.8 %collective-permute-start.3 = (bf16[4,256,128]{2,1,0:T(8,128)(2,1)S(1)}, bf16[4,256,128]{2,1,0:T(8,128)(2,1)S(1)}, u32[]{:S(2)}, u32[]{:S(2)}) collective-permute-start(bf16[4,256,128]{2,1,0:T(8,128)(2,1)S(1)} %shard_map.101), channel_id=1, source_target_pairs={{0,4},{4,0},{8,12},{12,8},{16,20},{20,16},{24,28},{28,24},{1,5},{5... | collective-permute-start | bytes 786440 | tf_op jit(solution)/shard_map/ppermute | solution.py:296
  35.4 27.9 %collective-permute-start.19 = (bf16[128,2048]{1,0:T(8,128)(2,1)S(1)}, bf16[128,2048]{1,0:T(8,128)(2,1)S(1)}, u32[]{:S(2)}, u32[]{:S(2)}) collective-permute-start(bf16[128,2048]{1,0:T(8,128)(2,1)S(1)} %collective-permute-done.16.refs_10_), channel_id=1, source_target_pairs={{0,4},{4,0},{8,12},{12,8},{16,20},{20,16},{24,28},{28,24},{1,5},{5... | collective-permute-start | bytes 1572872 | tf_op jit(solution)/shard_map/ppermute | solution.py:296
  35.9 27.3 %collective-permute-start.20 = (bf16[128,2048]{1,0:T(8,128)(2,1)S(1)}, bf16[128,2048]{1,0:T(8,128)(2,1)S(1)}, u32[]{:S(2)}, u32[]{:S(2)}) collective-permute-start(bf16[128,2048]{1,0:T(8,128)(2,1)S(1)} %collective-permute-done.17.refs_11_), channel_id=1, source_target_pairs={{0,4},{4,0},{8,12},{12,8},{16,20},{20,16},{24,28},{28,24},{1,5},{5... | collective-permute-start | bytes 1572872 | tf_op jit(solution)/shard_map/ppermute | solution.py:296
  36.0 27.3 %collective-permute-start.21 = (bf16[128,2048]{1,0:T(8,128)(2,1)S(1)}, bf16[128,2048]{1,0:T(8,128)(2,1)S(1)}, u32[]{:S(2)}, u32[]{:S(2)}) collective-permute-start(bf16[128,2048]{1,0:T(8,128)(2,1)S(1)} %collective-permute-done.18.refs_12_), channel_id=1, source_target_pairs={{0,4},{4,0},{8,12},{12,8},{16,20},{20,16},{24,28},{28,24},{1,5},{5... | collective-permute-start | bytes 1572872 | tf_op jit(solution)/shard_map/ppermute | solution.py:296
  38.0 25.2 %copy-start.4 = (bf16[128,256]{1,0:T(8,128)(2,1)S(1)}, bf16[128,256]{1,0:T(8,128)(2,1)}, u32[]{:S(2)}) copy-start(bf16[128,256]{1,0:T(8,128)(2,1)} %constant.20.clone.refs_5_) | copy-start | bytes 196612
  38.1 25.2 %copy-start.5 = (bf16[128,256]{1,0:T(8,128)(2,1)S(1)}, bf16[128,256]{1,0:T(8,128)(2,1)}, u32[]{:S(2)}) copy-start(bf16[128,256]{1,0:T(8,128)(2,1)} %constant.19.clone.refs_4_) | copy-start | bytes 196612
  38.1 5.4 %collective-permute-start.12 = (bf16[2,128,128]{2,1,0:T(8,128)(2,1)S(1)}, bf16[2,128,128]{2,1,0:T(8,128)(2,1)S(1)}, u32[]{:S(2)}, u32[]{:S(2)}) collective-permute-start(bf16[2,128,128]{2,1,0:T(8,128)(2,1)S(1)} %get-tuple-element.42), channel_id=1, source_target_pairs={{0,8},{4,12},{8,0},{12,4},{16,24},{20,28},{24,16},{28,20},{1,9},{5... | collective-permute-start | bytes 196616 | tf_op jit(solution)/shard_map/ppermute | solution.py:296
  38.2 6.6 %collective-permute-start.13 = (bf16[2,128,128]{2,1,0:T(8,128)(2,1)S(1)}, bf16[2,128,128]{2,1,0:T(8,128)(2,1)S(1)}, u32[]{:S(2)}, u32[]{:S(2)}) collective-permute-start(bf16[2,128,128]{2,1,0:T(8,128)(2,1)S(1)} %get-tuple-element.43), channel_id=1, source_target_pairs={{0,16},{4,20},{8,24},{12,28},{16,0},{20,4},{24,8},{28,12},{1,17},{... | collective-permute-start | bytes 196616 | tf_op jit(solution)/shard_map/ppermute | solution.py:296
  43.5 7.5 %collective-permute-start.4 = (bf16[4,128,128]{2,1,0:T(8,128)(2,1)S(1)}, bf16[4,128,128]{2,1,0:T(8,128)(2,1)S(1)}, u32[]{:S(2)}, u32[]{:S(2)}) collective-permute-start(bf16[4,128,128]{2,1,0:T(8,128)(2,1)S(1)} %get-tuple-element.32), channel_id=1, source_target_pairs={{0,4},{4,0},{8,12},{12,8},{16,20},{20,16},{24,28},{28,24},{1,5},{5... | collective-permute-start | bytes 393224 | tf_op jit(solution)/shard_map/ppermute | solution.py:296
  44.8 6.1 %collective-permute-start.14 = (bf16[2,128,128]{2,1,0:T(8,128)(2,1)S(1)}, bf16[2,128,128]{2,1,0:T(8,128)(2,1)S(1)}, u32[]{:S(2)}, u32[]{:S(2)}) collective-permute-start(bf16[2,128,128]{2,1,0:T(8,128)(2,1)S(1)} %get-tuple-element.44), channel_id=1, source_target_pairs={{0,24},{4,28},{8,16},{12,20},{16,8},{20,12},{24,0},{28,4},{1,25},{... | collective-permute-start | bytes 196616 | tf_op jit(solution)/shard_map/ppermute | solution.py:296
  50.9 5.5 %collective-permute-start.15 = (bf16[4,128,128]{2,1,0:T(8,128)(2,1)S(1)}, bf16[4,128,128]{2,1,0:T(8,128)(2,1)S(1)}, u32[]{:S(2)}, u32[]{:S(2)}) collective-permute-start(bf16[4,128,128]{2,1,0:T(8,128)(2,1)S(1)} %shard_map.106), channel_id=1, source_target_pairs={{0,4},{4,0},{8,12},{12,8},{16,20},{20,16},{24,28},{28,24},{1,5},{5... | collective-permute-start | bytes 393224 | tf_op jit(solution)/shard_map/ppermute | solution.py:296
  51.0 4.5 %collective-permute-start.5 = (bf16[2,128,128]{2,1,0:T(8,128)(2,1)S(1)}, bf16[2,128,128]{2,1,0:T(8,128)(2,1)S(1)}, u32[]{:S(2)}, u32[]{:S(2)}) collective-permute-start(bf16[2,128,128]{2,1,0:T(8,128)(2,1)S(1)} %get-tuple-element.34), channel_id=1, source_target_pairs={{0,8},{4,12},{8,0},{12,4},{16,24},{20,28},{24,16},{28,20},{1,9},{5... | collective-permute-start | bytes 196616 | tf_op jit(solution)/shard_map/ppermute | solution.py:296
  55.5 7.7 %collective-permute-start.6 = (bf16[2,128,128]{2,1,0:T(8,128)(2,1)S(1)}, bf16[2,128,128]{2,1,0:T(8,128)(2,1)S(1)}, u32[]{:S(2)}, u32[]{:S(2)}) collective-permute-start(bf16[2,128,128]{2,1,0:T(8,128)(2,1)S(1)} %get-tuple-element.35), channel_id=1, source_target_pairs={{0,16},{4,20},{8,24},{12,28},{16,0},{20,4},{24,8},{28,12},{1,17},{... | collective-permute-start | bytes 196616 | tf_op jit(solution)/shard_map/ppermute | solution.py:296
  56.4 6.9 %collective-permute-start.7 = (bf16[2,128,128]{2,1,0:T(8,128)(2,1)S(1)}, bf16[2,128,128]{2,1,0:T(8,128)(2,1)S(1)}, u32[]{:S(2)}, u32[]{:S(2)}) collective-permute-start(bf16[2,128,128]{2,1,0:T(8,128)(2,1)S(1)} %get-tuple-element.36), channel_id=1, source_target_pairs={{0,24},{4,28},{8,16},{12,20},{16,8},{20,12},{24,0},{28,4},{1,25},{... | collective-permute-start | bytes 196616 | tf_op jit(solution)/shard_map/ppermute | solution.py:296

commit v5 on v4

--- a/solution.py
+++ b/solution.py
@@ -61,9 +61,9 @@
 
 
 def pick_kernel(chips, fast, *refs):
-    x_ref, w_ref = refs[:2]
-    outs = [refs[2 + q * chips : 2 + (q + 1) * chips] for q in range(CHUNKS)]
-    halves = refs[2 + CHUNKS * chips : -3]
+    x_ref, w_ref, narrow_ref = refs[:3]
+    outs = [refs[3 + q * chips : 3 + (q + 1) * chips] for q in range(CHUNKS)]
+    narrow, *halves = refs[3 + CHUNKS * chips : -3]
     tokens, x_sems, w_sems = refs[-3:]
     row = lax.axis_index("row")
     core, chip = row % 2, row // 2
@@ -78,7 +78,8 @@
     order = [*send_order(chips), 0]
     for zs in order:
         loads[zs].start()
-    fetches = []
+    fetches = [pltpu.make_async_copy(narrow_ref.at[core], narrow, w_sems.at[2])]
+    fetches[0].start()
     if fast:
         half = GROUP // 2
         for i, h in enumerate((core, 1 - core)):
@@ -103,6 +104,11 @@
         fetch.wait()
 
 
+def twist_kernel(narrow, out):
+    for i in range(out.shape[0]):
+        out[i] = jnp.broadcast_to(narrow[:, i : i + 1], out.shape[1:])
+
+
 def stack_kernel(*refs):
     for zs, piece in enumerate(refs[:-1]):
         refs[-1][zs] = piece[...]
@@ -140,39 +146,40 @@
     core, chip = row % 2, row // 2
     half = rows // 2
 
-    lane = lax.broadcasted_iota(jnp.int32, (1, lanes), 1)
-    chips_per_group = GROUP // (CHUNKS * lanes)
-    first = (chip % chips_per_group == 0) if q == 0 else False
-    lone_low = (lane == 0) & first
-    lone_high = (lane == pairs) & first
-    own = jnp.where((lane < pairs) | lone_high, 1.0, -1.0).astype(jnp.float32)
-    other = jnp.where(lone_low | lone_high, 0.0, 1.0).astype(jnp.float32)
-    cosine = (lane < pairs) | lone_high
-
     odd_core = core == 1
     sign = jnp.where(odd_core, -1.0, 1.0).astype(jnp.float32)
     upper = row >= half
     near, far = jnp.where(upper, sign, 1.0), jnp.where(upper, 1.0, sign)
 
+    lane = lax.broadcasted_iota(jnp.int32, (2 * lanes, lanes), 1)
+    line = lax.broadcasted_iota(jnp.int32, (2 * lanes, lanes), 0)
+    chips_per_group = GROUP // (CHUNKS * lanes)
+    first = (chip % chips_per_group == 0) if q == 0 else False
+    lone_high = (lane == pairs) & first
+    alone = ((lane == 0) | (lane == pairs)) & first
+    own = jnp.where((lane < pairs) | lone_high, 1.0, -1.0)
+    other = jnp.where(alone, 0.0, 1.0)
+    side = jnp.where(line < lanes, near, far)
+    there = line % lanes
+    entry = jnp.where(there == lane, own, jnp.where(there == (lane + pairs) % lanes, other, 0.0))
+    fold = (entry * side).astype(jnp.bfloat16)
+
     def block(s):
-        value = mine[s // 2][...] if s % 2 == 0 else theirs[s // 2]
-        return value.astype(jnp.float32)
+        return mine[s // 2][...] if s % 2 == 0 else theirs[s // 2]
 
     for s in range(half):
-        value = near * block(s) + far * block(s ^ half)
-        if lanes % 128 == 0:
-            rolled = pltpu.roll(value, pairs, 1)
-        else:
-            rolled = jnp.concatenate([value[:, pairs:], value[:, :pairs]], axis=1)
-        folded[(row % half) ^ s] = value * own + rolled * other
-
+        both = jnp.concatenate([block(s), block(s ^ half)], axis=1)
+        folded[(row % half) ^ s] = jnp.dot(both, fold, preferred_element_type=jnp.float32)
+
+    lane = lax.broadcasted_iota(jnp.int32, (1, lanes), 1)
+    cosine = (lane < pairs) | ((lane == pairs) & first)
     turns = []
     for n in range(half):
         angle = 2 * math.pi * n / rows
         c = jnp.where(odd_core, math.cos(angle), 1.0).astype(jnp.float32)
         d = jnp.where(odd_core, math.sin(angle), 0.0).astype(jnp.float32)
         turns.append((jnp.where(cosine, c, d), jnp.where(cosine, -d, c)))
-    tile = min(inner, 32)
+    tile = min(inner, 128)
 
     def step(i, carry):
         at = pl.ds(pl.multiple_of(i * tile, tile), tile)
@@ -181,9 +188,8 @@
         for n in range(half):
             v = folded[n, at, :]
             values.append((v * turns[n][0], v * turns[n][1]))
-        tw = twist[core, at, :]
         for j, (a, b) in enumerate(complex_dft(values)):
-            c, s = tw[:, j : j + 1], tw[:, half + j : half + j + 1]
+            c, s = twist[j, at, :], twist[half + j, at, :]
             cols = slice(j * lanes, (j + 1) * lanes)
             turned_z[at, cols] = (a * c + b * s).astype(jnp.bfloat16)
             turned_z[low_at, cols] = (b * c - a * s).astype(jnp.bfloat16)
@@ -330,7 +336,7 @@
     width = w_proj.shape[1]
     scale = 1.0 / math.sqrt(count * rows * GROUP)
     table_hi, table_lo = split_halves(position_table(count, scale))
-    twist = twist_table(rows, count)
+    narrow = jnp.asarray(twist_table(rows, count))
     features_of = feature_table(lanes // 2)
     feat_hi, feat_lo = split_halves(features_of)
     bf = jnp.bfloat16
@@ -340,23 +346,24 @@
     picked = pl.pallas_call(
         functools.partial(pick_kernel, chips, fast),
         out_shape=[jax.ShapeDtypeStruct((count, lanes), bf)] * (CHUNKS * chips)
+        + [jax.ShapeDtypeStruct((count, rows), jnp.float32)]
         + [half_w] * (2 * fast),
-        in_specs=[pl.BlockSpec(memory_space=pltpu.HBM)] * 2,
-        out_specs=[pl.BlockSpec(memory_space=pltpu.VMEM)] * (CHUNKS * chips + 2 * fast),
+        in_specs=[pl.BlockSpec(memory_space=pltpu.HBM)] * 3,
+        out_specs=[pl.BlockSpec(memory_space=pltpu.VMEM)] * (CHUNKS * chips + 1 + 2 * fast),
         scratch_shapes=[
             pltpu.VMEM((chips, count, GROUP), bf),
             pltpu.SemaphoreType.DMA((chips,)),
-            pltpu.SemaphoreType.DMA((2,)),
+            pltpu.SemaphoreType.DMA((3,)),
         ],
         compiler_params=pltpu.CompilerParams(vmem_limit_bytes=24 * MIB),
         cost_estimate=pl.CostEstimate(
             flops=2 * count * GROUP * features, bytes_accessed=MIB, transcendentals=0
         ),
-    )(*(pltpu.with_memory_space_constraint(v, pltpu.HBM) for v in (tokens, w_proj)))
+    )(*(pltpu.with_memory_space_constraint(v, pltpu.HBM) for v in (tokens, w_proj, narrow)))
     arrived = [across_chips(picked[q * chips : (q + 1) * chips], rows) for q in range(CHUNKS)]
 
     if fast:
-        mine, rest = picked[CHUNKS * chips :]
+        mine, rest = picked[CHUNKS * chips + 1 :]
         w_a = turn_swap(mine, rows, n_col, (1, 2))
         w_b = turn_swap(mine, rows, n_col, (2, 1))
         w_c = turn_swap(w_a, rows, n_col, (2, 1))
@@ -368,6 +375,9 @@
     piece = jax.ShapeDtypeStruct((2, lines, lanes), bf)
     small = (count * features // 4, count * features)
     stacked = jax.ShapeDtypeStruct((chips, lines, lanes), bf)
+    twist = vmem_call(
+        twist_kernel, jax.ShapeDtypeStruct((rows, count, lanes), jnp.float32), [], *small
+    )(picked[CHUNKS * chips])
     sent = []
     for q in range(CHUNKS):
         stack = vmem_call(

time: 66.1 us -> 62.9 us (0.952)
  starting transfers between devices: 24 us -> 20 us
  waiting for transfers between devices: 33.1 us -> 34.6 us
  Pallas kernels: 8.61 us -> 7.89 us
    ppermute x19, starting transfers between devices: 17.9 us -> 13.9 us  [swap(): return lax.ppermute(value, axis, [(i, i ^ bit) for i in range(size)])]
    ppermute x19, waiting for transfers between devices: 22.4 us -> 23.9 us  [swap(): return lax.ppermute(value, axis, [(i, i ^ bit) for i in range(size)])]
    pallas_call x2, Pallas kernels: 3.2 us -> 2.15 us  [program(): vmem_call(functools.partial(position_kernel, rows, q), [piece] * chips if...]
  transfers between devices with their start and end apart: 22 -> 22, of which waited for: 9 -> 11; matrix products, arithmetic and copies ran while one was open for 0% -> 0% of each run, Pallas kernels for 6% -> 5%
where the time goes in v5:
time: 62.9 us; the launch traced here: 62.8 us
  waiting for transfers between devices  34.6 us (55%)
  starting transfers between devices  20 us (32%)
  Pallas kernels  7.89 us (13%)
    ppermute x19, waiting for transfers between devices, swap(): return lax.ppermute(value, axis, [(i, i ^ bit) for i in range(size)])  23.9 us
    ppermute x19, starting transfers between devices, swap(): return lax.ppermute(value, axis, [(i, i ^ bit) for i in range(size)])  13.9 us
    ppermute x3, waiting for transfers between devices, turn_swap(): return lax.ppermute(value, ('row', 'col'), turn)  10.7 us
    ppermute x3, starting transfers between devices, turn_swap(): return lax.ppermute(value, ('row', 'col'), turn)  6.11 us
    pallas_call x1, Pallas kernels, program(): pl.pallas_call(functools.partial(final_kernel, rows), out_shape=jax.Shape...  2.66 us
    pallas_call x2, Pallas kernels, program(): vmem_call(functools.partial(position_kernel, rows, q), [piece] * chips if...  2.15 us
    pallas_call x1, Pallas kernels, program(): pl.pallas_call(functools.partial(pick_kernel, chips, fast), out_shape=[ja...  1.89 us
  transfers between devices with their start and end apart: 22, of which 11 were waited for; matrix products, arithmetic and copies ran while one was open for 0% of the time, Pallas kernels for 5%

profile of v5, /device:TPU:0, one launch (start us, length us, event | category | flops | bytes accessed | tf_op | source)
XLA Modules:
  0.0 62.8 jit_solution(6216117614145088890)
XLA Ops:
  0.0 1.9 %shard_map.100 = (bf16[256,128]{1,0:T(8,128)(2,1)S(1)}, bf16[256,128]{1,0:T(8,128)(2,1)S(1)}, bf16[256,128]{1,0:T(8,128)(2,1)S(1)}, bf16[256,128]{1,0:T(8,128)(2...) custom-call(bf16[256,1024]{1,0:T(8,128)(2,1)} %bitcast.4, ...), custom_call_target="tpu_custom_call" | custom-call | flops 134217728 | bytes 1048576 | tf_op jit(solution)/shard_map/pallas_call | solution.py:346
  1.9 3.0 %collective-permute-start.16 = (bf16[128,2048]{1,0:T(8,128)(2,1)S(1)}, bf16[128,2048]{1,0:T(8,128)(2,1)S(1)}, u32[]{:S(2)}, u32[]{:S(2)}) collective-permute-start(bf16[128,2048]{1,0:T(8,128)(2,1)S(1)} %get-tuple-element.49.refs_8_), channel_id=1, source_target_pairs={{0,1},{1,0},{2,3},{3,2},{4,6},{5,7},{6,4},{7,5},{8,9},{9,8},{10,11... | collective-permute-start | bytes 1572872 | tf_op jit(solution)/shard_map/ppermute | solution.py:311
  4.9 1.5 %collective-permute-start.17 = (bf16[128,2048]{1,0:T(8,128)(2,1)S(1)}, bf16[128,2048]{1,0:T(8,128)(2,1)S(1)}, u32[]{:S(2)}, u32[]{:S(2)}) collective-permute-start(bf16[128,2048]{1,0:T(8,128)(2,1)S(1)} %get-tuple-element.49.refs_8_), channel_id=1, source_target_pairs={{0,2},{1,3},{2,0},{3,1},{4,5},{5,4},{6,7},{7,6},{8,10},{9,11},{10,... | collective-permute-start | bytes 1572872 | tf_op jit(solution)/shard_map/ppermute | solution.py:311
  6.5 10.7 %collective-permute-done.16.refs_10_ = bf16[128,2048]{1,0:T(8,128)(2,1)S(1)} collective-permute-done((bf16[128,2048]{1,0:T(8,128)(2,1)S(1)}, bf16[128,2048]{1,0:T(8,128)(2,1)S(1)}, u32[]{:S(2)}, u32[]{:S(2)}) %collective-permute-start.16) | collective-permute-done | bytes 524320 | tf_op jit(solution)/shard_map/ppermute | solution.py:311
  17.1 1.6 %collective-permute-start.18 = (bf16[128,2048]{1,0:T(8,128)(2,1)S(1)}, bf16[128,2048]{1,0:T(8,128)(2,1)S(1)}, u32[]{:S(2)}, u32[]{:S(2)}) collective-permute-start(bf16[128,2048]{1,0:T(8,128)(2,1)S(1)} %collective-permute-done.16.refs_10_), channel_id=1, source_target_pairs={{0,2},{1,3},{2,0},{3,1},{4,5},{5,4},{6,7},{7,6},{8,10},{9,11},{10,... | collective-permute-start | bytes 1572872 | tf_op jit(solution)/shard_map/ppermute | solution.py:311
  18.7 1.7 %collective-permute-start.8 = (bf16[256,128]{1,0:T(8,128)(2,1)S(1)}, bf16[256,128]{1,0:T(8,128)(2,1)S(1)}, u32[]{:S(2)}, u32[]{:S(2)}) collective-permute-start(bf16[256,128]{1,0:T(8,128)(2,1)S(1)} %get-tuple-element.40), channel_id=1, source_target_pairs={{0,8},{4,12},{8,0},{12,4},{16,24},{20,28},{24,16},{28,20},{1,9},{5... | collective-permute-start | bytes 196616 | tf_op jit(solution)/shard_map/ppermute | solution.py:302
  20.4 2.6 %collective-permute-start.9 = (bf16[256,128]{1,0:T(8,128)(2,1)S(1)}, bf16[256,128]{1,0:T(8,128)(2,1)S(1)}, u32[]{:S(2)}, u32[]{:S(2)}) collective-permute-start(bf16[256,128]{1,0:T(8,128)(2,1)S(1)} %get-tuple-element.41), channel_id=1, source_target_pairs={{0,16},{4,20},{8,24},{12,28},{16,0},{20,4},{24,8},{28,12},{1,17},{... | collective-permute-start | bytes 196616 | tf_op jit(solution)/shard_map/ppermute | solution.py:302
  23.0 0.1 collective-permute-start.10
  23.1 2.3 %collective-permute-start = (bf16[256,128]{1,0:T(8,128)(2,1)S(1)}, bf16[256,128]{1,0:T(8,128)(2,1)S(1)}, u32[]{:S(2)}, u32[]{:S(2)}) collective-permute-start(bf16[256,128]{1,0:T(8,128)(2,1)S(1)} %get-tuple-element.29), channel_id=1, source_target_pairs={{0,8},{4,12},{8,0},{12,4},{16,24},{20,28},{24,16},{28,20},{1,9},{5... | collective-permute-start | bytes 196616 | tf_op jit(solution)/shard_map/ppermute | solution.py:302
  25.4 1.9 %collective-permute-done.9.refs_2_ = bf16[256,128]{1,0:T(8,128)(2,1)S(1)} collective-permute-done((bf16[256,128]{1,0:T(8,128)(2,1)S(1)}, bf16[256,128]{1,0:T(8,128)(2,1)S(1)}, u32[]{:S(2)}, u32[]{:S(2)}) %collective-permute-start.9) | collective-permute-done | bytes 65568 | tf_op jit(solution)/shard_map/ppermute | solution.py:302
  27.3 1.9 %collective-permute-start.1 = (bf16[256,128]{1,0:T(8,128)(2,1)S(1)}, bf16[256,128]{1,0:T(8,128)(2,1)S(1)}, u32[]{:S(2)}, u32[]{:S(2)}) collective-permute-start(bf16[256,128]{1,0:T(8,128)(2,1)S(1)} %get-tuple-element.30), channel_id=1, source_target_pairs={{0,16},{4,20},{8,24},{12,28},{16,0},{20,4},{24,8},{28,12},{1,17},{... | collective-permute-start | bytes 196616 | tf_op jit(solution)/shard_map/ppermute | solution.py:302
  29.2 1.3 %collective-permute-start.2 = (bf16[256,128]{1,0:T(8,128)(2,1)S(1)}, bf16[256,128]{1,0:T(8,128)(2,1)S(1)}, u32[]{:S(2)}, u32[]{:S(2)}) collective-permute-start(bf16[256,128]{1,0:T(8,128)(2,1)S(1)} %get-tuple-element.31), channel_id=1, source_target_pairs={{0,24},{4,28},{8,16},{12,20},{16,8},{20,12},{24,0},{28,4},{1,25},{... | collective-permute-start | bytes 196616 | tf_op jit(solution)/shard_map/ppermute | solution.py:302
  30.6 2.4 %collective-permute-done.1.refs_2_ = bf16[256,128]{1,0:T(8,128)(2,1)S(1)} collective-permute-done((bf16[256,128]{1,0:T(8,128)(2,1)S(1)}, bf16[256,128]{1,0:T(8,128)(2,1)S(1)}, u32[]{:S(2)}, u32[]{:S(2)}) %collective-permute-start.1) | collective-permute-done | bytes 65568 | tf_op jit(solution)/shard_map/ppermute | solution.py:302
  33.0 2.3 %collective-permute-done.2.refs_3_ = bf16[256,128]{1,0:T(8,128)(2,1)S(1)} collective-permute-done((bf16[256,128]{1,0:T(8,128)(2,1)S(1)}, bf16[256,128]{1,0:T(8,128)(2,1)S(1)}, u32[]{:S(2)}, u32[]{:S(2)}) %collective-permute-start.2) | collective-permute-done | bytes 65568 | tf_op jit(solution)/shard_map/ppermute | solution.py:302
  35.4 0.5 collective-permute-start.19
  35.9 0.1 collective-permute-start.20
  36.0 0.4 collective-permute-start.21
  36.4 0.3 shard_map.102.refs_7_
  36.8 1.1 %shard_map.106 = (bf16[2,128,128]{2,1,0:T(8,128)(2,1)S(1)}, bf16[2,128,128]{2,1,0:T(8,128)(2,1)S(1)}, bf16[2,128,128]{2,1,0:T(8,128)(2,1)S(1)}, bf16[2,128,128]{2,1,0:T(8,128)(2,1)S(1)}) custom-call(bf16[256,128]{1,0:T(8,128)(2,1)S(1)} %get-tuple-element.39.refs_0_, bf16[256,128]{1,0:T(8,128)(2,1)S(1)} %collective-permute-done.8.refs_1_, ...), custom_call_target="tpu_custom_call" | custom-call | flops 268435456 | bytes 1048576 | tf_op jit(solution)/shard_map/pallas_call | solution.py:388
  38.0 1.9 %collective-permute-start.13 = (bf16[2,128,128]{2,1,0:T(8,128)(2,1)S(1)}, bf16[2,128,128]{2,1,0:T(8,128)(2,1)S(1)}, u32[]{:S(2)}, u32[]{:S(2)}) collective-permute-start(bf16[2,128,128]{2,1,0:T(8,128)(2,1)S(1)} %get-tuple-element.45), channel_id=1, source_target_pairs={{0,16},{4,20},{8,24},{12,28},{16,0},{20,4},{24,8},{28,12},{1,17},{... | collective-permute-start | bytes 196616 | tf_op jit(solution)/shard_map/ppermute | solution.py:302
  39.9 1.1 %shard_map.103 = (bf16[4,128,128]{2,1,0:T(8,128)(2,1)S(1)}, bf16[4,128,128]{2,1,0:T(8,128)(2,1)S(1)}) custom-call(bf16[256,128]{1,0:T(8,128)(2,1)S(1)} %get-tuple-element.28.refs_0_, bf16[256,128]{1,0:T(8,128)(2,1)S(1)} %collective-permute-done.refs_1_, bf16[256,128]{1,0:T(8,128)(2,1)S(1)} %collective-permute-done.1.refs_2_, ...), custom_call_target="tpu_custom_call" | custom-call | flops 268435456 | bytes 1048576 | tf_op jit(solution)/shard_map/pallas_call | solution.py:388
  41.0 2.2 %collective-permute-done.12.refs_1_ = bf16[2,128,128]{2,1,0:T(8,128)(2,1)S(1)} collective-permute-done((bf16[2,128,128]{2,1,0:T(8,128)(2,1)S(1)}, bf16[2,128,128]{2,1,0:T(8,128)(2,1)S(1)}, u32[]{:S(2)}, u32[]{:S(2)}) %collective-permute-start.12) | collective-permute-done | bytes 65568 | tf_op jit(solution)/shard_map/ppermute | solution.py:302
  43.3 0.4 collective-permute-start.14
  43.6 1.1 %collective-permute-done.13.refs_2_ = bf16[2,128,128]{2,1,0:T(8,128)(2,1)S(1)} collective-permute-done((bf16[2,128,128]{2,1,0:T(8,128)(2,1)S(1)}, bf16[2,128,128]{2,1,0:T(8,128)(2,1)S(1)}, u32[]{:S(2)}, u32[]{:S(2)}) %collective-permute-start.13) | collective-permute-done | bytes 65568 | tf_op jit(solution)/shard_map/ppermute | solution.py:302
  44.7 4.6 %collective-permute-done.14.refs_3_ = bf16[2,128,128]{2,1,0:T(8,128)(2,1)S(1)} collective-permute-done((bf16[2,128,128]{2,1,0:T(8,128)(2,1)S(1)}, bf16[2,128,128]{2,1,0:T(8,128)(2,1)S(1)}, u32[]{:S(2)}, u32[]{:S(2)}) %collective-permute-start.14) | collective-permute-done | bytes 65568 | tf_op jit(solution)/shard_map/ppermute | solution.py:302
  49.5 1.2 %collective-permute-done.15.refs_4_ = bf16[4,128,128]{2,1,0:T(8,128)(2,1)S(1)} collective-permute-done((bf16[4,128,128]{2,1,0:T(8,128)(2,1)S(1)}, bf16[4,128,128]{2,1,0:T(8,128)(2,1)S(1)}, u32[]{:S(2)}, u32[]{:S(2)}) %collective-permute-start.15) | collective-permute-done | bytes 131104 | tf_op jit(solution)/shard_map/ppermute | solution.py:302
  50.7 3.2 %collective-permute-done.5.refs_1_ = bf16[2,128,128]{2,1,0:T(8,128)(2,1)S(1)} collective-permute-done((bf16[2,128,128]{2,1,0:T(8,128)(2,1)S(1)}, bf16[2,128,128]{2,1,0:T(8,128)(2,1)S(1)}, u32[]{:S(2)}, u32[]{:S(2)}) %collective-permute-start.5) | collective-permute-done | bytes 65568 | tf_op jit(solution)/shard_map/ppermute | solution.py:302
  54.0 0.4 collective-permute-start.7
  54.4 0.8 %shard_map.108 = (f32[4,256,256]{2,1,0:T(8,128)S(1)}, f32[256,2048]{1,0:T(8,128)S(1)}) custom-call(bf16[2,128,128]{2,1,0:T(8,128)(2,1)S(1)} %get-tuple-element.43.refs_0_, bf16[2,128,128]{2,1,0:T(8,128)(2,1)S(1)} %collective-permute-done.12.refs_1_, bf16[2,128,128]{2,1,0:T(8,128)(2,1)S(1)} %collective-permute-done.13.refs_2_, ...), custom_call_target="tpu_custom_call" | custom-call | flops 134217728 | bytes 3145728 | tf_op jit(solution)/shard_map/pallas_call | solution.py:408
  55.2 2.4 %collective-permute-done.6.refs_2_ = bf16[2,128,128]{2,1,0:T(8,128)(2,1)S(1)} collective-permute-done((bf16[2,128,128]{2,1,0:T(8,128)(2,1)S(1)}, bf16[2,128,128]{2,1,0:T(8,128)(2,1)S(1)}, u32[]{:S(2)}, u32[]{:S(2)}) %collective-permute-start.6) | collective-permute-done | bytes 65568 | tf_op jit(solution)/shard_map/ppermute | solution.py:302
  57.6 2.5 %collective-permute-done.7.refs_3_ = bf16[2,128,128]{2,1,0:T(8,128)(2,1)S(1)} collective-permute-done((bf16[2,128,128]{2,1,0:T(8,128)(2,1)S(1)}, bf16[2,128,128]{2,1,0:T(8,128)(2,1)S(1)}, u32[]{:S(2)}, u32[]{:S(2)}) %collective-permute-start.7) | collective-permute-done | bytes 65568 | tf_op jit(solution)/shard_map/ppermute | solution.py:302
  60.1 2.7 %shard_map.109 = bf16[256,2048]{1,0:T(8,128)(2,1)} custom-call(bf16[2,128,128]{2,1,0:T(8,128)(2,1)S(1)} %get-tuple-element.35.refs_0_, bf16[2,128,128]{2,1,0:T(8,128)(2,1)S(1)} %collective-permute-done.5.refs_1_, bf16[2,128,128]{2,1,0:T(8,128)(2,1)S(1)} %collective-permute-done.6.refs_2_, bf16[2,128,128]{2,1,0:T(8,128)(2,1)S(1)} %collective-permute-done.7.refs_3_, ...), custom_call_target="tpu_custom_call" | custom-call | flops 1073741824 | bytes 4194304 | tf_op jit(solution)/shard_map/pallas_call | solution.py:418
  (36 shorter events, 0.5 us)
Async XLA Ops:
  0.0 36.8 %copy-start.1 = (bf16[256,512]{1,0:T(8,128)(2,1)S(1)}, bf16[256,512]{1,0:T(8,128)(2,1)}, u32[]{:S(2)}) copy-start(bf16[256,512]{1,0:T(8,128)(2,1)} %constant.16.clone.refs_6_) | copy-start | bytes 786436
  0.0 36.8 %copy-start.2 = (bf16[256,512]{1,0:T(8,128)(2,1)S(1)}, bf16[256,512]{1,0:T(8,128)(2,1)}, u32[]{:S(2)}) copy-start(bf16[256,512]{1,0:T(8,128)(2,1)} %constant.15.clone.refs_5_) | copy-start | bytes 786436
  1.9 15.2 %collective-permute-start.16 = (bf16[128,2048]{1,0:T(8,128)(2,1)S(1)}, bf16[128,2048]{1,0:T(8,128)(2,1)S(1)}, u32[]{:S(2)}, u32[]{:S(2)}) collective-permute-start(bf16[128,2048]{1,0:T(8,128)(2,1)S(1)} %get-tuple-element.49.refs_8_), channel_id=1, source_target_pairs={{0,1},{1,0},{2,3},{3,2},{4,6},{5,7},{6,4},{7,5},{8,9},{9,8},{10,11... | collective-permute-start | bytes 1572872 | tf_op jit(solution)/shard_map/ppermute | solution.py:311
  4.9 30.9 %collective-permute-start.17 = (bf16[128,2048]{1,0:T(8,128)(2,1)S(1)}, bf16[128,2048]{1,0:T(8,128)(2,1)S(1)}, u32[]{:S(2)}, u32[]{:S(2)}) collective-permute-start(bf16[128,2048]{1,0:T(8,128)(2,1)S(1)} %get-tuple-element.49.refs_8_), channel_id=1, source_target_pairs={{0,2},{1,3},{2,0},{3,1},{4,5},{5,4},{6,7},{7,6},{8,10},{9,11},{10,... | collective-permute-start | bytes 1572872 | tf_op jit(solution)/shard_map/ppermute | solution.py:311
  17.1 18.8 %collective-permute-start.18 = (bf16[128,2048]{1,0:T(8,128)(2,1)S(1)}, bf16[128,2048]{1,0:T(8,128)(2,1)S(1)}, u32[]{:S(2)}, u32[]{:S(2)}) collective-permute-start(bf16[128,2048]{1,0:T(8,128)(2,1)S(1)} %collective-permute-done.16.refs_10_), channel_id=1, source_target_pairs={{0,2},{1,3},{2,0},{3,1},{4,5},{5,4},{6,7},{7,6},{8,10},{9,11},{10,... | collective-permute-start | bytes 1572872 | tf_op jit(solution)/shard_map/ppermute | solution.py:311
  18.7 4.4 %collective-permute-start.8 = (bf16[256,128]{1,0:T(8,128)(2,1)S(1)}, bf16[256,128]{1,0:T(8,128)(2,1)S(1)}, u32[]{:S(2)}, u32[]{:S(2)}) collective-permute-start(bf16[256,128]{1,0:T(8,128)(2,1)S(1)} %get-tuple-element.40), channel_id=1, source_target_pairs={{0,8},{4,12},{8,0},{12,4},{16,24},{20,28},{24,16},{28,20},{1,9},{5... | collective-permute-start | bytes 196616 | tf_op jit(solution)/shard_map/ppermute | solution.py:302
  20.4 6.9 %collective-permute-start.9 = (bf16[256,128]{1,0:T(8,128)(2,1)S(1)}, bf16[256,128]{1,0:T(8,128)(2,1)S(1)}, u32[]{:S(2)}, u32[]{:S(2)}) collective-permute-start(bf16[256,128]{1,0:T(8,128)(2,1)S(1)} %get-tuple-element.41), channel_id=1, source_target_pairs={{0,16},{4,20},{8,24},{12,28},{16,0},{20,4},{24,8},{28,12},{1,17},{... | collective-permute-start | bytes 196616 | tf_op jit(solution)/shard_map/ppermute | solution.py:302
  23.0 6.2 %collective-permute-start.10 = (bf16[256,128]{1,0:T(8,128)(2,1)S(1)}, bf16[256,128]{1,0:T(8,128)(2,1)S(1)}, u32[]{:S(2)}, u32[]{:S(2)}) collective-permute-start(bf16[256,128]{1,0:T(8,128)(2,1)S(1)} %get-tuple-element.42), channel_id=1, source_target_pairs={{0,24},{4,28},{8,16},{12,20},{16,8},{20,12},{24,0},{28,4},{1,25},{... | collective-permute-start | bytes 196616 | tf_op jit(solution)/shard_map/ppermute | solution.py:302
  23.1 7.4 %collective-permute-start = (bf16[256,128]{1,0:T(8,128)(2,1)S(1)}, bf16[256,128]{1,0:T(8,128)(2,1)S(1)}, u32[]{:S(2)}, u32[]{:S(2)}) collective-permute-start(bf16[256,128]{1,0:T(8,128)(2,1)S(1)} %get-tuple-element.29), channel_id=1, source_target_pairs={{0,8},{4,12},{8,0},{12,4},{16,24},{20,28},{24,16},{28,20},{1,9},{5... | collective-permute-start | bytes 196616 | tf_op jit(solution)/shard_map/ppermute | solution.py:302
  27.3 5.7 %collective-permute-start.1 = (bf16[256,128]{1,0:T(8,128)(2,1)S(1)}, bf16[256,128]{1,0:T(8,128)(2,1)S(1)}, u32[]{:S(2)}, u32[]{:S(2)}) collective-permute-start(bf16[256,128]{1,0:T(8,128)(2,1)S(1)} %get-tuple-element.30), channel_id=1, source_target_pairs={{0,16},{4,20},{8,24},{12,28},{16,0},{20,4},{24,8},{28,12},{1,17},{... | collective-permute-start | bytes 196616 | tf_op jit(solution)/shard_map/ppermute | solution.py:302
  29.2 6.1 %collective-permute-start.2 = (bf16[256,128]{1,0:T(8,128)(2,1)S(1)}, bf16[256,128]{1,0:T(8,128)(2,1)S(1)}, u32[]{:S(2)}, u32[]{:S(2)}) collective-permute-start(bf16[256,128]{1,0:T(8,128)(2,1)S(1)} %get-tuple-element.31), channel_id=1, source_target_pairs={{0,24},{4,28},{8,16},{12,20},{16,8},{20,12},{24,0},{28,4},{1,25},{... | collective-permute-start | bytes 196616 | tf_op jit(solution)/shard_map/ppermute | solution.py:302
  30.6 6.2 %collective-permute-start.11 = (bf16[4,256,128]{2,1,0:T(8,128)(2,1)S(1)}, bf16[4,256,128]{2,1,0:T(8,128)(2,1)S(1)}, u32[]{:S(2)}, u32[]{:S(2)}) collective-permute-start(bf16[4,256,128]{2,1,0:T(8,128)(2,1)S(1)} %shard_map.105), channel_id=1, source_target_pairs={{0,4},{4,0},{8,12},{12,8},{16,20},{20,16},{24,28},{28,24},{1,5},{5... | collective-permute-start | bytes 786440 | tf_op jit(solution)/shard_map/ppermute | solution.py:302
  35.3 2.7 %collective-permute-start.3 = (bf16[4,256,128]{2,1,0:T(8,128)(2,1)S(1)}, bf16[4,256,128]{2,1,0:T(8,128)(2,1)S(1)}, u32[]{:S(2)}, u32[]{:S(2)}) collective-permute-start(bf16[4,256,128]{2,1,0:T(8,128)(2,1)S(1)} %shard_map.101), channel_id=1, source_target_pairs={{0,4},{4,0},{8,12},{12,8},{16,20},{20,16},{24,28},{28,24},{1,5},{5... | collective-permute-start | bytes 786440 | tf_op jit(solution)/shard_map/ppermute | solution.py:302
  35.4 24.7 %collective-permute-start.19 = (bf16[128,2048]{1,0:T(8,128)(2,1)S(1)}, bf16[128,2048]{1,0:T(8,128)(2,1)S(1)}, u32[]{:S(2)}, u32[]{:S(2)}) collective-permute-start(bf16[128,2048]{1,0:T(8,128)(2,1)S(1)} %collective-permute-done.16.refs_10_), channel_id=1, source_target_pairs={{0,4},{4,0},{8,12},{12,8},{16,20},{20,16},{24,28},{28,24},{1,5},{5... | collective-permute-start | bytes 1572872 | tf_op jit(solution)/shard_map/ppermute | solution.py:302
  35.9 24.2 %collective-permute-start.20 = (bf16[128,2048]{1,0:T(8,128)(2,1)S(1)}, bf16[128,2048]{1,0:T(8,128)(2,1)S(1)}, u32[]{:S(2)}, u32[]{:S(2)}) collective-permute-start(bf16[128,2048]{1,0:T(8,128)(2,1)S(1)} %collective-permute-done.17.refs_11_), channel_id=1, source_target_pairs={{0,4},{4,0},{8,12},{12,8},{16,20},{20,16},{24,28},{28,24},{1,5},{5... | collective-permute-start | bytes 1572872 | tf_op jit(solution)/shard_map/ppermute | solution.py:302
  36.0 24.1 %collective-permute-start.21 = (bf16[128,2048]{1,0:T(8,128)(2,1)S(1)}, bf16[128,2048]{1,0:T(8,128)(2,1)S(1)}, u32[]{:S(2)}, u32[]{:S(2)}) collective-permute-start(bf16[128,2048]{1,0:T(8,128)(2,1)S(1)} %collective-permute-done.18.refs_12_), channel_id=1, source_target_pairs={{0,4},{4,0},{8,12},{12,8},{16,20},{20,16},{24,28},{28,24},{1,5},{5... | collective-permute-start | bytes 1572872 | tf_op jit(solution)/shard_map/ppermute | solution.py:302
  36.7 17.6 %copy-start = (bf16[1,256,2048]{2,1,0:T(8,128)(2,1)S(1)}, bf16[1,256,2048]{2,1,0:T(8,128)(2,1)}, u32[]{:S(2)}) copy-start(bf16[1,256,2048]{2,1,0:T(8,128)(2,1)} %param.11) | copy-start | bytes 3145732
  36.7 17.6 %copy-start.5 = (bf16[128,256]{1,0:T(8,128)(2,1)S(1)}, bf16[128,256]{1,0:T(8,128)(2,1)}, u32[]{:S(2)}) copy-start(bf16[128,256]{1,0:T(8,128)(2,1)} %constant.18.clone.refs_6_) | copy-start | bytes 196612
  36.8 17.6 %copy-start.6 = (bf16[128,256]{1,0:T(8,128)(2,1)S(1)}, bf16[128,256]{1,0:T(8,128)(2,1)}, u32[]{:S(2)}) copy-start(bf16[128,256]{1,0:T(8,128)(2,1)} %constant.17.clone.refs_5_) | copy-start | bytes 196612
  37.9 5.4 %collective-permute-start.12 = (bf16[2,128,128]{2,1,0:T(8,128)(2,1)S(1)}, bf16[2,128,128]{2,1,0:T(8,128)(2,1)S(1)}, u32[]{:S(2)}, u32[]{:S(2)}) collective-permute-start(bf16[2,128,128]{2,1,0:T(8,128)(2,1)S(1)} %get-tuple-element.44), channel_id=1, source_target_pairs={{0,8},{4,12},{8,0},{12,4},{16,24},{20,28},{24,16},{28,20},{1,9},{5... | collective-permute-start | bytes 196616 | tf_op jit(solution)/shard_map/ppermute | solution.py:302
  38.0 22.1 %copy-start.3 = (bf16[128,256]{1,0:T(8,128)(2,1)S(1)}, bf16[128,256]{1,0:T(8,128)(2,1)}, u32[]{:S(2)}) copy-start(bf16[128,256]{1,0:T(8,128)(2,1)} %constant.20.clone.refs_5_) | copy-start | bytes 196612
  38.0 22.1 %copy-start.4 = (bf16[128,256]{1,0:T(8,128)(2,1)S(1)}, bf16[128,256]{1,0:T(8,128)(2,1)}, u32[]{:S(2)}) copy-start(bf16[128,256]{1,0:T(8,128)(2,1)} %constant.19.clone.refs_4_) | copy-start | bytes 196612
  38.0 6.7 %collective-permute-start.13 = (bf16[2,128,128]{2,1,0:T(8,128)(2,1)S(1)}, bf16[2,128,128]{2,1,0:T(8,128)(2,1)S(1)}, u32[]{:S(2)}, u32[]{:S(2)}) collective-permute-start(bf16[2,128,128]{2,1,0:T(8,128)(2,1)S(1)} %get-tuple-element.45), channel_id=1, source_target_pairs={{0,16},{4,20},{8,24},{12,28},{16,0},{20,4},{24,8},{28,12},{1,17},{... | collective-permute-start | bytes 196616 | tf_op jit(solution)/shard_map/ppermute | solution.py:302
  43.3 6.1 %collective-permute-start.14 = (bf16[2,128,128]{2,1,0:T(8,128)(2,1)S(1)}, bf16[2,128,128]{2,1,0:T(8,128)(2,1)S(1)}, u32[]{:S(2)}, u32[]{:S(2)}) collective-permute-start(bf16[2,128,128]{2,1,0:T(8,128)(2,1)S(1)} %get-tuple-element.46), channel_id=1, source_target_pairs={{0,24},{4,28},{8,16},{12,20},{16,8},{20,12},{24,0},{28,4},{1,25},{... | collective-permute-start | bytes 196616 | tf_op jit(solution)/shard_map/ppermute | solution.py:302
  44.7 4.7 %collective-permute-start.4 = (bf16[4,128,128]{2,1,0:T(8,128)(2,1)S(1)}, bf16[4,128,128]{2,1,0:T(8,128)(2,1)S(1)}, u32[]{:S(2)}, u32[]{:S(2)}) collective-permute-start(bf16[4,128,128]{2,1,0:T(8,128)(2,1)S(1)} %get-tuple-element.34), channel_id=1, source_target_pairs={{0,4},{4,0},{8,12},{12,8},{16,20},{20,16},{24,28},{28,24},{1,5},{5... | collective-permute-start | bytes 393224 | tf_op jit(solution)/shard_map/ppermute | solution.py:302
  49.3 1.4 %collective-permute-start.15 = (bf16[4,128,128]{2,1,0:T(8,128)(2,1)S(1)}, bf16[4,128,128]{2,1,0:T(8,128)(2,1)S(1)}, u32[]{:S(2)}, u32[]{:S(2)}) collective-permute-start(bf16[4,128,128]{2,1,0:T(8,128)(2,1)S(1)} %shard_map.107), channel_id=1, source_target_pairs={{0,4},{4,0},{8,12},{12,8},{16,20},{20,16},{24,28},{28,24},{1,5},{5... | collective-permute-start | bytes 393224 | tf_op jit(solution)/shard_map/ppermute | solution.py:302
  49.4 4.5 %collective-permute-start.5 = (bf16[2,128,128]{2,1,0:T(8,128)(2,1)S(1)}, bf16[2,128,128]{2,1,0:T(8,128)(2,1)S(1)}, u32[]{:S(2)}, u32[]{:S(2)}) collective-permute-start(bf16[2,128,128]{2,1,0:T(8,128)(2,1)S(1)} %get-tuple-element.36), channel_id=1, source_target_pairs={{0,8},{4,12},{8,0},{12,4},{16,24},{20,28},{24,16},{28,20},{1,9},{5... | collective-permute-start | bytes 196616 | tf_op jit(solution)/shard_map/ppermute | solution.py:302
  50.7 6.8 %collective-permute-start.6 = (bf16[2,128,128]{2,1,0:T(8,128)(2,1)S(1)}, bf16[2,128,128]{2,1,0:T(8,128)(2,1)S(1)}, u32[]{:S(2)}, u32[]{:S(2)}) collective-permute-start(bf16[2,128,128]{2,1,0:T(8,128)(2,1)S(1)} %get-tuple-element.37), channel_id=1, source_target_pairs={{0,16},{4,20},{8,24},{12,28},{16,0},{20,4},{24,8},{28,12},{1,17},{... | collective-permute-start | bytes 196616 | tf_op jit(solution)/shard_map/ppermute | solution.py:302
  54.0 6.1 %collective-permute-start.7 = (bf16[2,128,128]{2,1,0:T(8,128)(2,1)S(1)}, bf16[2,128,128]{2,1,0:T(8,128)(2,1)S(1)}, u32[]{:S(2)}, u32[]{:S(2)}) collective-permute-start(bf16[2,128,128]{2,1,0:T(8,128)(2,1)S(1)} %get-tuple-element.38), channel_id=1, source_target_pairs={{0,24},{4,28},{8,16},{12,20},{16,8},{20,12},{24,0},{28,4},{1,25},{... | collective-permute-start | bytes 196616 | tf_op jit(solution)/shard_map/ppermute | solution.py:302

commit v6 on v5

--- a/solution.py
+++ b/solution.py
@@ -12,6 +12,7 @@
 
 GROUP = 256
 CHUNKS = 2
+NEAR = 1
 MIB = 1 << 20
 
 
@@ -62,12 +63,12 @@
 
 def pick_kernel(chips, fast, *refs):
     x_ref, w_ref, narrow_ref = refs[:3]
-    outs = [refs[3 + q * chips : 3 + (q + 1) * chips] for q in range(CHUNKS)]
-    narrow, *halves = refs[3 + CHUNKS * chips : -3]
+    outs = refs[3 : 3 + CHUNKS * chips - 1]
+    narrow, *halves = refs[2 + CHUNKS * chips : -3]
     tokens, x_sems, w_sems = refs[-3:]
     row = lax.axis_index("row")
     core, chip = row % 2, row // 2
-    lanes = outs[0][0].shape[1]
+    lanes = outs[0].shape[1]
     pairs = lanes // 2
     chips_per_group = GROUP // (CHUNKS * lanes)
     loads = []
@@ -99,7 +100,11 @@
         loads[zs].wait()
         got = jnp.dot(tokens[zs], choose, preferred_element_type=jnp.float32).astype(jnp.bfloat16)
         for q in range(CHUNKS):
-            outs[q][zs][...] = got[:, q * lanes : (q + 1) * lanes]
+            piece = got[:, q * lanes : (q + 1) * lanes]
+            if zs == NEAR:
+                outs[NEAR][q] = piece
+            else:
+                outs[zs + q * (chips - (zs > NEAR))][...] = piece
     for fetch in fetches:
         fetch.wait()
 
@@ -109,9 +114,9 @@
         out[i] = jnp.broadcast_to(narrow[:, i : i + 1], out.shape[1:])
 
 
-def stack_kernel(*refs):
+def stack_kernel(q, *refs):
     for zs, piece in enumerate(refs[:-1]):
-        refs[-1][zs] = piece[...]
+        refs[-1][zs] = piece[q] if zs == NEAR else piece[...]
 
 
 def complex_dft(values):
@@ -140,6 +145,9 @@
     mine, theirs = refs[:chips], refs[chips]
     table_hi, table_lo, twist = refs[chips + 1 : chips + 4]
     *outs, folded, turned_z, spect = refs[chips + 4 :]
+    if q == 1:
+        near_give, *outs = outs
+        outs[1][chips] = near_give[...]
     inner, lanes = mine[0].shape
     pairs = lanes // 2
     row = lax.axis_index("row")
@@ -149,7 +157,7 @@
     odd_core = core == 1
     sign = jnp.where(odd_core, -1.0, 1.0).astype(jnp.float32)
     upper = row >= half
-    near, far = jnp.where(upper, sign, 1.0), jnp.where(upper, 1.0, sign)
+    here, away = jnp.where(upper, sign, 1.0), jnp.where(upper, 1.0, sign)
 
     lane = lax.broadcasted_iota(jnp.int32, (2 * lanes, lanes), 1)
     line = lax.broadcasted_iota(jnp.int32, (2 * lanes, lanes), 0)
@@ -159,13 +167,15 @@
     alone = ((lane == 0) | (lane == pairs)) & first
     own = jnp.where((lane < pairs) | lone_high, 1.0, -1.0)
     other = jnp.where(alone, 0.0, 1.0)
-    side = jnp.where(line < lanes, near, far)
+    side = jnp.where(line < lanes, here, away)
     there = line % lanes
     entry = jnp.where(there == lane, own, jnp.where(there == (lane + pairs) % lanes, other, 0.0))
     fold = (entry * side).astype(jnp.bfloat16)
 
     def block(s):
-        return mine[s // 2][...] if s % 2 == 0 else theirs[s // 2]
+        if s % 2 == 1:
+            return theirs[s // 2]
+        return mine[NEAR][q] if s // 2 == NEAR else mine[s // 2][...]
 
     for s in range(half):
         both = jnp.concatenate([block(s), block(s ^ half)], axis=1)
@@ -211,10 +221,12 @@
             for j in range(half):
                 piece = spect[j, pl.ds(pl.multiple_of(dest * per, per), per), :]
                 lines = slice(j * per, (j + 1) * per)
-                if q == 0:
-                    outs[zs][rel, lines, :] = piece.astype(jnp.bfloat16)
+                if q == 1:
+                    outs[rel][zs, lines, :] = piece.astype(jnp.bfloat16)
+                elif zs == NEAR:
+                    outs[chips - 1 + rel][lines, :] = piece.astype(jnp.bfloat16)
                 else:
-                    outs[rel][zs, lines, :] = piece.astype(jnp.bfloat16)
+                    outs[zs - (zs > NEAR)][rel, lines, :] = piece.astype(jnp.bfloat16)
 
 
 def order_rows(rows, count):
@@ -232,32 +244,39 @@
         out[zs] = ref[1]
 
 
-def join_kernel(keep, got, *outs):
+def join_kernel(keep, got, near_keep, *outs):
     for zs, out in enumerate(outs):
         out[0] = keep[zs]
         out[1] = got[zs]
-
-
-def channel_part(order, pieces, feat_hi, feat_lo):
-    lanes = feat_hi.shape[0]
+    outs[NEAR][2] = near_keep[...]
+    outs[NEAR][3] = got[len(outs)]
+
+
+def in_order(order, pieces):
+    lanes = pieces[0][0].shape[1]
     got = jnp.concatenate([jnp.concatenate(piece, axis=0) for piece in pieces], axis=1)
     got = jnp.dot(order, got, preferred_element_type=jnp.float32).astype(jnp.bfloat16)
-    parts = []
-    for zs in range(len(pieces)):
-        piece = got[:, zs * lanes : (zs + 1) * lanes]
-        part = jnp.dot(piece, feat_hi, preferred_element_type=jnp.float32)
-        parts.append(part + jnp.dot(piece, feat_lo, preferred_element_type=jnp.float32))
-    return parts
+    return [got[:, i * lanes : (i + 1) * lanes] for i in range(len(pieces))]
+
+
+def channel_part(piece, feat_hi, feat_lo):
+    part = jnp.dot(piece, feat_hi, preferred_element_type=jnp.float32)
+    return part + jnp.dot(piece, feat_lo, preferred_element_type=jnp.float32)
+
+
+def all_but_near(chips):
+    return [zs for zs in range(chips) if zs != NEAR]
 
 
 def prepare_kernel(rows, *refs):
     chips = rows // 2
-    mine, theirs, feat_hi, feat_lo, gate_ref = refs[:chips], *refs[chips : chips + 4]
-    spect, opened = refs[chips + 4 :]
+    far = all_but_near(chips)
+    mine, theirs, feat_hi, feat_lo, gate_ref = refs[: chips - 1], *refs[chips - 1 : chips + 3]
+    spect, opened = refs[chips + 3 :]
     order = order_rows(rows, gate_ref.shape[0])
-    pieces = [(ref[0], theirs[zs]) for zs, ref in enumerate(mine)]
-    for zs, part in enumerate(channel_part(order, pieces, feat_hi[...], feat_lo[...])):
-        spect[zs] = part
+    pieces = [(ref[0], theirs[i]) for i, ref in enumerate(mine)]
+    for zs, piece in zip(far, in_order(order, pieces)):
+        spect[zs] = channel_part(piece, feat_hi[...], feat_lo[...])
     for start in range(0, gate_ref.shape[1], GROUP):
         cols = slice(start, start + GROUP)
         opened[:, cols] = jax.nn.sigmoid(gate_ref[:, cols].astype(jnp.float32))
@@ -272,9 +291,14 @@
     row, col = lax.axis_index("row"), lax.axis_index("col")
     core, chip = row % 2, row // 2
     order = order_rows(rows, count)
-    pieces = [(ref[0], ref[1]) for ref in mine]
-    for zs, part in enumerate(channel_part(order, pieces, feat_hi[...], feat_lo[...])):
-        whole = (part + spect[zs]).astype(jnp.bfloat16)
+    pieces = [(ref[0], ref[1]) for ref in mine] + [(mine[NEAR][2], mine[NEAR][3])]
+    *late, near_early = in_order(order, pieces)
+    for zs, piece in enumerate(late):
+        if zs == NEAR:
+            early = channel_part(near_early, feat_hi[0], feat_lo[0])
+        else:
+            early = spect[zs]
+        whole = (channel_part(piece, feat_hi[1], feat_lo[1]) + early).astype(jnp.bfloat16)
         for h in range(2):
             spot = pl.ds(pl.multiple_of((core ^ h) * half, half), half)
             lhs[zs, :, spot] = whole[:, h * half : (h + 1) * half]
@@ -316,10 +340,12 @@
 
 
 def across_chips(pieces, rows):
-    chips = rows // 2
-    got = [pieces[0]] + [None] * (chips - 1)
-    for zs in send_order(chips):
-        got[zs] = swap(pieces[zs], "row", rows, 2 * zs)
+    got = dict(pieces)
+    for zs in send_order(rows // 2):
+        if zs in pieces and zs != NEAR:
+            got[zs] = swap(pieces[zs], "row", rows, 2 * zs)
+    if NEAR in pieces:
+        got[NEAR] = swap(pieces[NEAR], "row", rows, 2 * NEAR)
     return got
 
 
@@ -345,11 +371,13 @@
     half_w = jax.ShapeDtypeStruct((GROUP // 2, width), bf)
     picked = pl.pallas_call(
         functools.partial(pick_kernel, chips, fast),
-        out_shape=[jax.ShapeDtypeStruct((count, lanes), bf)] * (CHUNKS * chips)
+        out_shape=[jax.ShapeDtypeStruct((count, lanes), bf)]
+        + [jax.ShapeDtypeStruct((CHUNKS, count, lanes), bf)]
+        + [jax.ShapeDtypeStruct((count, lanes), bf)] * (CHUNKS * (chips - 1) - 1)
         + [jax.ShapeDtypeStruct((count, rows), jnp.float32)]
         + [half_w] * (2 * fast),
         in_specs=[pl.BlockSpec(memory_space=pltpu.HBM)] * 3,
-        out_specs=[pl.BlockSpec(memory_space=pltpu.VMEM)] * (CHUNKS * chips + 1 + 2 * fast),
+        out_specs=[pl.BlockSpec(memory_space=pltpu.VMEM)] * (CHUNKS * chips + 2 * fast),
         scratch_shapes=[
             pltpu.VMEM((chips, count, GROUP), bf),
             pltpu.SemaphoreType.DMA((chips,)),
@@ -360,10 +388,15 @@
             flops=2 * count * GROUP * features, bytes_accessed=MIB, transcendentals=0
         ),
     )(*(pltpu.with_memory_space_constraint(v, pltpu.HBM) for v in (tokens, w_proj, narrow)))
-    arrived = [across_chips(picked[q * chips : (q + 1) * chips], rows) for q in range(CHUNKS)]
+    far = all_but_near(chips)
+    first = across_chips(dict(enumerate(picked[:chips])), rows)
+    second = across_chips(dict(zip(far, picked[chips:])), rows)
+    arrived = [[first[zs] for zs in range(chips)]]
+    arrived.append([{**second, NEAR: first[NEAR]}[zs] for zs in range(chips)])
+    narrow_own, *halves = picked[2 * chips - 1 :]
 
     if fast:
-        mine, rest = picked[CHUNKS * chips + 1 :]
+        mine, rest = halves
         w_a = turn_swap(mine, rows, n_col, (1, 2))
         w_b = turn_swap(mine, rows, n_col, (2, 1))
         w_c = turn_swap(w_a, rows, n_col, (2, 1))
@@ -374,20 +407,28 @@
     lines = half * (count // rows)
     piece = jax.ShapeDtypeStruct((2, lines, lanes), bf)
     small = (count * features // 4, count * features)
-    stacked = jax.ShapeDtypeStruct((chips, lines, lanes), bf)
+
+    def stacked(n):
+        return jax.ShapeDtypeStruct((n, lines, lanes), bf)
+
     twist = vmem_call(
         twist_kernel, jax.ShapeDtypeStruct((rows, count, lanes), jnp.float32), [], *small
-    )(picked[CHUNKS * chips])
+    )(narrow_own)
+    line = jax.ShapeDtypeStruct((lines, lanes), bf)
+    made = ([piece] * (chips - 1) + [line] * 2, [stacked(chips), stacked(chips + 1)])
     sent = []
     for q in range(CHUNKS):
         stack = vmem_call(
-            stack_kernel, jax.ShapeDtypeStruct((chips, count, lanes), bf), [], *small
+            functools.partial(stack_kernel, q),
+            jax.ShapeDtypeStruct((chips, count, lanes), bf),
+            [],
+            *small,
         )(*arrived[q])
         theirs = swap(stack, "row", rows, 1)
         sent.append(
             vmem_call(
                 functools.partial(position_kernel, rows, q),
-                [piece] * chips if q == 0 else [stacked] * 2,
+                made[q],
                 [
                     pltpu.VMEM((half, count, lanes), jnp.float32),
                     pltpu.VMEM((2 * count, half * lanes), bf),
@@ -395,15 +436,19 @@
                 ],
                 8 * count * count * half * lanes,
                 rows * count * lanes * 4,
-            )(*arrived[q], theirs, table_hi, table_lo, twist)
+            )(*arrived[q], theirs, table_hi, table_lo, twist, *(sent[0][chips:] if q else ()))
         )
-    early = across_chips(sent[0], rows)
-    give = vmem_call(give_kernel, stacked, [], *small)(*early)
+    early = across_chips(dict(zip(far, sent[0])), rows)
+    early = [early[zs] for zs in far]
+    give = vmem_call(give_kernel, stacked(chips - 1), [], *small)(*early)
     early.append(swap(give, "row", rows, 1))
     keep, give = sent[1]
     got = swap(give, "row", rows, 1)
-    joined = vmem_call(join_kernel, [piece] * chips, [], *small)(keep, got)
-    late = across_chips(joined, rows)
+    joined = vmem_call(
+        join_kernel, [stacked(4 if zs == NEAR else 2) for zs in range(chips)], [], *small
+    )(keep, got, sent[0][chips - 1])
+    late = across_chips(dict(enumerate(joined)), rows)
+    late = [late[zs] for zs in range(chips)]
     if fast:
         spect, opened = vmem_call(
             functools.partial(prepare_kernel, rows),
@@ -431,7 +476,7 @@
                 bytes_accessed=2 * features * width,
                 transcendentals=0,
             ),
-        )(*late, feat_hi[1], feat_lo[1], spect, opened, mine, rest, w_a, w_b, w_c, *others)
+        )(*late, feat_hi, feat_lo, spect, opened, mine, rest, w_a, w_b, w_c, *others)
 
     weights = lax.all_gather(w_proj, "col", axis=0, tiled=True).reshape(-1, GROUP, width)
     order = order_rows(rows, count)
@@ -442,7 +487,8 @@
     here = chip ^ jnp.arange(chips)
     for q in range(CHUNKS):
         if q == 0:
-            parts = [(early[zs][0], early[chips][zs]) for zs in range(chips)]
+            parts = [(early[i][0], early[-1][i]) for i in range(chips - 1)]
+            parts.insert(NEAR, (late[NEAR][2], late[NEAR][3]))
         else:
             parts = [(ref[0], ref[1]) for ref in late]
         got = jnp.stack([jnp.concatenate(pair, axis=0) for pair in parts])[here]

time: 62.9 us -> 65.4 us (1.040)
  starting transfers between devices: 20 us -> 21.9 us
    ppermute x19 -> x17, starting transfers between devices: 13.9 us -> 15.8 us  [swap(): return lax.ppermute(value, axis, [(i, i ^ bit) for i in range(size)])]
    ppermute x19 -> x17, waiting for transfers between devices: 23.9 us -> 24.5 us  [swap(): return lax.ppermute(value, axis, [(i, i ^ bit) for i in range(size)])]
  transfers between devices with their start and end apart: 22 -> 20, of which waited for: 11 -> 10; matrix products, arithmetic and copies ran while one was open for 0% -> 0% of each run, Pallas kernels for 5% -> 5%
where the time goes in v6:
time: 65.4 us; the launch traced here: 65.3 us
  waiting for transfers between devices  35.2 us (54%)
  starting transfers between devices  21.9 us (33%)
  Pallas kernels  7.94 us (12%)
    ppermute x17, waiting for transfers between devices, swap(): return lax.ppermute(value, axis, [(i, i ^ bit) for i in range(size)])  24.5 us
    ppermute x17, starting transfers between devices, swap(): return lax.ppermute(value, axis, [(i, i ^ bit) for i in range(size)])  15.8 us
    ppermute x3, waiting for transfers between devices, turn_swap(): return lax.ppermute(value, ('row', 'col'), turn)  10.7 us
    ppermute x3, starting transfers between devices, turn_swap(): return lax.ppermute(value, ('row', 'col'), turn)  6.11 us
    pallas_call x1, Pallas kernels, program(): pl.pallas_call(functools.partial(final_kernel, rows), out_shape=jax.Shape...  2.77 us
    pallas_call x2, Pallas kernels, program(): vmem_call(functools.partial(position_kernel, rows, q), made[q], [pltpu.VM...  2.15 us
    pallas_call x1, Pallas kernels, program(): pl.pallas_call(functools.partial(pick_kernel, chips, fast), out_shape=[ja...  1.89 us
  transfers between devices with their start and end apart: 20, of which 10 were waited for; matrix products, arithmetic and copies ran while one was open for 0% of the time, Pallas kernels for 5%

profile of v6, /device:TPU:0, one launch (start us, length us, event | category | flops | bytes accessed | tf_op | source)
XLA Modules:
  0.0 65.3 jit_solution(3084841512273424402)
XLA Ops:
  0.0 1.9 %shard_map.100 = (bf16[256,128]{1,0:T(8,128)(2,1)S(1)}, bf16[2,256,128]{2,1,0:T(8,128)(2,1)S(1)}, bf16[256,128]{1,0:T(8,128)(2,1)S(1)}, bf16[256,128]{1,0:T(8,12...) custom-call(bf16[256,1024]{1,0:T(8,128)(2,1)} %bitcast.4, ...), custom_call_target="tpu_custom_call" | custom-call | flops 134217728 | bytes 1048576 | tf_op jit(solution)/shard_map/pallas_call | solution.py:372
  1.9 3.0 %collective-permute-start.14 = (bf16[128,2048]{1,0:T(8,128)(2,1)S(1)}, bf16[128,2048]{1,0:T(8,128)(2,1)S(1)}, u32[]{:S(2)}, u32[]{:S(2)}) collective-permute-start(bf16[128,2048]{1,0:T(8,128)(2,1)S(1)} %get-tuple-element.49.refs_8_), channel_id=1, source_target_pairs={{0,1},{1,0},{2,3},{3,2},{4,6},{5,7},{6,4},{7,5},{8,9},{9,8},{10,11... | collective-permute-start | bytes 1572872 | tf_op jit(solution)/shard_map/ppermute | solution.py:335
  4.9 1.5 %collective-permute-start.15 = (bf16[128,2048]{1,0:T(8,128)(2,1)S(1)}, bf16[128,2048]{1,0:T(8,128)(2,1)S(1)}, u32[]{:S(2)}, u32[]{:S(2)}) collective-permute-start(bf16[128,2048]{1,0:T(8,128)(2,1)S(1)} %get-tuple-element.49.refs_8_), channel_id=1, source_target_pairs={{0,2},{1,3},{2,0},{3,1},{4,5},{5,4},{6,7},{7,6},{8,10},{9,11},{10,... | collective-permute-start | bytes 1572872 | tf_op jit(solution)/shard_map/ppermute | solution.py:335
  6.5 10.7 %collective-permute-done.14.refs_10_ = bf16[128,2048]{1,0:T(8,128)(2,1)S(1)} collective-permute-done((bf16[128,2048]{1,0:T(8,128)(2,1)S(1)}, bf16[128,2048]{1,0:T(8,128)(2,1)S(1)}, u32[]{:S(2)}, u32[]{:S(2)}) %collective-permute-start.14) | collective-permute-done | bytes 524320 | tf_op jit(solution)/shard_map/ppermute | solution.py:335
  17.1 1.6 %collective-permute-start.16 = (bf16[128,2048]{1,0:T(8,128)(2,1)S(1)}, bf16[128,2048]{1,0:T(8,128)(2,1)S(1)}, u32[]{:S(2)}, u32[]{:S(2)}) collective-permute-start(bf16[128,2048]{1,0:T(8,128)(2,1)S(1)} %collective-permute-done.14.refs_10_), channel_id=1, source_target_pairs={{0,2},{1,3},{2,0},{3,1},{4,5},{5,4},{6,7},{7,6},{8,10},{9,11},{10,... | collective-permute-start | bytes 1572872 | tf_op jit(solution)/shard_map/ppermute | solution.py:335
  18.7 1.7 %collective-permute-start = (bf16[2,256,128]{2,1,0:T(8,128)(2,1)S(1)}, bf16[2,256,128]{2,1,0:T(8,128)(2,1)S(1)}, u32[]{:S(2)}, u32[]{:S(2)}) collective-permute-start(bf16[2,256,128]{2,1,0:T(8,128)(2,1)S(1)} %get-tuple-element.29), channel_id=1, source_target_pairs={{0,8},{4,12},{8,0},{12,4},{16,24},{20,28},{24,16},{28,20},{1,9},{5... | collective-permute-start | bytes 393224 | tf_op jit(solution)/shard_map/ppermute | solution.py:326
  20.4 2.6 %collective-permute-start.4 = (bf16[256,128]{1,0:T(8,128)(2,1)S(1)}, bf16[256,128]{1,0:T(8,128)(2,1)S(1)}, u32[]{:S(2)}, u32[]{:S(2)}) collective-permute-start(bf16[256,128]{1,0:T(8,128)(2,1)S(1)} %get-tuple-element.34), channel_id=1, source_target_pairs={{0,16},{4,20},{8,24},{12,28},{16,0},{20,4},{24,8},{28,12},{1,17},{... | collective-permute-start | bytes 196616 | tf_op jit(solution)/shard_map/ppermute | solution.py:326
  23.0 0.1 collective-permute-start.5
  23.1 3.5 %collective-permute-done.4.refs_2_ = bf16[256,128]{1,0:T(8,128)(2,1)S(1)} collective-permute-done((bf16[256,128]{1,0:T(8,128)(2,1)S(1)}, bf16[256,128]{1,0:T(8,128)(2,1)S(1)}, u32[]{:S(2)}, u32[]{:S(2)}) %collective-permute-start.4) | collective-permute-done | bytes 65568 | tf_op jit(solution)/shard_map/ppermute | solution.py:326
  26.6 1.7 %collective-permute-start.1 = (bf16[256,128]{1,0:T(8,128)(2,1)S(1)}, bf16[256,128]{1,0:T(8,128)(2,1)S(1)}, u32[]{:S(2)}, u32[]{:S(2)}) collective-permute-start(bf16[256,128]{1,0:T(8,128)(2,1)S(1)} %get-tuple-element.30), channel_id=1, source_target_pairs={{0,16},{4,20},{8,24},{12,28},{16,0},{20,4},{24,8},{28,12},{1,17},{... | collective-permute-start | bytes 196616 | tf_op jit(solution)/shard_map/ppermute | solution.py:326
  28.3 0.8 %collective-permute-done.5.refs_3_ = bf16[256,128]{1,0:T(8,128)(2,1)S(1)} collective-permute-done((bf16[256,128]{1,0:T(8,128)(2,1)S(1)}, bf16[256,128]{1,0:T(8,128)(2,1)S(1)}, u32[]{:S(2)}, u32[]{:S(2)}) %collective-permute-start.5) | collective-permute-done | bytes 65568 | tf_op jit(solution)/shard_map/ppermute | solution.py:326
  29.1 1.6 %collective-permute-start.2 = (bf16[256,128]{1,0:T(8,128)(2,1)S(1)}, bf16[256,128]{1,0:T(8,128)(2,1)S(1)}, u32[]{:S(2)}, u32[]{:S(2)}) collective-permute-start(bf16[256,128]{1,0:T(8,128)(2,1)S(1)} %get-tuple-element.31), channel_id=1, source_target_pairs={{0,24},{4,28},{8,16},{12,20},{16,8},{20,12},{24,0},{28,4},{1,25},{... | collective-permute-start | bytes 196616 | tf_op jit(solution)/shard_map/ppermute | solution.py:326
  30.7 0.1 collective-permute-start.6
  30.8 1.1 %collective-permute-done.1.refs_2_ = bf16[256,128]{1,0:T(8,128)(2,1)S(1)} collective-permute-done((bf16[256,128]{1,0:T(8,128)(2,1)S(1)}, bf16[256,128]{1,0:T(8,128)(2,1)S(1)}, u32[]{:S(2)}, u32[]{:S(2)}) %collective-permute-start.1) | collective-permute-done | bytes 65568 | tf_op jit(solution)/shard_map/ppermute | solution.py:326
  31.9 3.3 %collective-permute-done.2.refs_3_ = bf16[256,128]{1,0:T(8,128)(2,1)S(1)} collective-permute-done((bf16[256,128]{1,0:T(8,128)(2,1)S(1)}, bf16[256,128]{1,0:T(8,128)(2,1)S(1)}, u32[]{:S(2)}, u32[]{:S(2)}) %collective-permute-start.2) | collective-permute-done | bytes 65568 | tf_op jit(solution)/shard_map/ppermute | solution.py:326
  35.3 0.5 collective-permute-start.17
  35.8 0.1 collective-permute-start.18
  35.8 0.4 collective-permute-start.19
  36.3 0.3 shard_map.102.refs_7_
  36.7 1.1 %shard_map.104 = (bf16[2,128,128]{2,1,0:T(8,128)(2,1)S(1)}, bf16[2,128,128]{2,1,0:T(8,128)(2,1)S(1)}, bf16[2,128,128]{2,1,0:T(8,128)(2,1)S(1)}, bf16[128,128]{1,0:T(8,128)(2,1)S(1)}, bf16[128,128]{1,0:T(8,128)(2,1)S(1)}) custom-call(bf16[256,128]{1,0:T(8,128)(2,1)S(1)} %get-tuple-element.33.refs_0_, bf16[2,256,128]{2,1,0:T(8,128)(2,1)S(1)} %collective-permute-done.refs_1_, ...), custom_call_target="tpu_custom_call" | custom-call | flops 268435456 | bytes 1048576 | tf_op jit(solution)/shard_map/pallas_call | solution.py:429
  37.8 1.2 %collective-permute-start.11 = (bf16[2,128,128]{2,1,0:T(8,128)(2,1)S(1)}, bf16[2,128,128]{2,1,0:T(8,128)(2,1)S(1)}, u32[]{:S(2)}, u32[]{:S(2)}) collective-permute-start(bf16[2,128,128]{2,1,0:T(8,128)(2,1)S(1)} %get-tuple-element.45), channel_id=1, source_target_pairs={{0,16},{4,20},{8,24},{12,28},{16,0},{20,4},{24,8},{28,12},{1,17},{... | collective-permute-start | bytes 196616 | tf_op jit(solution)/shard_map/ppermute | solution.py:326
  39.0 1.1 %shard_map.105 = (bf16[4,128,128]{2,1,0:T(8,128)(2,1)S(1)}, bf16[5,128,128]{2,1,0:T(8,128)(2,1)S(1)}) custom-call(bf16[256,128]{1,0:T(8,128)(2,1)S(1)} %get-tuple-element.28.refs_0_, bf16[2,256,128]{2,1,0:T(8,128)(2,1)S(1)} %collective-permute-done.refs_1_, bf16[256,128]{1,0:T(8,128)(2,1)S(1)} %collective-permute-done.1.refs_2_, ...), custom_call_target="tpu_custom_call" | custom-call | flops 268435456 | bytes 1048576 | tf_op jit(solution)/shard_map/pallas_call | solution.py:429
  40.1 3.4 %collective-permute-done.11.refs_1_ = bf16[2,128,128]{2,1,0:T(8,128)(2,1)S(1)} collective-permute-done((bf16[2,128,128]{2,1,0:T(8,128)(2,1)S(1)}, bf16[2,128,128]{2,1,0:T(8,128)(2,1)S(1)}, u32[]{:S(2)}, u32[]{:S(2)}) %collective-permute-start.11) | collective-permute-done | bytes 65568 | tf_op jit(solution)/shard_map/ppermute | solution.py:326
  43.5 2.4 %collective-permute-start.12 = (bf16[2,128,128]{2,1,0:T(8,128)(2,1)S(1)}, bf16[2,128,128]{2,1,0:T(8,128)(2,1)S(1)}, u32[]{:S(2)}, u32[]{:S(2)}) collective-permute-start(bf16[2,128,128]{2,1,0:T(8,128)(2,1)S(1)} %get-tuple-element.46), channel_id=1, source_target_pairs={{0,24},{4,28},{8,16},{12,20},{16,8},{20,12},{24,0},{28,4},{1,25},{... | collective-permute-start | bytes 196616 | tf_op jit(solution)/shard_map/ppermute | solution.py:326
  45.9 3.7 %collective-permute-done.12.refs_2_ = bf16[2,128,128]{2,1,0:T(8,128)(2,1)S(1)} collective-permute-done((bf16[2,128,128]{2,1,0:T(8,128)(2,1)S(1)}, bf16[2,128,128]{2,1,0:T(8,128)(2,1)S(1)}, u32[]{:S(2)}, u32[]{:S(2)}) %collective-permute-start.12) | collective-permute-done | bytes 65568 | tf_op jit(solution)/shard_map/ppermute | solution.py:326
  49.8 1.2 %collective-permute-done.13.refs_3_ = bf16[3,128,128]{2,1,0:T(8,128)(2,1)S(1)} collective-permute-done((bf16[3,128,128]{2,1,0:T(8,128)(2,1)S(1)}, bf16[3,128,128]{2,1,0:T(8,128)(2,1)S(1)}, u32[]{:S(2)}, u32[]{:S(2)}) %collective-permute-start.13) | collective-permute-done | bytes 98336 | tf_op jit(solution)/shard_map/ppermute | solution.py:326
  51.0 1.8 %collective-permute-start.8 = (bf16[4,128,128]{2,1,0:T(8,128)(2,1)S(1)}, bf16[4,128,128]{2,1,0:T(8,128)(2,1)S(1)}, u32[]{:S(2)}, u32[]{:S(2)}) collective-permute-start(bf16[4,128,128]{2,1,0:T(8,128)(2,1)S(1)} %get-tuple-element.41), channel_id=1, source_target_pairs={{0,8},{4,12},{8,0},{12,4},{16,24},{20,28},{24,16},{28,20},{1,9},{5... | collective-permute-start | bytes 393224 | tf_op jit(solution)/shard_map/ppermute | solution.py:326
  52.7 3.7 %collective-permute-done.9.refs_2_ = bf16[2,128,128]{2,1,0:T(8,128)(2,1)S(1)} collective-permute-done((bf16[2,128,128]{2,1,0:T(8,128)(2,1)S(1)}, bf16[2,128,128]{2,1,0:T(8,128)(2,1)S(1)}, u32[]{:S(2)}, u32[]{:S(2)}) %collective-permute-start.9) | collective-permute-done | bytes 65568 | tf_op jit(solution)/shard_map/ppermute | solution.py:326
  56.4 1.4 %collective-permute-start.10 = (bf16[2,128,128]{2,1,0:T(8,128)(2,1)S(1)}, bf16[2,128,128]{2,1,0:T(8,128)(2,1)S(1)}, u32[]{:S(2)}, u32[]{:S(2)}) collective-permute-start(bf16[2,128,128]{2,1,0:T(8,128)(2,1)S(1)} %get-tuple-element.43), channel_id=1, source_target_pairs={{0,24},{4,28},{8,16},{12,20},{16,8},{20,12},{24,0},{28,4},{1,25},{... | collective-permute-start | bytes 196616 | tf_op jit(solution)/shard_map/ppermute | solution.py:326
  57.9 0.7 %shard_map.108 = (f32[4,256,256]{2,1,0:T(8,128)S(1)}, f32[256,2048]{1,0:T(8,128)S(1)}) custom-call(bf16[2,128,128]{2,1,0:T(8,128)(2,1)S(1)} %get-tuple-element.44.refs_0_, bf16[2,128,128]{2,1,0:T(8,128)(2,1)S(1)} %collective-permute-done.11.refs_1_, bf16[2,128,128]{2,1,0:T(8,128)(2,1)S(1)} %collective-permute-done.12.refs_2_, ...), custom_call_target="tpu_custom_call" | custom-call | flops 134217728 | bytes 3145728 | tf_op jit(solution)/shard_map/pallas_call | solution.py:453
  58.6 3.9 %collective-permute-done.10.refs_3_ = bf16[2,128,128]{2,1,0:T(8,128)(2,1)S(1)} collective-permute-done((bf16[2,128,128]{2,1,0:T(8,128)(2,1)S(1)}, bf16[2,128,128]{2,1,0:T(8,128)(2,1)S(1)}, u32[]{:S(2)}, u32[]{:S(2)}) %collective-permute-start.10) | collective-permute-done | bytes 65568 | tf_op jit(solution)/shard_map/ppermute | solution.py:326
  62.5 2.8 %shard_map.109 = bf16[256,2048]{1,0:T(8,128)(2,1)} custom-call(bf16[2,128,128]{2,1,0:T(8,128)(2,1)S(1)} %get-tuple-element.40.refs_0_, bf16[4,128,128]{2,1,0:T(8,128)(2,1)S(1)} %collective-permute-done.8.refs_1_, bf16[2,128,128]{2,1,0:T(8,128)(2,1)S(1)} %collective-permute-done.9.refs_2_, bf16[2,128,128]{2,1,0:T(8,128)(2,1)S(1)} %collective-permute-done.10.refs_3_, ...), custom_call_target="tpu_custom_call" | custom-call | flops 1073741824 | bytes 4194304 | tf_op jit(solution)/shard_map/pallas_call | solution.py:463
  (32 shorter events, 0.4 us)
Async XLA Ops:
  0.0 36.7 %copy-start = (bf16[256,512]{1,0:T(8,128)(2,1)S(1)}, bf16[256,512]{1,0:T(8,128)(2,1)}, u32[]{:S(2)}) copy-start(bf16[256,512]{1,0:T(8,128)(2,1)} %constant.16.clone.refs_6_) | copy-start | bytes 786436
  0.0 36.7 %copy-start.1 = (bf16[256,512]{1,0:T(8,128)(2,1)S(1)}, bf16[256,512]{1,0:T(8,128)(2,1)}, u32[]{:S(2)}) copy-start(bf16[256,512]{1,0:T(8,128)(2,1)} %constant.15.clone.refs_5_) | copy-start | bytes 786436
  1.9 15.2 %collective-permute-start.14 = (bf16[128,2048]{1,0:T(8,128)(2,1)S(1)}, bf16[128,2048]{1,0:T(8,128)(2,1)S(1)}, u32[]{:S(2)}, u32[]{:S(2)}) collective-permute-start(bf16[128,2048]{1,0:T(8,128)(2,1)S(1)} %get-tuple-element.49.refs_8_), channel_id=1, source_target_pairs={{0,1},{1,0},{2,3},{3,2},{4,6},{5,7},{6,4},{7,5},{8,9},{9,8},{10,11... | collective-permute-start | bytes 1572872 | tf_op jit(solution)/shard_map/ppermute | solution.py:335
  4.9 30.8 %collective-permute-start.15 = (bf16[128,2048]{1,0:T(8,128)(2,1)S(1)}, bf16[128,2048]{1,0:T(8,128)(2,1)S(1)}, u32[]{:S(2)}, u32[]{:S(2)}) collective-permute-start(bf16[128,2048]{1,0:T(8,128)(2,1)S(1)} %get-tuple-element.49.refs_8_), channel_id=1, source_target_pairs={{0,2},{1,3},{2,0},{3,1},{4,5},{5,4},{6,7},{7,6},{8,10},{9,11},{10,... | collective-permute-start | bytes 1572872 | tf_op jit(solution)/shard_map/ppermute | solution.py:335
  17.1 18.7 %collective-permute-start.16 = (bf16[128,2048]{1,0:T(8,128)(2,1)S(1)}, bf16[128,2048]{1,0:T(8,128)(2,1)S(1)}, u32[]{:S(2)}, u32[]{:S(2)}) collective-permute-start(bf16[128,2048]{1,0:T(8,128)(2,1)S(1)} %collective-permute-done.14.refs_10_), channel_id=1, source_target_pairs={{0,2},{1,3},{2,0},{3,1},{4,5},{5,4},{6,7},{7,6},{8,10},{9,11},{10,... | collective-permute-start | bytes 1572872 | tf_op jit(solution)/shard_map/ppermute | solution.py:335
  18.7 12.0 %collective-permute-start = (bf16[2,256,128]{2,1,0:T(8,128)(2,1)S(1)}, bf16[2,256,128]{2,1,0:T(8,128)(2,1)S(1)}, u32[]{:S(2)}, u32[]{:S(2)}) collective-permute-start(bf16[2,256,128]{2,1,0:T(8,128)(2,1)S(1)} %get-tuple-element.29), channel_id=1, source_target_pairs={{0,8},{4,12},{8,0},{12,4},{16,24},{20,28},{24,16},{28,20},{1,9},{5... | collective-permute-start | bytes 393224 | tf_op jit(solution)/shard_map/ppermute | solution.py:326
  20.4 6.2 %collective-permute-start.4 = (bf16[256,128]{1,0:T(8,128)(2,1)S(1)}, bf16[256,128]{1,0:T(8,128)(2,1)S(1)}, u32[]{:S(2)}, u32[]{:S(2)}) collective-permute-start(bf16[256,128]{1,0:T(8,128)(2,1)S(1)} %get-tuple-element.34), channel_id=1, source_target_pairs={{0,16},{4,20},{8,24},{12,28},{16,0},{20,4},{24,8},{28,12},{1,17},{... | collective-permute-start | bytes 196616 | tf_op jit(solution)/shard_map/ppermute | solution.py:326
  23.0 6.1 %collective-permute-start.5 = (bf16[256,128]{1,0:T(8,128)(2,1)S(1)}, bf16[256,128]{1,0:T(8,128)(2,1)S(1)}, u32[]{:S(2)}, u32[]{:S(2)}) collective-permute-start(bf16[256,128]{1,0:T(8,128)(2,1)S(1)} %get-tuple-element.35), channel_id=1, source_target_pairs={{0,24},{4,28},{8,16},{12,20},{16,8},{20,12},{24,0},{28,4},{1,25},{... | collective-permute-start | bytes 196616 | tf_op jit(solution)/shard_map/ppermute | solution.py:326
  26.6 5.3 %collective-permute-start.1 = (bf16[256,128]{1,0:T(8,128)(2,1)S(1)}, bf16[256,128]{1,0:T(8,128)(2,1)S(1)}, u32[]{:S(2)}, u32[]{:S(2)}) collective-permute-start(bf16[256,128]{1,0:T(8,128)(2,1)S(1)} %get-tuple-element.30), channel_id=1, source_target_pairs={{0,16},{4,20},{8,24},{12,28},{16,0},{20,4},{24,8},{28,12},{1,17},{... | collective-permute-start | bytes 196616 | tf_op jit(solution)/shard_map/ppermute | solution.py:326
  29.1 6.1 %collective-permute-start.2 = (bf16[256,128]{1,0:T(8,128)(2,1)S(1)}, bf16[256,128]{1,0:T(8,128)(2,1)S(1)}, u32[]{:S(2)}, u32[]{:S(2)}) collective-permute-start(bf16[256,128]{1,0:T(8,128)(2,1)S(1)} %get-tuple-element.31), channel_id=1, source_target_pairs={{0,24},{4,28},{8,16},{12,20},{16,8},{20,12},{24,0},{28,4},{1,25},{... | collective-permute-start | bytes 196616 | tf_op jit(solution)/shard_map/ppermute | solution.py:326
  30.7 6.0 %collective-permute-start.6 = (bf16[4,256,128]{2,1,0:T(8,128)(2,1)S(1)}, bf16[4,256,128]{2,1,0:T(8,128)(2,1)S(1)}, u32[]{:S(2)}, u32[]{:S(2)}) collective-permute-start(bf16[4,256,128]{2,1,0:T(8,128)(2,1)S(1)} %shard_map.103), channel_id=1, source_target_pairs={{0,4},{4,0},{8,12},{12,8},{16,20},{20,16},{24,28},{28,24},{1,5},{5... | collective-permute-start | bytes 786440 | tf_op jit(solution)/shard_map/ppermute | solution.py:326
  35.2 3.8 %collective-permute-start.3 = (bf16[4,256,128]{2,1,0:T(8,128)(2,1)S(1)}, bf16[4,256,128]{2,1,0:T(8,128)(2,1)S(1)}, u32[]{:S(2)}, u32[]{:S(2)}) collective-permute-start(bf16[4,256,128]{2,1,0:T(8,128)(2,1)S(1)} %shard_map.101), channel_id=1, source_target_pairs={{0,4},{4,0},{8,12},{12,8},{16,20},{20,16},{24,28},{28,24},{1,5},{5... | collective-permute-start | bytes 786440 | tf_op jit(solution)/shard_map/ppermute | solution.py:326
  35.3 27.2 %collective-permute-start.17 = (bf16[128,2048]{1,0:T(8,128)(2,1)S(1)}, bf16[128,2048]{1,0:T(8,128)(2,1)S(1)}, u32[]{:S(2)}, u32[]{:S(2)}) collective-permute-start(bf16[128,2048]{1,0:T(8,128)(2,1)S(1)} %collective-permute-done.14.refs_10_), channel_id=1, source_target_pairs={{0,4},{4,0},{8,12},{12,8},{16,20},{20,16},{24,28},{28,24},{1,5},{5... | collective-permute-start | bytes 1572872 | tf_op jit(solution)/shard_map/ppermute | solution.py:326
  35.8 26.7 %collective-permute-start.18 = (bf16[128,2048]{1,0:T(8,128)(2,1)S(1)}, bf16[128,2048]{1,0:T(8,128)(2,1)S(1)}, u32[]{:S(2)}, u32[]{:S(2)}) collective-permute-start(bf16[128,2048]{1,0:T(8,128)(2,1)S(1)} %collective-permute-done.15.refs_11_), channel_id=1, source_target_pairs={{0,4},{4,0},{8,12},{12,8},{16,20},{20,16},{24,28},{28,24},{1,5},{5... | collective-permute-start | bytes 1572872 | tf_op jit(solution)/shard_map/ppermute | solution.py:326
  35.8 26.7 %collective-permute-start.19 = (bf16[128,2048]{1,0:T(8,128)(2,1)S(1)}, bf16[128,2048]{1,0:T(8,128)(2,1)S(1)}, u32[]{:S(2)}, u32[]{:S(2)}) collective-permute-start(bf16[128,2048]{1,0:T(8,128)(2,1)S(1)} %collective-permute-done.16.refs_12_), channel_id=1, source_target_pairs={{0,4},{4,0},{8,12},{12,8},{16,20},{20,16},{24,28},{28,24},{1,5},{5... | collective-permute-start | bytes 1572872 | tf_op jit(solution)/shard_map/ppermute | solution.py:326
  36.6 21.2 %copy-start.2 = (bf16[1,256,2048]{2,1,0:T(8,128)(2,1)S(1)}, bf16[1,256,2048]{2,1,0:T(8,128)(2,1)}, u32[]{:S(2)}) copy-start(bf16[1,256,2048]{2,1,0:T(8,128)(2,1)} %param.11) | copy-start | bytes 3145732
  36.6 21.2 %copy-start.5 = (bf16[128,256]{1,0:T(8,128)(2,1)S(1)}, bf16[128,256]{1,0:T(8,128)(2,1)}, u32[]{:S(2)}) copy-start(bf16[128,256]{1,0:T(8,128)(2,1)} %constant.18.clone.refs_5_) | copy-start | bytes 196612
  36.6 21.2 %copy-start.6 = (bf16[128,256]{1,0:T(8,128)(2,1)S(1)}, bf16[128,256]{1,0:T(8,128)(2,1)}, u32[]{:S(2)}) copy-start(bf16[128,256]{1,0:T(8,128)(2,1)} %constant.17.clone.refs_4_) | copy-start | bytes 196612
  37.8 5.7 %collective-permute-start.11 = (bf16[2,128,128]{2,1,0:T(8,128)(2,1)S(1)}, bf16[2,128,128]{2,1,0:T(8,128)(2,1)S(1)}, u32[]{:S(2)}, u32[]{:S(2)}) collective-permute-start(bf16[2,128,128]{2,1,0:T(8,128)(2,1)S(1)} %get-tuple-element.45), channel_id=1, source_target_pairs={{0,16},{4,20},{8,24},{12,28},{16,0},{20,4},{24,8},{28,12},{1,17},{... | collective-permute-start | bytes 196616 | tf_op jit(solution)/shard_map/ppermute | solution.py:326
  39.0 23.5 %copy-start.3 = (bf16[2,128,256]{2,1,0:T(8,128)(2,1)S(1)}, bf16[2,128,256]{2,1,0:T(8,128)(2,1)}, u32[]{:S(2)}) copy-start(bf16[2,128,256]{2,1,0:T(8,128)(2,1)} %constant.20.clone.refs_5_) | copy-start | bytes 393220
  39.0 23.6 %copy-start.4 = (bf16[2,128,256]{2,1,0:T(8,128)(2,1)S(1)}, bf16[2,128,256]{2,1,0:T(8,128)(2,1)}, u32[]{:S(2)}) copy-start(bf16[2,128,256]{2,1,0:T(8,128)(2,1)} %constant.19.clone.refs_4_) | copy-start | bytes 393220
  40.0 9.6 %collective-permute-start.7 = (bf16[5,128,128]{2,1,0:T(8,128)(2,1)S(1)}, bf16[5,128,128]{2,1,0:T(8,128)(2,1)S(1)}, u32[]{:S(2)}, u32[]{:S(2)}) collective-permute-start(bf16[5,128,128]{2,1,0:T(8,128)(2,1)S(1)} %get-tuple-element.38), channel_id=1, source_target_pairs={{0,4},{4,0},{8,12},{12,8},{16,20},{20,16},{24,28},{28,24},{1,5},{5... | collective-permute-start | bytes 491528 | tf_op jit(solution)/shard_map/ppermute | solution.py:326
  43.5 6.1 %collective-permute-start.12 = (bf16[2,128,128]{2,1,0:T(8,128)(2,1)S(1)}, bf16[2,128,128]{2,1,0:T(8,128)(2,1)S(1)}, u32[]{:S(2)}, u32[]{:S(2)}) collective-permute-start(bf16[2,128,128]{2,1,0:T(8,128)(2,1)S(1)} %get-tuple-element.46), channel_id=1, source_target_pairs={{0,24},{4,28},{8,16},{12,20},{16,8},{20,12},{24,0},{28,4},{1,25},{... | collective-permute-start | bytes 196616 | tf_op jit(solution)/shard_map/ppermute | solution.py:326
  49.6 1.4 %collective-permute-start.13 = (bf16[3,128,128]{2,1,0:T(8,128)(2,1)S(1)}, bf16[3,128,128]{2,1,0:T(8,128)(2,1)S(1)}, u32[]{:S(2)}, u32[]{:S(2)}) collective-permute-start(bf16[3,128,128]{2,1,0:T(8,128)(2,1)S(1)} %shard_map.107), channel_id=1, source_target_pairs={{0,4},{4,0},{8,12},{12,8},{16,20},{20,16},{24,28},{28,24},{1,5},{5... | collective-permute-start | bytes 294920 | tf_op jit(solution)/shard_map/ppermute | solution.py:326
  49.7 6.7 %collective-permute-start.9 = (bf16[2,128,128]{2,1,0:T(8,128)(2,1)S(1)}, bf16[2,128,128]{2,1,0:T(8,128)(2,1)S(1)}, u32[]{:S(2)}, u32[]{:S(2)}) collective-permute-start(bf16[2,128,128]{2,1,0:T(8,128)(2,1)S(1)} %get-tuple-element.42), channel_id=1, source_target_pairs={{0,16},{4,20},{8,24},{12,28},{16,0},{20,4},{24,8},{28,12},{1,17},{... | collective-permute-start | bytes 196616 | tf_op jit(solution)/shard_map/ppermute | solution.py:326
  51.0 11.5 %collective-permute-start.8 = (bf16[4,128,128]{2,1,0:T(8,128)(2,1)S(1)}, bf16[4,128,128]{2,1,0:T(8,128)(2,1)S(1)}, u32[]{:S(2)}, u32[]{:S(2)}) collective-permute-start(bf16[4,128,128]{2,1,0:T(8,128)(2,1)S(1)} %get-tuple-element.41), channel_id=1, source_target_pairs={{0,8},{4,12},{8,0},{12,4},{16,24},{20,28},{24,16},{28,20},{1,9},{5... | collective-permute-start | bytes 393224 | tf_op jit(solution)/shard_map/ppermute | solution.py:326
  56.4 6.1 %collective-permute-start.10 = (bf16[2,128,128]{2,1,0:T(8,128)(2,1)S(1)}, bf16[2,128,128]{2,1,0:T(8,128)(2,1)S(1)}, u32[]{:S(2)}, u32[]{:S(2)}) collective-permute-start(bf16[2,128,128]{2,1,0:T(8,128)(2,1)S(1)} %get-tuple-element.43), channel_id=1, source_target_pairs={{0,24},{4,28},{8,16},{12,20},{16,8},{20,12},{24,0},{28,4},{1,25},{... | collective-permute-start | bytes 196616 | tf_op jit(solution)/shard_map/ppermute | solution.py:326

commit v7 on v6

--- a/solution.py
+++ b/solution.py
@@ -12,6 +12,7 @@
 
 GROUP = 256
 CHUNKS = 2
+SPAN = 2
 NEAR = 1
 MIB = 1 << 20
 
@@ -65,20 +66,14 @@
     x_ref, w_ref, narrow_ref = refs[:3]
     outs = refs[3 : 3 + CHUNKS * chips - 1]
     narrow, *halves = refs[2 + CHUNKS * chips : -3]
-    tokens, x_sems, w_sems = refs[-3:]
+    tokens, x_sem, w_sems = refs[-3:]
     row = lax.axis_index("row")
     core, chip = row % 2, row // 2
     lanes = outs[0].shape[1]
     pairs = lanes // 2
     chips_per_group = GROUP // (CHUNKS * lanes)
-    loads = []
-    for zs in range(chips):
-        group = (chip ^ zs) // chips_per_group
-        columns = pl.ds(pl.multiple_of(group * GROUP, GROUP), GROUP)
-        loads.append(pltpu.make_async_copy(x_ref.at[:, columns], tokens.at[zs], x_sems.at[zs]))
-    order = [*send_order(chips), 0]
-    for zs in order:
-        loads[zs].start()
+    load = pltpu.make_async_copy(x_ref, tokens, x_sem)
+    load.start()
     fetches = [pltpu.make_async_copy(narrow_ref.at[core], narrow, w_sems.at[2])]
     fetches[0].start()
     if fast:
@@ -90,15 +85,19 @@
     src = lax.broadcasted_iota(jnp.int32, (GROUP, CHUNKS * lanes), 0)
     column = lax.broadcasted_iota(jnp.int32, (GROUP, CHUNKS * lanes), 1)
     lane, j = column % lanes, column % lanes - pairs
-    choose = None
-    for zs in order:
-        if choose is None or chips_per_group > 1:
-            part = ((chip ^ zs) % chips_per_group) * CHUNKS + column // lanes
-            mirrored = jnp.where((j == 0) & (part == 0), GROUP // 2, GROUP - pairs * part - j)
-            wanted = jnp.where(lane < pairs, pairs * part + lane, mirrored)
-            choose = (src == wanted).astype(jnp.bfloat16)
-        loads[zs].wait()
-        got = jnp.dot(tokens[zs], choose, preferred_element_type=jnp.float32).astype(jnp.bfloat16)
+
+    def chosen(zs):
+        part = ((chip ^ zs) % chips_per_group) * CHUNKS + column // lanes
+        mirrored = jnp.where((j == 0) & (part == 0), GROUP // 2, GROUP - pairs * part - j)
+        return (src == jnp.where(lane < pairs, pairs * part + lane, mirrored)).astype(jnp.bfloat16)
+
+    same = chosen(0) if chips_per_group == 1 else None
+    load.wait()
+    for zs in range(chips):
+        group = (chip ^ zs) // chips_per_group
+        block = tokens[:, pl.ds(pl.multiple_of(group * GROUP, GROUP), GROUP)]
+        choose = chosen(zs) if same is None else same
+        got = jnp.dot(block, choose, preferred_element_type=jnp.float32).astype(jnp.bfloat16)
         for q in range(CHUNKS):
             piece = got[:, q * lanes : (q + 1) * lanes]
             if zs == NEAR:
@@ -259,9 +258,9 @@
     return [got[:, i * lanes : (i + 1) * lanes] for i in range(len(pieces))]
 
 
-def channel_part(piece, feat_hi, feat_lo):
-    part = jnp.dot(piece, feat_hi, preferred_element_type=jnp.float32)
-    return part + jnp.dot(piece, feat_lo, preferred_element_type=jnp.float32)
+def channel_part(piece, feat):
+    twice = jnp.concatenate([piece, piece], axis=1)
+    return jnp.dot(twice, feat, preferred_element_type=jnp.float32)
 
 
 def all_but_near(chips):
@@ -271,12 +270,12 @@
 def prepare_kernel(rows, *refs):
     chips = rows // 2
     far = all_but_near(chips)
-    mine, theirs, feat_hi, feat_lo, gate_ref = refs[: chips - 1], *refs[chips - 1 : chips + 3]
-    spect, opened = refs[chips + 3 :]
+    mine, theirs, feat, gate_ref = refs[: chips - 1], *refs[chips - 1 : chips + 2]
+    spect, opened = refs[chips + 2 :]
     order = order_rows(rows, gate_ref.shape[0])
     pieces = [(ref[0], theirs[i]) for i, ref in enumerate(mine)]
     for zs, piece in zip(far, in_order(order, pieces)):
-        spect[zs] = channel_part(piece, feat_hi[...], feat_lo[...])
+        spect[zs] = channel_part(piece, feat[0])
     for start in range(0, gate_ref.shape[1], GROUP):
         cols = slice(start, start + GROUP)
         opened[:, cols] = jax.nn.sigmoid(gate_ref[:, cols].astype(jnp.float32))
@@ -284,8 +283,8 @@
 
 def final_kernel(rows, *refs):
     chips = rows // 2
-    mine, feat_hi, feat_lo, spect, opened = refs[:chips], *refs[chips : chips + 4]
-    w_mine, w_rest, w_a, w_b, w_c, v_a, v_b, v_c, out_ref, lhs, result, sems = refs[chips + 4 :]
+    mine, feat, spect, opened = refs[:chips], *refs[chips : chips + 3]
+    w_mine, w_rest, w_a, w_b, w_c, v_a, v_b, v_c, out_ref, lhs, result, sems = refs[chips + 3 :]
     count, width = opened.shape
     half = GROUP // 2
     row, col = lax.axis_index("row"), lax.axis_index("col")
@@ -295,10 +294,10 @@
     *late, near_early = in_order(order, pieces)
     for zs, piece in enumerate(late):
         if zs == NEAR:
-            early = channel_part(near_early, feat_hi[0], feat_lo[0])
+            early = channel_part(near_early, feat[0])
         else:
             early = spect[zs]
-        whole = (channel_part(piece, feat_hi[1], feat_lo[1]) + early).astype(jnp.bfloat16)
+        whole = (channel_part(piece, feat[1]) + early).astype(jnp.bfloat16)
         for h in range(2):
             spot = pl.ds(pl.multiple_of((core ^ h) * half, half), half)
             lhs[zs, :, spot] = whole[:, h * half : (h + 1) * half]
@@ -316,8 +315,11 @@
             rhs = jnp.concatenate([w_here[:, cols], w_there[:, cols]], axis=0)
             total += jnp.dot(lhs[chip ^ col ^ s], rhs, preferred_element_type=jnp.float32)
         result[:, cols] = (opened[:, cols] * total).astype(jnp.bfloat16)
-        copies.append(pltpu.make_async_copy(result.at[:, cols], out_ref.at[:, cols], sems.at[t]))
-        copies[-1].start()
+        if (t + 1) % SPAN == 0:
+            span = slice((t + 1 - SPAN) * GROUP, (t + 1) * GROUP)
+            copy = pltpu.make_async_copy(result.at[:, span], out_ref.at[:, span], sems.at[t // SPAN])
+            copy.start()
+            copies.append(copy)
     for copy in copies:
         copy.wait()
 
@@ -336,7 +338,7 @@
 
 
 def send_order(chips):
-    return sorted(range(1, chips), key=lambda zs: (zs < 2, zs))
+    return sorted(range(1, chips), reverse=True)
 
 
 def across_chips(pieces, rows):
@@ -364,7 +366,7 @@
     table_hi, table_lo = split_halves(position_table(count, scale))
     narrow = jnp.asarray(twist_table(rows, count))
     features_of = feature_table(lanes // 2)
-    feat_hi, feat_lo = split_halves(features_of)
+    feat = np.concatenate(split_halves(features_of), axis=1)
     bf = jnp.bfloat16
     fast = w_proj.shape[0] == GROUP and CHUNKS * lanes == GROUP and n_col == chips == 4
 
@@ -379,8 +381,8 @@
         in_specs=[pl.BlockSpec(memory_space=pltpu.HBM)] * 3,
         out_specs=[pl.BlockSpec(memory_space=pltpu.VMEM)] * (CHUNKS * chips + 2 * fast),
         scratch_shapes=[
-            pltpu.VMEM((chips, count, GROUP), bf),
-            pltpu.SemaphoreType.DMA((chips,)),
+            pltpu.VMEM((count, features), bf),
+            pltpu.SemaphoreType.DMA,
             pltpu.SemaphoreType.DMA((3,)),
         ],
         compiler_params=pltpu.CompilerParams(vmem_limit_bytes=24 * MIB),
@@ -459,11 +461,11 @@
             [],
             2 * count * features * GROUP,
             6 * count * width,
-        )(*early, feat_hi[0], feat_lo[0], gate)
+        )(*early, feat, gate)
         return pl.pallas_call(
             functools.partial(final_kernel, rows),
             out_shape=jax.ShapeDtypeStruct((count, width), bf),
-            in_specs=[pl.BlockSpec(memory_space=pltpu.VMEM)] * (chips + 12),
+            in_specs=[pl.BlockSpec(memory_space=pltpu.VMEM)] * (chips + 11),
             out_specs=pl.BlockSpec(memory_space=pl.ANY),
             scratch_shapes=[
                 pltpu.VMEM((chips, count, GROUP), bf),
@@ -476,7 +478,7 @@
                 bytes_accessed=2 * features * width,
                 transcendentals=0,
             ),
-        )(*late, feat_hi, feat_lo, spect, opened, mine, rest, w_a, w_b, w_c, *others)
+        )(*late, feat, spect, opened, mine, rest, w_a, w_b, w_c, *others)
 
     weights = lax.all_gather(w_proj, "col", axis=0, tiled=True).reshape(-1, GROUP, width)
     order = order_rows(rows, count)

time: 65.4 us -> 64.8 us (level)
  Pallas kernels: 7.94 us -> 7.21 us
where the time goes in v7:
time: 64.8 us; the launch traced here: 64.6 us
  waiting for transfers between devices  35.3 us (54%)
  starting transfers between devices  21.9 us (34%)
  Pallas kernels  7.21 us (11%)
    ppermute x17, waiting for transfers between devices, swap(): return lax.ppermute(value, axis, [(i, i ^ bit) for i in range(size)])  24.6 us
    ppermute x17, starting transfers between devices, swap(): return lax.ppermute(value, axis, [(i, i ^ bit) for i in range(size)])  15.8 us
    ppermute x3, waiting for transfers between devices, turn_swap(): return lax.ppermute(value, ('row', 'col'), turn)  10.7 us
    ppermute x3, starting transfers between devices, turn_swap(): return lax.ppermute(value, ('row', 'col'), turn)  6.11 us
    pallas_call x1, Pallas kernels, program(): pl.pallas_call(functools.partial(final_kernel, rows), out_shape=jax.Shape...  2.54 us
    pallas_call x2, Pallas kernels, program(): vmem_call(functools.partial(position_kernel, rows, q), made[q], [pltpu.VM...  2.16 us
    pallas_call x1, Pallas kernels, program(): pl.pallas_call(functools.partial(pick_kernel, chips, fast), out_shape=[ja...  1.49 us
  transfers between devices with their start and end apart: 20, of which 10 were waited for; matrix products, arithmetic and copies ran while one was open for 0% of the time, Pallas kernels for 5%

profile of v7, /device:TPU:0, one launch (start us, length us, event | category | flops | bytes accessed | tf_op | source)
XLA Modules:
  0.0 64.6 jit_solution(12670030980147747921)
XLA Ops:
  0.0 1.5 %shard_map.73 = (bf16[256,128]{1,0:T(8,128)(2,1)S(1)}, bf16[2,256,128]{2,1,0:T(8,128)(2,1)S(1)}, bf16[256,128]{1,0:T(8,128)(2,1)S(1)}, bf16[256,128]{1,0:T(8,128...) custom-call(bf16[256,1024]{1,0:T(8,128)(2,1)} %bitcast.4, ...), custom_call_target="tpu_custom_call" | custom-call | flops 134217728 | bytes 1048576 | tf_op jit(solution)/shard_map/pallas_call | solution.py:374
  1.5 3.0 %collective-permute-start.14 = (bf16[128,2048]{1,0:T(8,128)(2,1)S(1)}, bf16[128,2048]{1,0:T(8,128)(2,1)S(1)}, u32[]{:S(2)}, u32[]{:S(2)}) collective-permute-start(bf16[128,2048]{1,0:T(8,128)(2,1)S(1)} %get-tuple-element.49.refs_7_), channel_id=1, source_target_pairs={{0,1},{1,0},{2,3},{3,2},{4,6},{5,7},{6,4},{7,5},{8,9},{9,8},{10,11... | collective-permute-start | bytes 1572872 | tf_op jit(solution)/shard_map/ppermute | solution.py:337
  4.5 1.5 %collective-permute-start.15 = (bf16[128,2048]{1,0:T(8,128)(2,1)S(1)}, bf16[128,2048]{1,0:T(8,128)(2,1)S(1)}, u32[]{:S(2)}, u32[]{:S(2)}) collective-permute-start(bf16[128,2048]{1,0:T(8,128)(2,1)S(1)} %get-tuple-element.49.refs_7_), channel_id=1, source_target_pairs={{0,2},{1,3},{2,0},{3,1},{4,5},{5,4},{6,7},{7,6},{8,10},{9,11},{10,... | collective-permute-start | bytes 1572872 | tf_op jit(solution)/shard_map/ppermute | solution.py:337
  6.1 10.7 %collective-permute-done.14.refs_9_ = bf16[128,2048]{1,0:T(8,128)(2,1)S(1)} collective-permute-done((bf16[128,2048]{1,0:T(8,128)(2,1)S(1)}, bf16[128,2048]{1,0:T(8,128)(2,1)S(1)}, u32[]{:S(2)}, u32[]{:S(2)}) %collective-permute-start.14) | collective-permute-done | bytes 524320 | tf_op jit(solution)/shard_map/ppermute | solution.py:337
  16.7 1.6 %collective-permute-start.16 = (bf16[128,2048]{1,0:T(8,128)(2,1)S(1)}, bf16[128,2048]{1,0:T(8,128)(2,1)S(1)}, u32[]{:S(2)}, u32[]{:S(2)}) collective-permute-start(bf16[128,2048]{1,0:T(8,128)(2,1)S(1)} %collective-permute-done.14.refs_9_), channel_id=1, source_target_pairs={{0,2},{1,3},{2,0},{3,1},{4,5},{5,4},{6,7},{7,6},{8,10},{9,11},{10,... | collective-permute-start | bytes 1572872 | tf_op jit(solution)/shard_map/ppermute | solution.py:337
  18.3 1.7 %collective-permute-start = (bf16[2,256,128]{2,1,0:T(8,128)(2,1)S(1)}, bf16[2,256,128]{2,1,0:T(8,128)(2,1)S(1)}, u32[]{:S(2)}, u32[]{:S(2)}) collective-permute-start(bf16[2,256,128]{2,1,0:T(8,128)(2,1)S(1)} %get-tuple-element.29), channel_id=1, source_target_pairs={{0,8},{4,12},{8,0},{12,4},{16,24},{20,28},{24,16},{28,20},{1,9},{5... | collective-permute-start | bytes 393224 | tf_op jit(solution)/shard_map/ppermute | solution.py:328
  20.0 2.6 %collective-permute-start.4 = (bf16[256,128]{1,0:T(8,128)(2,1)S(1)}, bf16[256,128]{1,0:T(8,128)(2,1)S(1)}, u32[]{:S(2)}, u32[]{:S(2)}) collective-permute-start(bf16[256,128]{1,0:T(8,128)(2,1)S(1)} %get-tuple-element.34), channel_id=1, source_target_pairs={{0,16},{4,20},{8,24},{12,28},{16,0},{20,4},{24,8},{28,12},{1,17},{... | collective-permute-start | bytes 196616 | tf_op jit(solution)/shard_map/ppermute | solution.py:328
  22.6 0.1 collective-permute-start.5
  22.7 3.5 %collective-permute-done.4.refs_2_ = bf16[256,128]{1,0:T(8,128)(2,1)S(1)} collective-permute-done((bf16[256,128]{1,0:T(8,128)(2,1)S(1)}, bf16[256,128]{1,0:T(8,128)(2,1)S(1)}, u32[]{:S(2)}, u32[]{:S(2)}) %collective-permute-start.4) | collective-permute-done | bytes 65568 | tf_op jit(solution)/shard_map/ppermute | solution.py:328
  26.2 1.7 %collective-permute-start.1 = (bf16[256,128]{1,0:T(8,128)(2,1)S(1)}, bf16[256,128]{1,0:T(8,128)(2,1)S(1)}, u32[]{:S(2)}, u32[]{:S(2)}) collective-permute-start(bf16[256,128]{1,0:T(8,128)(2,1)S(1)} %get-tuple-element.30), channel_id=1, source_target_pairs={{0,16},{4,20},{8,24},{12,28},{16,0},{20,4},{24,8},{28,12},{1,17},{... | collective-permute-start | bytes 196616 | tf_op jit(solution)/shard_map/ppermute | solution.py:328
  27.9 0.8 %collective-permute-done.5.refs_3_ = bf16[256,128]{1,0:T(8,128)(2,1)S(1)} collective-permute-done((bf16[256,128]{1,0:T(8,128)(2,1)S(1)}, bf16[256,128]{1,0:T(8,128)(2,1)S(1)}, u32[]{:S(2)}, u32[]{:S(2)}) %collective-permute-start.5) | collective-permute-done | bytes 65568 | tf_op jit(solution)/shard_map/ppermute | solution.py:328
  28.7 1.6 %collective-permute-start.2 = (bf16[256,128]{1,0:T(8,128)(2,1)S(1)}, bf16[256,128]{1,0:T(8,128)(2,1)S(1)}, u32[]{:S(2)}, u32[]{:S(2)}) collective-permute-start(bf16[256,128]{1,0:T(8,128)(2,1)S(1)} %get-tuple-element.31), channel_id=1, source_target_pairs={{0,24},{4,28},{8,16},{12,20},{16,8},{20,12},{24,0},{28,4},{1,25},{... | collective-permute-start | bytes 196616 | tf_op jit(solution)/shard_map/ppermute | solution.py:328
  30.4 1.1 %collective-permute-done.1.refs_2_ = bf16[256,128]{1,0:T(8,128)(2,1)S(1)} collective-permute-done((bf16[256,128]{1,0:T(8,128)(2,1)S(1)}, bf16[256,128]{1,0:T(8,128)(2,1)S(1)}, u32[]{:S(2)}, u32[]{:S(2)}) %collective-permute-start.1) | collective-permute-done | bytes 65568 | tf_op jit(solution)/shard_map/ppermute | solution.py:328
  31.4 3.3 %collective-permute-done.2.refs_3_ = bf16[256,128]{1,0:T(8,128)(2,1)S(1)} collective-permute-done((bf16[256,128]{1,0:T(8,128)(2,1)S(1)}, bf16[256,128]{1,0:T(8,128)(2,1)S(1)}, u32[]{:S(2)}, u32[]{:S(2)}) %collective-permute-start.2) | collective-permute-done | bytes 65568 | tf_op jit(solution)/shard_map/ppermute | solution.py:328
  34.8 0.1 collective-permute-start.3
  34.8 0.5 collective-permute-start.17
  35.3 0.1 collective-permute-start.18
  35.4 0.4 collective-permute-start.19
  35.9 0.3 shard_map.75.refs_7_
  36.3 1.1 %shard_map.77 = (bf16[2,128,128]{2,1,0:T(8,128)(2,1)S(1)}, bf16[2,128,128]{2,1,0:T(8,128)(2,1)S(1)}, bf16[2,128,128]{2,1,0:T(8,128)(2,1)S(1)}, bf16[128,128]{1,0:T(8,128)(2,1)S(1)}, bf16[128,128]{1,0:T(8,128)(2,1)S(1)}) custom-call(bf16[256,128]{1,0:T(8,128)(2,1)S(1)} %get-tuple-element.33.refs_0_, bf16[2,256,128]{2,1,0:T(8,128)(2,1)S(1)} %collective-permute-done.refs_1_, ...), custom_call_target="tpu_custom_call" | custom-call | flops 268435456 | bytes 1048576 | tf_op jit(solution)/shard_map/pallas_call | solution.py:431
  37.3 1.2 %collective-permute-start.11 = (bf16[2,128,128]{2,1,0:T(8,128)(2,1)S(1)}, bf16[2,128,128]{2,1,0:T(8,128)(2,1)S(1)}, u32[]{:S(2)}, u32[]{:S(2)}) collective-permute-start(bf16[2,128,128]{2,1,0:T(8,128)(2,1)S(1)} %get-tuple-element.45), channel_id=1, source_target_pairs={{0,16},{4,20},{8,24},{12,28},{16,0},{20,4},{24,8},{28,12},{1,17},{... | collective-permute-start | bytes 196616 | tf_op jit(solution)/shard_map/ppermute | solution.py:328
  38.5 1.1 %shard_map.78 = (bf16[4,128,128]{2,1,0:T(8,128)(2,1)S(1)}, bf16[5,128,128]{2,1,0:T(8,128)(2,1)S(1)}) custom-call(bf16[256,128]{1,0:T(8,128)(2,1)S(1)} %get-tuple-element.28.refs_0_, bf16[2,256,128]{2,1,0:T(8,128)(2,1)S(1)} %collective-permute-done.refs_1_, bf16[256,128]{1,0:T(8,128)(2,1)S(1)} %collective-permute-done.1.refs_2_, ...), custom_call_target="tpu_custom_call" | custom-call | flops 268435456 | bytes 1048576 | tf_op jit(solution)/shard_map/pallas_call | solution.py:431
  39.7 3.4 %collective-permute-done.11.refs_1_ = bf16[2,128,128]{2,1,0:T(8,128)(2,1)S(1)} collective-permute-done((bf16[2,128,128]{2,1,0:T(8,128)(2,1)S(1)}, bf16[2,128,128]{2,1,0:T(8,128)(2,1)S(1)}, u32[]{:S(2)}, u32[]{:S(2)}) %collective-permute-start.11) | collective-permute-done | bytes 65568 | tf_op jit(solution)/shard_map/ppermute | solution.py:328
  43.1 2.4 %collective-permute-start.12 = (bf16[2,128,128]{2,1,0:T(8,128)(2,1)S(1)}, bf16[2,128,128]{2,1,0:T(8,128)(2,1)S(1)}, u32[]{:S(2)}, u32[]{:S(2)}) collective-permute-start(bf16[2,128,128]{2,1,0:T(8,128)(2,1)S(1)} %get-tuple-element.46), channel_id=1, source_target_pairs={{0,24},{4,28},{8,16},{12,20},{16,8},{20,12},{24,0},{28,4},{1,25},{... | collective-permute-start | bytes 196616 | tf_op jit(solution)/shard_map/ppermute | solution.py:328
  45.5 3.7 %collective-permute-done.12.refs_2_ = bf16[2,128,128]{2,1,0:T(8,128)(2,1)S(1)} collective-permute-done((bf16[2,128,128]{2,1,0:T(8,128)(2,1)S(1)}, bf16[2,128,128]{2,1,0:T(8,128)(2,1)S(1)}, u32[]{:S(2)}, u32[]{:S(2)}) %collective-permute-start.12) | collective-permute-done | bytes 65568 | tf_op jit(solution)/shard_map/ppermute | solution.py:328
  49.4 1.2 %collective-permute-done.13.refs_3_ = bf16[3,128,128]{2,1,0:T(8,128)(2,1)S(1)} collective-permute-done((bf16[3,128,128]{2,1,0:T(8,128)(2,1)S(1)}, bf16[3,128,128]{2,1,0:T(8,128)(2,1)S(1)}, u32[]{:S(2)}, u32[]{:S(2)}) %collective-permute-start.13) | collective-permute-done | bytes 98336 | tf_op jit(solution)/shard_map/ppermute | solution.py:328
  50.5 1.8 %collective-permute-start.8 = (bf16[4,128,128]{2,1,0:T(8,128)(2,1)S(1)}, bf16[4,128,128]{2,1,0:T(8,128)(2,1)S(1)}, u32[]{:S(2)}, u32[]{:S(2)}) collective-permute-start(bf16[4,128,128]{2,1,0:T(8,128)(2,1)S(1)} %get-tuple-element.41), channel_id=1, source_target_pairs={{0,8},{4,12},{8,0},{12,4},{16,24},{20,28},{24,16},{28,20},{1,9},{5... | collective-permute-start | bytes 393224 | tf_op jit(solution)/shard_map/ppermute | solution.py:328
  52.3 3.7 %collective-permute-done.9.refs_2_ = bf16[2,128,128]{2,1,0:T(8,128)(2,1)S(1)} collective-permute-done((bf16[2,128,128]{2,1,0:T(8,128)(2,1)S(1)}, bf16[2,128,128]{2,1,0:T(8,128)(2,1)S(1)}, u32[]{:S(2)}, u32[]{:S(2)}) %collective-permute-start.9) | collective-permute-done | bytes 65568 | tf_op jit(solution)/shard_map/ppermute | solution.py:328
  56.0 1.4 %collective-permute-start.10 = (bf16[2,128,128]{2,1,0:T(8,128)(2,1)S(1)}, bf16[2,128,128]{2,1,0:T(8,128)(2,1)S(1)}, u32[]{:S(2)}, u32[]{:S(2)}) collective-permute-start(bf16[2,128,128]{2,1,0:T(8,128)(2,1)S(1)} %get-tuple-element.43), channel_id=1, source_target_pairs={{0,24},{4,28},{8,16},{12,20},{16,8},{20,12},{24,0},{28,4},{1,25},{... | collective-permute-start | bytes 196616 | tf_op jit(solution)/shard_map/ppermute | solution.py:328
  57.4 0.6 shard_map.81
  58.0 4.0 %collective-permute-done.10.refs_3_ = bf16[2,128,128]{2,1,0:T(8,128)(2,1)S(1)} collective-permute-done((bf16[2,128,128]{2,1,0:T(8,128)(2,1)S(1)}, bf16[2,128,128]{2,1,0:T(8,128)(2,1)S(1)}, u32[]{:S(2)}, u32[]{:S(2)}) %collective-permute-start.10) | collective-permute-done | bytes 65568 | tf_op jit(solution)/shard_map/ppermute | solution.py:328
  62.1 2.5 %shard_map.82 = bf16[256,2048]{1,0:T(8,128)(2,1)} custom-call(bf16[2,128,128]{2,1,0:T(8,128)(2,1)S(1)} %get-tuple-element.40.refs_0_, bf16[4,128,128]{2,1,0:T(8,128)(2,1)S(1)} %collective-permute-done.8.refs_1_, bf16[2,128,128]{2,1,0:T(8,128)(2,1)S(1)} %collective-permute-done.9.refs_2_, bf16[2,128,128]{2,1,0:T(8,128)(2,1)S(1)} %collective-permute-done.10.refs_3_, ...), custom_call_target="tpu_custom_call" | custom-call | flops 1073741824 | bytes 4194304 | tf_op jit(solution)/shard_map/pallas_call | solution.py:465
  (26 shorter events, 0.4 us)
Async XLA Ops:
  0.0 36.2 %copy-start.1 = (bf16[256,512]{1,0:T(8,128)(2,1)S(1)}, bf16[256,512]{1,0:T(8,128)(2,1)}, u32[]{:S(2)}) copy-start(bf16[256,512]{1,0:T(8,128)(2,1)} %constant.10.clone.refs_6_) | copy-start | bytes 786436
  0.0 36.2 %copy-start.2 = (bf16[256,512]{1,0:T(8,128)(2,1)S(1)}, bf16[256,512]{1,0:T(8,128)(2,1)}, u32[]{:S(2)}) copy-start(bf16[256,512]{1,0:T(8,128)(2,1)} %constant.9.clone.refs_5_) | copy-start | bytes 786436
  1.5 15.2 %collective-permute-start.14 = (bf16[128,2048]{1,0:T(8,128)(2,1)S(1)}, bf16[128,2048]{1,0:T(8,128)(2,1)S(1)}, u32[]{:S(2)}, u32[]{:S(2)}) collective-permute-start(bf16[128,2048]{1,0:T(8,128)(2,1)S(1)} %get-tuple-element.49.refs_7_), channel_id=1, source_target_pairs={{0,1},{1,0},{2,3},{3,2},{4,6},{5,7},{6,4},{7,5},{8,9},{9,8},{10,11... | collective-permute-start | bytes 1572872 | tf_op jit(solution)/shard_map/ppermute | solution.py:337
  4.5 30.8 %collective-permute-start.15 = (bf16[128,2048]{1,0:T(8,128)(2,1)S(1)}, bf16[128,2048]{1,0:T(8,128)(2,1)S(1)}, u32[]{:S(2)}, u32[]{:S(2)}) collective-permute-start(bf16[128,2048]{1,0:T(8,128)(2,1)S(1)} %get-tuple-element.49.refs_7_), channel_id=1, source_target_pairs={{0,2},{1,3},{2,0},{3,1},{4,5},{5,4},{6,7},{7,6},{8,10},{9,11},{10,... | collective-permute-start | bytes 1572872 | tf_op jit(solution)/shard_map/ppermute | solution.py:337
  16.7 18.7 %collective-permute-start.16 = (bf16[128,2048]{1,0:T(8,128)(2,1)S(1)}, bf16[128,2048]{1,0:T(8,128)(2,1)S(1)}, u32[]{:S(2)}, u32[]{:S(2)}) collective-permute-start(bf16[128,2048]{1,0:T(8,128)(2,1)S(1)} %collective-permute-done.14.refs_9_), channel_id=1, source_target_pairs={{0,2},{1,3},{2,0},{3,1},{4,5},{5,4},{6,7},{7,6},{8,10},{9,11},{10,... | collective-permute-start | bytes 1572872 | tf_op jit(solution)/shard_map/ppermute | solution.py:337
  18.3 12.0 %collective-permute-start = (bf16[2,256,128]{2,1,0:T(8,128)(2,1)S(1)}, bf16[2,256,128]{2,1,0:T(8,128)(2,1)S(1)}, u32[]{:S(2)}, u32[]{:S(2)}) collective-permute-start(bf16[2,256,128]{2,1,0:T(8,128)(2,1)S(1)} %get-tuple-element.29), channel_id=1, source_target_pairs={{0,8},{4,12},{8,0},{12,4},{16,24},{20,28},{24,16},{28,20},{1,9},{5... | collective-permute-start | bytes 393224 | tf_op jit(solution)/shard_map/ppermute | solution.py:328
  20.0 6.2 %collective-permute-start.4 = (bf16[256,128]{1,0:T(8,128)(2,1)S(1)}, bf16[256,128]{1,0:T(8,128)(2,1)S(1)}, u32[]{:S(2)}, u32[]{:S(2)}) collective-permute-start(bf16[256,128]{1,0:T(8,128)(2,1)S(1)} %get-tuple-element.34), channel_id=1, source_target_pairs={{0,16},{4,20},{8,24},{12,28},{16,0},{20,4},{24,8},{28,12},{1,17},{... | collective-permute-start | bytes 196616 | tf_op jit(solution)/shard_map/ppermute | solution.py:328
  22.6 6.1 %collective-permute-start.5 = (bf16[256,128]{1,0:T(8,128)(2,1)S(1)}, bf16[256,128]{1,0:T(8,128)(2,1)S(1)}, u32[]{:S(2)}, u32[]{:S(2)}) collective-permute-start(bf16[256,128]{1,0:T(8,128)(2,1)S(1)} %get-tuple-element.35), channel_id=1, source_target_pairs={{0,24},{4,28},{8,16},{12,20},{16,8},{20,12},{24,0},{28,4},{1,25},{... | collective-permute-start | bytes 196616 | tf_op jit(solution)/shard_map/ppermute | solution.py:328
  26.2 5.3 %collective-permute-start.1 = (bf16[256,128]{1,0:T(8,128)(2,1)S(1)}, bf16[256,128]{1,0:T(8,128)(2,1)S(1)}, u32[]{:S(2)}, u32[]{:S(2)}) collective-permute-start(bf16[256,128]{1,0:T(8,128)(2,1)S(1)} %get-tuple-element.30), channel_id=1, source_target_pairs={{0,16},{4,20},{8,24},{12,28},{16,0},{20,4},{24,8},{28,12},{1,17},{... | collective-permute-start | bytes 196616 | tf_op jit(solution)/shard_map/ppermute | solution.py:328
  28.7 6.1 %collective-permute-start.2 = (bf16[256,128]{1,0:T(8,128)(2,1)S(1)}, bf16[256,128]{1,0:T(8,128)(2,1)S(1)}, u32[]{:S(2)}, u32[]{:S(2)}) collective-permute-start(bf16[256,128]{1,0:T(8,128)(2,1)S(1)} %get-tuple-element.31), channel_id=1, source_target_pairs={{0,24},{4,28},{8,16},{12,20},{16,8},{20,12},{24,0},{28,4},{1,25},{... | collective-permute-start | bytes 196616 | tf_op jit(solution)/shard_map/ppermute | solution.py:328
  30.3 5.9 %collective-permute-start.6 = (bf16[4,256,128]{2,1,0:T(8,128)(2,1)S(1)}, bf16[4,256,128]{2,1,0:T(8,128)(2,1)S(1)}, u32[]{:S(2)}, u32[]{:S(2)}) collective-permute-start(bf16[4,256,128]{2,1,0:T(8,128)(2,1)S(1)} %shard_map.76), channel_id=1, source_target_pairs={{0,4},{4,0},{8,12},{12,8},{16,20},{20,16},{24,28},{28,24},{1,5},{5... | collective-permute-start | bytes 786440 | tf_op jit(solution)/shard_map/ppermute | solution.py:328
  34.8 3.8 %collective-permute-start.3 = (bf16[4,256,128]{2,1,0:T(8,128)(2,1)S(1)}, bf16[4,256,128]{2,1,0:T(8,128)(2,1)S(1)}, u32[]{:S(2)}, u32[]{:S(2)}) collective-permute-start(bf16[4,256,128]{2,1,0:T(8,128)(2,1)S(1)} %shard_map.74), channel_id=1, source_target_pairs={{0,4},{4,0},{8,12},{12,8},{16,20},{20,16},{24,28},{28,24},{1,5},{5... | collective-permute-start | bytes 786440 | tf_op jit(solution)/shard_map/ppermute | solution.py:328
  34.8 27.2 %collective-permute-start.17 = (bf16[128,2048]{1,0:T(8,128)(2,1)S(1)}, bf16[128,2048]{1,0:T(8,128)(2,1)S(1)}, u32[]{:S(2)}, u32[]{:S(2)}) collective-permute-start(bf16[128,2048]{1,0:T(8,128)(2,1)S(1)} %collective-permute-done.14.refs_9_), channel_id=1, source_target_pairs={{0,4},{4,0},{8,12},{12,8},{16,20},{20,16},{24,28},{28,24},{1,5},{5... | collective-permute-start | bytes 1572872 | tf_op jit(solution)/shard_map/ppermute | solution.py:328
  35.3 26.7 %collective-permute-start.18 = (bf16[128,2048]{1,0:T(8,128)(2,1)S(1)}, bf16[128,2048]{1,0:T(8,128)(2,1)S(1)}, u32[]{:S(2)}, u32[]{:S(2)}) collective-permute-start(bf16[128,2048]{1,0:T(8,128)(2,1)S(1)} %collective-permute-done.15.refs_10_), channel_id=1, source_target_pairs={{0,4},{4,0},{8,12},{12,8},{16,20},{20,16},{24,28},{28,24},{1,5},{5... | collective-permute-start | bytes 1572872 | tf_op jit(solution)/shard_map/ppermute | solution.py:328
  35.4 26.6 %collective-permute-start.19 = (bf16[128,2048]{1,0:T(8,128)(2,1)S(1)}, bf16[128,2048]{1,0:T(8,128)(2,1)S(1)}, u32[]{:S(2)}, u32[]{:S(2)}) collective-permute-start(bf16[128,2048]{1,0:T(8,128)(2,1)S(1)} %collective-permute-done.16.refs_11_), channel_id=1, source_target_pairs={{0,4},{4,0},{8,12},{12,8},{16,20},{20,16},{24,28},{28,24},{1,5},{5... | collective-permute-start | bytes 1572872 | tf_op jit(solution)/shard_map/ppermute | solution.py:328
  36.2 21.2 %copy-start = (bf16[2,256,256]{2,1,0:T(8,128)(2,1)S(1)}, bf16[2,256,256]{2,1,0:T(8,128)(2,1)}, u32[]{:S(2)}) copy-start(bf16[2,256,256]{2,1,0:T(8,128)(2,1)} %constant.11.clone.refs_4_) | copy-start | bytes 786436
  36.2 21.2 %copy-start.3 = (bf16[1,256,2048]{2,1,0:T(8,128)(2,1)S(1)}, bf16[1,256,2048]{2,1,0:T(8,128)(2,1)}, u32[]{:S(2)}) copy-start(bf16[1,256,2048]{2,1,0:T(8,128)(2,1)} %param.8) | copy-start | bytes 3145732
  37.3 5.7 %collective-permute-start.11 = (bf16[2,128,128]{2,1,0:T(8,128)(2,1)S(1)}, bf16[2,128,128]{2,1,0:T(8,128)(2,1)S(1)}, u32[]{:S(2)}, u32[]{:S(2)}) collective-permute-start(bf16[2,128,128]{2,1,0:T(8,128)(2,1)S(1)} %get-tuple-element.45), channel_id=1, source_target_pairs={{0,16},{4,20},{8,24},{12,28},{16,0},{20,4},{24,8},{28,12},{1,17},{... | collective-permute-start | bytes 196616 | tf_op jit(solution)/shard_map/ppermute | solution.py:328
  39.6 9.6 %collective-permute-start.7 = (bf16[5,128,128]{2,1,0:T(8,128)(2,1)S(1)}, bf16[5,128,128]{2,1,0:T(8,128)(2,1)S(1)}, u32[]{:S(2)}, u32[]{:S(2)}) collective-permute-start(bf16[5,128,128]{2,1,0:T(8,128)(2,1)S(1)} %get-tuple-element.38), channel_id=1, source_target_pairs={{0,4},{4,0},{8,12},{12,8},{16,20},{20,16},{24,28},{28,24},{1,5},{5... | collective-permute-start | bytes 491528 | tf_op jit(solution)/shard_map/ppermute | solution.py:328
  43.1 6.1 %collective-permute-start.12 = (bf16[2,128,128]{2,1,0:T(8,128)(2,1)S(1)}, bf16[2,128,128]{2,1,0:T(8,128)(2,1)S(1)}, u32[]{:S(2)}, u32[]{:S(2)}) collective-permute-start(bf16[2,128,128]{2,1,0:T(8,128)(2,1)S(1)} %get-tuple-element.46), channel_id=1, source_target_pairs={{0,24},{4,28},{8,16},{12,20},{16,8},{20,12},{24,0},{28,4},{1,25},{... | collective-permute-start | bytes 196616 | tf_op jit(solution)/shard_map/ppermute | solution.py:328
  49.2 1.4 %collective-permute-start.13 = (bf16[3,128,128]{2,1,0:T(8,128)(2,1)S(1)}, bf16[3,128,128]{2,1,0:T(8,128)(2,1)S(1)}, u32[]{:S(2)}, u32[]{:S(2)}) collective-permute-start(bf16[3,128,128]{2,1,0:T(8,128)(2,1)S(1)} %shard_map.80), channel_id=1, source_target_pairs={{0,4},{4,0},{8,12},{12,8},{16,20},{20,16},{24,28},{28,24},{1,5},{5... | collective-permute-start | bytes 294920 | tf_op jit(solution)/shard_map/ppermute | solution.py:328
  49.3 6.7 %collective-permute-start.9 = (bf16[2,128,128]{2,1,0:T(8,128)(2,1)S(1)}, bf16[2,128,128]{2,1,0:T(8,128)(2,1)S(1)}, u32[]{:S(2)}, u32[]{:S(2)}) collective-permute-start(bf16[2,128,128]{2,1,0:T(8,128)(2,1)S(1)} %get-tuple-element.42), channel_id=1, source_target_pairs={{0,16},{4,20},{8,24},{12,28},{16,0},{20,4},{24,8},{28,12},{1,17},{... | collective-permute-start | bytes 196616 | tf_op jit(solution)/shard_map/ppermute | solution.py:328
  50.5 11.5 %collective-permute-start.8 = (bf16[4,128,128]{2,1,0:T(8,128)(2,1)S(1)}, bf16[4,128,128]{2,1,0:T(8,128)(2,1)S(1)}, u32[]{:S(2)}, u32[]{:S(2)}) collective-permute-start(bf16[4,128,128]{2,1,0:T(8,128)(2,1)S(1)} %get-tuple-element.41), channel_id=1, source_target_pairs={{0,8},{4,12},{8,0},{12,4},{16,24},{20,28},{24,16},{28,20},{1,9},{5... | collective-permute-start | bytes 393224 | tf_op jit(solution)/shard_map/ppermute | solution.py:328
  56.0 6.1 %collective-permute-start.10 = (bf16[2,128,128]{2,1,0:T(8,128)(2,1)S(1)}, bf16[2,128,128]{2,1,0:T(8,128)(2,1)S(1)}, u32[]{:S(2)}, u32[]{:S(2)}) collective-permute-start(bf16[2,128,128]{2,1,0:T(8,128)(2,1)S(1)} %get-tuple-element.43), channel_id=1, source_target_pairs={{0,24},{4,28},{8,16},{12,20},{16,8},{20,12},{24,0},{28,4},{1,25},{... | collective-permute-start | bytes 196616 | tf_op jit(solution)/shard_map/ppermute | solution.py:328
